TPU v7x, 256 devices: a whole 4x4x8 slice. The times are simulated.
256 devices in a mesh: ep: 64 (over z, y, core), tp: 4 (over x).
Axes of the slice: x: 4, y: 4, z: 8, core: 2. Of those that a mesh axis runs over, the one named last changes fastest.
Arguments:
- tokens: bfloat16 [1536, 2048], P('ep'), may hold values from -6 to 6
- norm_attn: float32 [2048], replicated, may hold values from 0.1 to 1.9
- w_query: bfloat16 [2048, 2048], P(None, 'tp'), may hold values from -0.125 to 0.125
- w_key: bfloat16 [2048, 256], P(None, 'tp'), may hold values from -0.125 to 0.125
- w_value: bfloat16 [2048, 256], P(None, 'tp'), may hold values from -0.125 to 0.125
- w_out: bfloat16 [2048, 2048], P('tp'), may hold values from -1 to 1
- head_bias: float32 [32], P('tp'), may hold values from -7 to -3
- key_cache: bfloat16 [1536, 4, 1024, 64], P('ep', 'tp'), may hold values from -6 to 6
- value_cache: bfloat16 [1536, 4, 1024, 64], P('ep', 'tp'), may hold values from -6 to 6
- lengths: int32 [1536], P('ep'), may hold values from 1 to 1024, 786432 in all
- norm_ffn: float32 [2048], replicated, may hold values from 0.1 to 1.9
- w_group: bfloat16 [2048, 4], replicated, may hold values from -0.125 to 0.125
- w_fine: bfloat16 [2048, 64], replicated, may hold values from -0.125 to 0.125
- routes: int32 [1536, 2], P('ep'), may hold values from 0 to 63, as said below
- e_gate: bfloat16 [64, 2048, 512], P('ep', 'tp'), may hold values from -0.125 to 0.125
- e_up: bfloat16 [64, 2048, 512], P('ep', 'tp'), may hold values from -0.125 to 0.125
- e_down: bfloat16 [64, 512, 2048], P('ep', None, 'tp'), may hold values from -1 to 1
- d_gate: bfloat16 [2048, 8192], P('tp', 'ep'), may hold values from -0.125 to 0.125
- d_up: bfloat16 [2048, 8192], P('tp', 'ep'), may hold values from -0.125 to 0.125
- d_down: bfloat16 [8192, 2048], P('ep', 'tp'), may hold values from -0.25 to 0.25
- w_mix: float32 [2048], replicated, may hold values from -0.125 to 0.125
Outputs:
- mixed: bfloat16 [1536, 2048], P('ep', 'tp')
- new_keys: bfloat16 [1536, 4, 64], P('ep', 'tp')
- new_values: bfloat16 [1536, 4, 64], P('ep', 'tp')
Inputs may be any that keep to these rules, and one draw needn't show every extreme that they name: `routes`: the 2 experts of a row are distinct and lie in one group of 16 consecutive experts. Among the rows of one device each expert is named at most 2 times. One group, the same on every device, is named by exactly 16 rows of every device, so that each of its experts is named exactly 2 times by every device.
All inputs are finite; a program needn't handle non-finite values. No bound on the sum of `lengths` on one device may be relied on, other than what follows from the above.
Results may differ from a plain program's by a relative error of at most 0.019.
Values may be sent and summed in bfloat16 or wider, within the bound.
No kernel may reach another device: no remote copies, remote signals or barrier semaphores. Data moves between devices by JAX's collectives and lax.ppermute only.
A program may use at most 128 MiB of HBM per device.

v0:
```python
import jax
import jax.numpy as jnp
from jax import lax
from jax.sharding import Mesh
from jax.sharding import PartitionSpec as P

GROUPS = 4
TOP_K = 2
EP = ("ep_0", "ep_1", "ep_2")


norm_eps = 1e-06
segment_len = 128


def copy_for_each(x, axis):
    devices = lax.axis_size(axis)
    return lax.all_to_all(jnp.broadcast_to(x[None], (devices, *x.shape)), axis, 0, 0, tiled=True)


def over_copies(x, axis):
    everything = copy_for_each(x, axis)
    return jnp.sum(everything.astype(jnp.float32), axis=0)


def in_order(tiles, dim):
    lengths = list(tiles.shape[1:])
    lengths[dim] *= tiles.shape[0]
    return jnp.moveaxis(tiles, 0, dim).reshape(lengths)


def all_blocks(x, axes, sequence):
    tiles = x[None]
    for k in sequence:
        tiles = lax.all_gather(tiles, axes[k], axis=0, tiled=True)
    current = [lax.axis_size(axes[k]) for k in reversed(sequence)]
    tiles = tiles.reshape(*current, *x.shape)
    turned = sorted(range(len(sequence)), key=lambda place: sequence[len(sequence) - 1 - place])
    return tiles.transpose(*turned, *range(len(sequence), tiles.ndim)).reshape(-1, *x.shape)


def whole_of(x, axes, sequence, dim):
    return in_order(all_blocks(x, axes, sequence), dim)


def normed(values, gains):
    wide = values.astype(jnp.float32)
    return wide * lax.rsqrt(jnp.mean(wide * wide, axis=-1, keepdims=True) + norm_eps) * gains


def suffix_sums(terms):
    length = terms.shape[-1]
    pieces = length // segment_len
    shaped = terms.reshape(terms.shape[:-1] + (pieces, segment_len))
    inner = lax.iota(jnp.int32, segment_len)
    later_inner = (inner[:, None] > inner[None, :]).astype(jnp.float32)
    within = jnp.einsum("...ij,jk->...ik", shaped, later_inner, precision=lax.Precision.HIGHEST)
    outer = lax.iota(jnp.int32, pieces)
    later_outer = (outer[:, None] > outer[None, :]).astype(jnp.float32)
    carried = jnp.einsum(
        "...i,ij->...j", jnp.sum(shaped, axis=-1), later_outer, precision=lax.Precision.HIGHEST
    )
    return (within + carried[..., None]).reshape(terms.shape)


def stick_read(queries, keys, values, lengths, bias_table):
    scores = jnp.einsum("bkgd,bksd->bkgs", queries, keys, preferred_element_type=jnp.float32)
    scores = scores * queries.shape[-1] ** (-0.5) + bias_table[None, :, :, None]
    positions = lax.iota(jnp.int32, keys.shape[2])
    inside = (positions[None, :] < lengths[:, None])[:, None, None, :]
    fails = jnp.where(inside, jax.nn.log_sigmoid(-scores), 0.0)
    weights = jnp.where(inside, jnp.exp(jax.nn.log_sigmoid(scores) + suffix_sums(fails)), 0.0)
    result = jnp.einsum(
        "bkgs,bksd->bkgd", weights.astype(jnp.bfloat16), values, preferred_element_type=jnp.float32
    )
    return result.astype(jnp.bfloat16).reshape(queries.shape[0], -1)


def route_weights(group_logits, fine_logits, chosen, per_group):
    group_iota = lax.iota(jnp.int32, group_logits.shape[1])
    own_group = chosen[:, 0] // per_group
    own_logit = jnp.sum(
        jnp.where(group_iota[None, :] == own_group[:, None], group_logits, 0.0), axis=1
    )
    group_share = 1.0 / jnp.sum(jnp.exp(group_logits - own_logit[:, None]), axis=1)
    expert_iota = lax.iota(jnp.int32, fine_logits.shape[1])
    picked = jnp.sum(
        jnp.where(expert_iota[None, None, :] == chosen[:, :, None], fine_logits[:, None, :], 0.0),
        axis=2,
    )
    within = 1.0 / jnp.sum(jnp.exp(picked[:, None, :] - picked[:, :, None]), axis=2)
    return group_share[:, None] * within


def slot_ranks(flat_routes):
    count = flat_routes.shape[0]
    same_expert = flat_routes[:, None] == flat_routes[None, :]
    position = lax.iota(jnp.int32, count)
    earlier = position[None, :] < position[:, None]
    return jnp.sum(same_expert & earlier, axis=1)


def shards(
    tokens,
    norm_attn,
    w_query,
    w_key,
    w_value,
    w_out,
    head_bias,
    key_cache,
    value_cache,
    lengths,
    norm_ffn,
    w_group,
    w_fine,
    routes,
    e_gate,
    e_up,
    e_down,
    d_gate,
    d_up,
    d_down,
    w_mix,
):
    seq_count = tokens.shape[0]
    width_part = d_gate.shape[0]
    dense_units = d_gate.shape[1]
    expert_units = e_gate.shape[2]
    kv_local = key_cache.shape[1]
    head_dim = key_cache.shape[3]
    ep_size = lax.axis_size(EP)
    per_group = ep_size // GROUPS
    capacity = max(2, (seq_count + per_group - 1) // per_group)
    h_first = normed(tokens, norm_attn).astype(jnp.bfloat16)
    queries = jnp.dot(h_first, w_query, preferred_element_type=jnp.float32).astype(jnp.bfloat16)
    new_keys = jnp.dot(h_first, w_key, preferred_element_type=jnp.float32).astype(jnp.bfloat16)
    new_values = jnp.dot(h_first, w_value, preferred_element_type=jnp.float32).astype(jnp.bfloat16)
    grouped = queries.reshape(seq_count, kv_local, -1, head_dim)
    heads_out = stick_read(
        grouped, key_cache, value_cache, lengths, head_bias.reshape(kv_local, -1)
    )
    partial_value = jnp.dot(heads_out, w_out, preferred_element_type=jnp.float32).astype(
        jnp.bfloat16
    )
    attended = over_copies(
        lax.optimization_barrier(partial_value).astype(jnp.float32).astype(jnp.bfloat16), "tp"
    ).astype(jnp.float32)
    resid = tokens.astype(jnp.float32) + attended
    h_second = normed(resid, norm_ffn).astype(jnp.bfloat16)
    column = lax.axis_index("tp") * width_part
    h_slice = lax.dynamic_slice_in_dim(h_second, column, width_part, 1)
    resid_slice = lax.dynamic_slice_in_dim(resid, column, width_part, 1)
    dense_in = jnp.concatenate([d_gate, d_up], axis=1)
    expert_in = jnp.concatenate([e_gate[0], e_up[0]], axis=1)
    group_logits = jnp.dot(h_second, w_group, preferred_element_type=jnp.float32)
    fine_logits = jnp.dot(h_second, w_fine, preferred_element_type=jnp.float32)
    shares = route_weights(group_logits, fine_logits, routes, per_group)
    mix_gate = jax.nn.sigmoid(
        jnp.dot(h_second.astype(jnp.float32), w_mix, precision=lax.Precision.HIGHEST)
    )
    flat_routes = routes.reshape(-1)
    slot_ids = flat_routes * capacity + slot_ranks(flat_routes)
    onehot = (lax.iota(jnp.int32, ep_size * capacity)[:, None] == slot_ids[None, :]).astype(
        jnp.float32
    )
    repeated = jnp.repeat(h_slice, TOP_K, axis=0)
    outbound = jnp.dot(onehot.astype(jnp.bfloat16), repeated, preferred_element_type=jnp.float32)
    outbound = outbound.astype(jnp.bfloat16).reshape(ep_size, capacity, width_part)
    received = lax.all_to_all(outbound, EP, split_axis=0, concat_axis=0, tiled=True)
    flat_rows = received.reshape(-1, width_part)
    pre_act = over_copies(
        jnp.dot(flat_rows, expert_in, preferred_element_type=jnp.float32).astype(jnp.bfloat16), "tp"
    ).astype(jnp.float32)
    hidden = (jax.nn.silu(pre_act[:, :expert_units]) * pre_act[:, expert_units:]).astype(
        jnp.bfloat16
    )
    result = jnp.dot(hidden, e_down[0], preferred_element_type=jnp.float32).astype(jnp.bfloat16)
    returned = lax.all_to_all(
        result.reshape(received.shape), EP, split_axis=0, concat_axis=0, tiled=True
    )
    weighted = onehot * shares.reshape(-1)[None, :]
    moe_rows = jnp.dot(
        weighted.T,
        returned.reshape(-1, width_part).astype(jnp.float32),
        precision=lax.Precision.HIGHEST,
    )
    moe_slice = jnp.sum(moe_rows.reshape(seq_count, TOP_K, width_part), axis=1)
    dense_pre = jnp.dot(
        whole_of(h_slice, EP, (1, 0, 2), 0), dense_in, preferred_element_type=jnp.float32
    )
    dense_pre = over_copies(dense_pre.astype(jnp.bfloat16), "tp").astype(jnp.float32)
    dense_hidden = (jax.nn.silu(dense_pre[:, :dense_units]) * dense_pre[:, dense_units:]).astype(
        jnp.bfloat16
    )
    own_hidden = lax.all_to_all(dense_hidden, EP, split_axis=0, concat_axis=1, tiled=True)
    dense_slice = jnp.dot(
        own_hidden,
        lax.all_gather(d_down, EP, axis=0, tiled=True),
        preferred_element_type=jnp.float32,
    )
    mixed = resid_slice + moe_slice + mix_gate[:, None] * dense_slice
    return (
        mixed.astype(jnp.bfloat16),
        new_keys.reshape(seq_count, kv_local, head_dim),
        new_values.reshape(seq_count, kv_local, head_dim),
    )


def solution(mesh):
    torus = Mesh(mesh.devices.reshape(8, 4, 2, mesh.shape["tp"]), ("ep_0", "ep_1", "ep_2", "tp"))
    placed = (
        P(EP, None),
        P(),
        P(None, "tp"),
        P(None, "tp"),
        P(None, "tp"),
        P("tp", None),
        P("tp"),
        P(EP, "tp", None, None),
        P(EP, "tp", None, None),
        P(EP),
        P(),
        P(),
        P(),
        P(EP, None),
        P(EP, "tp", None),
        P(EP, "tp", None),
        P(EP, None, "tp"),
        P("tp", EP),
        P("tp", EP),
        P(EP, "tp"),
        P(),
    )
    return jax.shard_map(
        shards,
        mesh=torus,
        in_specs=placed,
        out_specs=(P(EP, "tp"), P(EP, "tp", None), P(EP, "tp", None)),
        check_vma=False,
    )
```

profile of v0, /device:TPU:1, one launch (start us, length us, event | category | flops | bytes accessed | tf_op | source)
XLA Modules:
  0.0 220.9 jit_solution(17859736883952036732)
XLA Ops:
  7.2 1.2 fusion.44
  8.4 2.1 convolution_convert_fusion.5
  12.1 1.4 fusion.70
  13.9 2.6 %convolution_add_fusion = f32[24,8,8,128]{3,2,1,0:T(8,128)} fusion(f32[24,8,8,128]{3,1,2,0:T(8,128)} %get-tuple-element.6, f32[24,8,8]{2,1,0:T(8,128)S(1)} %copy.68), kind=kOutput, calls=%fused_computation.10 | convolution fusion | flops 302202880 | bytes 1579008 | tf_op jit(solution)/shard_map/...ij,jk->...ik/dot_general | solution.py:57
  16.5 2.1 reshape.207
  18.7 3.3 %fusion.10 = bf16[24,8,64]{2,1,0:T(8,128)(2,1)S(1)} fusion(bf16[24,1,1024,64]{2,3,1,0:T(8,128)(2,1)} %param.29, f32[24,8,1024]{2,1,0:T(8,128)} %reshape.207, f32[24,8,1024]{2,1,0:T(8,128)} %copy-done.1, pred[24,1024]{1,0:T(8,128)(4,1)S(1)} %iota_compare_fusion), kind=kOutput, calls=%fused_computation.16 | convolution fusion | flops 27340800 | bytes 4767744 | tf_op jit(solution)/shard_map/bkgs,bksd->bkgd/dot_general | solution.py:73
  22.1 2.0 convolution_convert_fusion.1
  24.9 5.0 %all-to-all-start = ((bf16[4,24,2048]{2,1,0:T(8,128)(2,1)}), bf16[4,24,2048]{2,1,0:T(8,128)(2,1)S(1)}, u32[]{:S(2)}, u32[]{:S(2)}) async-start(bf16[4,24,2048]{2,1,0:T(8,128)(2,1)} %broadcast_in_dim.41), calls=%async_computation | async-start | bytes 786432 | tf_op jit(solution)/shard_map/all_to_all | solution.py:18
  29.8 6.2 %all-to-all-done = bf16[4,24,2048]{2,1,0:T(8,128)(2,1)S(1)} async-done(((bf16[4,24,2048]{2,1,0:T(8,128)(2,1)}), bf16[4,24,2048]{2,1,0:T(8,128)(2,1)S(1)}, u32[]{:S(2)}, u32[]{:S(2)}) %all-to-all-start) | async-done | bytes 393248 | tf_op jit(solution)/shard_map/all_to_all | solution.py:18
  38.0 10.2 %all-gather = bf16[96,512]{1,0:T(8,128)(2,1)S(1)} all-gather(bf16[24,512]{1,0:T(8,128)(2,1)S(1)} %constant_dynamic-slice_fusion), channel_id=2, replica_groups=mesh['ep_0'=8,'ep_1'=4,'ep_2'=2,'tp'=4] {'ep_1'}, dimensions={0}, use_global_device_ids=true | all-gather | bytes 122880 | tf_op jit(solution)/shard_map/all_gather | solution.py:35
  48.2 26.3 %all_gather.13 = bf16[32,24,512]{2,1,0:T(8,128)(2,1)} all-gather(bf16[4,24,512]{2,1,0:T(8,128)(2,1)S(1)} %bitcast.85), channel_id=1, replica_groups=mesh['ep_0'=8,'ep_1'=4,'ep_2'=2,'tp'=4] {'ep_0'}, dimensions={0}, use_global_device_ids=true | all-gather | bytes 884736 | tf_op jit(solution)/shard_map/all_gather | solution.py:35
  76.0 28.8 %all_to_all.44 = bf16[64,2,512]{2,1,0:T(2,128)(2,1)S(1)} all-to-all(bf16[64,2,512]{2,1,0:T(2,128)(2,1)S(1)} %reshape.212), channel_id=1, replica_groups=mesh['ep_0'=8,'ep_1'=4,'ep_2'=2,'tp'=4] {'ep_0','ep_1','ep_2'}, dimensions={0} | all-to-all | bytes 262144 | tf_op jit(solution)/shard_map/all_to_all | solution.py:170
  104.8 1.5 convolution_convert_fusion.2
  106.4 1.1 broadcast_in_dim.46
  107.5 4.2 %all-to-all-start.2 = ((bf16[4,128,1024]{2,1,0:T(8,128)(2,1)}), bf16[4,128,1024]{2,1,0:T(8,128)(2,1)}, u32[]{:S(2)}, u32[]{:S(2)}) async-start(bf16[4,128,1024]{2,1,0:T(8,128)(2,1)} %broadcast_in_dim.46), calls=%async_computation.2 | async-start | bytes 2097152 | tf_op jit(solution)/shard_map/all_to_all | solution.py:18
  111.8 1.7 copy.71
  113.5 1.5 convolution_convert_fusion
  115.0 11.6 %all-to-all-done.2 = bf16[4,128,1024]{2,1,0:T(8,128)(2,1)} async-done(((bf16[4,128,1024]{2,1,0:T(8,128)(2,1)}), bf16[4,128,1024]{2,1,0:T(8,128)(2,1)}, u32[]{:S(2)}, u32[]{:S(2)}) %all-to-all-start.2) | async-done | bytes 1048608 | tf_op jit(solution)/shard_map/all_to_all | solution.py:18
  126.6 3.1 %broadcast_in_dim.48 = bf16[4,1536,256]{2,1,0:T(8,128)(2,1)} broadcast(bf16[1536,256]{1,0:T(8,128)(2,1)} %convolution_convert_fusion), dimensions={1,2} | broadcast | bytes 3932160 | tf_op jit(solution)/shard_map/broadcast_in_dim | solution.py:18
  129.7 4.8 %all-to-all-start.4 = ((bf16[4,1536,256]{2,1,0:T(8,128)(2,1)}), bf16[4,1536,256]{2,1,0:T(8,128)(2,1)}, u32[]{:S(2)}, u32[]{:S(2)}) async-start(bf16[4,1536,256]{2,1,0:T(8,128)(2,1)} %broadcast_in_dim.48), calls=%async_computation.4 | async-start | bytes 6291456 | tf_op jit(solution)/shard_map/all_to_all | solution.py:18
  134.7 1.9 fusion.15
  136.5 1.8 fusion.16
  139.9 1.5 convert_reduce_fusion.1
  142.3 28.6 %all-to-all-done.4 = bf16[4,1536,256]{2,1,0:T(8,128)(2,1)} async-done(((bf16[4,1536,256]{2,1,0:T(8,128)(2,1)}), bf16[4,1536,256]{2,1,0:T(8,128)(2,1)}, u32[]{:S(2)}, u32[]{:S(2)}) %all-to-all-start.4) | async-done | bytes 3145760 | tf_op jit(solution)/shard_map/all_to_all | solution.py:18
  171.0 6.1 %all-to-all-start.3 = ((bf16[64,2,512]{2,1,0:T(2,128)(2,1)}), bf16[64,2,512]{2,1,0:T(2,128)(2,1)S(1)}, u32[]{:S(2)}, u32[]{:S(2)}) async-start(bf16[64,2,512]{2,1,0:T(2,128)(2,1)} %reshape.214), calls=%async_computation.3 | async-start | bytes 262144 | tf_op jit(solution)/shard_map/all_to_all | solution.py:179
  177.1 2.6 %convert_reduce_fusion = f32[1536,256]{1,0:T(8,128)S(1)} fusion(bf16[4,1536,256]{2,1,0:T(8,128)(2,1)} %all-to-all-done.4), kind=kLoop, calls=%fused_computation | loop fusion | flops 2752512 | bytes 4718592 | tf_op jit(solution)/shard_map/reduce_sum | solution.py:23
  180.8 7.6 %all-to-all-done.3 = bf16[64,2,512]{2,1,0:T(2,128)(2,1)S(1)} async-done(((bf16[64,2,512]{2,1,0:T(2,128)(2,1)}), bf16[64,2,512]{2,1,0:T(2,128)(2,1)S(1)}, u32[]{:S(2)}, u32[]{:S(2)}) %all-to-all-start.3) | async-done | bytes 131104 | tf_op jit(solution)/shard_map/all_to_all | solution.py:179
  189.0 4.5 %all-to-all-start.5 = ((bf16[64,24,128]{2,1,0:T(8,128)(2,1)}), bf16[64,24,128]{2,1,0:T(8,128)(2,1)S(1)}, u32[]{:S(2)}, u32[]{:S(2)}) async-start(bf16[64,24,128]{2,1,0:T(8,128)(2,1)} %bitcast.84), calls=%async_computation.5 | async-start | bytes 786432 | tf_op jit(solution)/shard_map/all_to_all | solution.py:196
  194.5 1.7 reshape.222
  196.2 1.8 convolution_reduce_fusion
  198.0 10.8 %all-to-all-done.5 = bf16[64,24,128]{2,1,0:T(8,128)(2,1)S(1)} async-done(((bf16[64,24,128]{2,1,0:T(8,128)(2,1)}), bf16[64,24,128]{2,1,0:T(8,128)(2,1)S(1)}, u32[]{:S(2)}, u32[]{:S(2)}) %all-to-all-start.5) | async-done | bytes 393248 | tf_op jit(solution)/shard_map/all_to_all | solution.py:196
  208.8 5.3 %fusion.14 = bf16[24,512]{1,0:T(8,128)(2,1)} fusion(bf16[8192,512]{1,0:T(8,128)(2,1)} %all-gather.6.cloned.1.call-done, f32[24,512]{1,0:T(8,128)} %convolution_reduce_fusion, f32[24,2048]{1,0:T(8,128)} %copy-done.2, s32[]{:T(128)S(6)} %select_n.41, f32[24]{0:T(128)S(1)} %fusion.20, bf16[64,24,128]{2,1,0:T(8,128)(2,1)S(1)} %all-to-all-done.5), kind=kOutput, calls=%fused_computation.20 | convolution fusion | flops 201375744 | bytes 8904804 | tf_op jit(solution)/shard_map/dot_general | solution.py:197
  (74 shorter events, 11.5 us)
Async XLA Ops:
  7.2 3.5 %copy-start = (bf16[24,1,1024,64]{2,3,1,0:T(8,128)(2,1)S(1)}, bf16[24,1,1024,64]{2,3,1,0:T(8,128)(2,1)}, u32[]{:S(2)}) copy-start(bf16[24,1,1024,64]{2,3,1,0:T(8,128)(2,1)} %param.28) | copy-start | bytes 9437188
  7.2 3.4 %copy-start.10 = (s32[24]{0:T(128)S(1)}, s32[24]{0:T(128)}, u32[]{:S(2)}) copy-start(s32[24]{0:T(128)} %param.30) | copy-start | bytes 292
  7.2 3.5 %copy-start.9 = (f32[8]{0:T(128)S(1)}, f32[8]{0:T(128)}, u32[]{:S(2)}) copy-start(f32[8]{0:T(128)} %param.27) | copy-start | bytes 100
  11.2 0.9 copy-start.1
  22.1 15.8 %copy-start.8 = (f32[2048]{0:T(1024)S(1)}, f32[2048]{0:T(1024)}, u32[]{:S(2)}) copy-start(f32[2048]{0:T(1024)} %param.31) | copy-start | bytes 24580
  24.9 50.4 %copy-start.6 = (s32[24,2]{0,1:T(2,128)S(1)}, s32[24,2]{0,1:T(2,128)}, u32[]{:S(2)}) copy-start(s32[24,2]{0,1:T(2,128)} %param.34) | copy-start | bytes 580
  24.9 11.2 %all-to-all-start = ((bf16[4,24,2048]{2,1,0:T(8,128)(2,1)}), bf16[4,24,2048]{2,1,0:T(8,128)(2,1)S(1)}, u32[]{:S(2)}, u32[]{:S(2)}) async-start(bf16[4,24,2048]{2,1,0:T(8,128)(2,1)} %broadcast_in_dim.41), calls=%async_computation | async-start | bytes 786432 | tf_op jit(solution)/shard_map/all_to_all | solution.py:18
  29.8 82.0 %all-gather.4.cloned.1.call-start = ((), (), s32[]{:S(2)}) async-start(), calls=%async_computation.6 | async-start | bytes 2359296 | tf_op jit(solution)/shard_map/all_gather | solution.py:35
  37.2 0.7 copy-start.2
  37.9 100.6 %copy-start.5 = (bf16[24,2048]{1,0:T(8,128)(2,1)}, bf16[24,2048]{1,0:T(8,128)(2,1)S(1)}, u32[]{:S(2)}) copy-start(bf16[24,2048]{1,0:T(8,128)(2,1)S(1)} %multiply_convert_fusion) | copy-start | bytes 294916
  74.5 134.3 %all-gather.6.cloned.1.call-start = ((), (), s32[]{:S(2)}) async-start(), calls=%async_computation.7 | async-start | bytes 8519680 | tf_op jit(solution)/shard_map/all_gather | solution.py:199
  107.5 19.1 %all-to-all-start.2 = ((bf16[4,128,1024]{2,1,0:T(8,128)(2,1)}), bf16[4,128,1024]{2,1,0:T(8,128)(2,1)}, u32[]{:S(2)}, u32[]{:S(2)}) async-start(bf16[4,128,1024]{2,1,0:T(8,128)(2,1)} %broadcast_in_dim.46), calls=%async_computation.2 | async-start | bytes 2097152 | tf_op jit(solution)/shard_map/all_to_all | solution.py:18
  111.8 1.8 copy-start.12
  111.8 1.8 copy-start.13
  129.7 5.0 %copy-start.3 = (bf16[24,2048]{1,0:T(8,128)(2,1)S(1)}, bf16[24,2048]{1,0:T(8,128)(2,1)}, u32[]{:S(2)}) copy-start(bf16[24,2048]{1,0:T(8,128)(2,1)} %param.21) | copy-start | bytes 294916
  129.7 5.0 %copy-start.7 = (f32[2048]{0:T(1024)S(1)}, f32[2048]{0:T(1024)}, u32[]{:S(2)}) copy-start(f32[2048]{0:T(1024)} %param.22) | copy-start | bytes 24580
  129.7 8.7 %copy-start.14 = (bf16[2048,4]{0,1:T(4,128)(2,1)S(1)}, bf16[2048,4]{0,1:T(4,128)(2,1)}, u32[]{:S(2)}) copy-start(bf16[2048,4]{0,1:T(4,128)(2,1)} %param.32) | copy-start | bytes 49156
  129.7 41.3 %all-to-all-start.4 = ((bf16[4,1536,256]{2,1,0:T(8,128)(2,1)}), bf16[4,1536,256]{2,1,0:T(8,128)(2,1)}, u32[]{:S(2)}, u32[]{:S(2)}) async-start(bf16[4,1536,256]{2,1,0:T(8,128)(2,1)} %broadcast_in_dim.48), calls=%async_computation.4 | async-start | bytes 6291456 | tf_op jit(solution)/shard_map/all_to_all | solution.py:18
  134.7 6.7 %copy-start.11 = (bf16[1,512,512]{2,1,0:T(8,128)(2,1)S(1)}, bf16[1,512,512]{2,1,0:T(8,128)(2,1)}, u32[]{:S(2)}) copy-start(bf16[1,512,512]{2,1,0:T(8,128)(2,1)} %param.37) | copy-start | bytes 1572868
  171.0 17.4 %all-to-all-start.3 = ((bf16[64,2,512]{2,1,0:T(2,128)(2,1)}), bf16[64,2,512]{2,1,0:T(2,128)(2,1)S(1)}, u32[]{:S(2)}, u32[]{:S(2)}) async-start(bf16[64,2,512]{2,1,0:T(2,128)(2,1)} %reshape.214), calls=%async_computation.3 | async-start | bytes 262144 | tf_op jit(solution)/shard_map/all_to_all | solution.py:179
  188.4 0.6 copy-start.4
  189.0 19.8 %all-to-all-start.5 = ((bf16[64,24,128]{2,1,0:T(8,128)(2,1)}), bf16[64,24,128]{2,1,0:T(8,128)(2,1)S(1)}, u32[]{:S(2)}, u32[]{:S(2)}) async-start(bf16[64,24,128]{2,1,0:T(8,128)(2,1)} %bitcast.84), calls=%async_computation.5 | async-start | bytes 786432 | tf_op jit(solution)/shard_map/all_to_all | solution.py:196
Sparse Core Ops, SparseCore 0:
  74.7 22.5 all-gather.3
  100.0 85.2 all-gather.5
where the time goes:
time: 222 us; the launch traced here: 221 us
  waiting for transfers between devices  65.6 us (30%)
  blocking collectives  65.4 us (29%)
  matrix products  27.1 us (12%)
  starting transfers between devices  24.6 us (11%)
  local copies, waits for them, and re-layouts  14.4 us (6%)
  between operations  14.4 us (6%)
  other arithmetic  9.43 us (4%)
    all_to_all x3, waiting for transfers between devices, copy_for_each(): lax.all_to_all(jnp.broadcast_to(x[None], (devices, *x.shape)), axis, 0, 0...  46.5 us
    all_gather x2, blocking collectives, all_blocks(): tiles = lax.all_gather(tiles, axes[k], axis=0, tiled=True)  36.5 us
    all_to_all x1, blocking collectives, shards(): lax.all_to_all(outbound, EP, split_axis=0, concat_axis=0, tiled=True)  28.8 us
    all_to_all x3, starting transfers between devices, copy_for_each(): lax.all_to_all(jnp.broadcast_to(x[None], (devices, *x.shape)), axis, 0, 0...  14 us
    all_to_all x1, waiting for transfers between devices, shards(): lax.all_to_all(dense_hidden, EP, split_axis=0, concat_axis=1, tiled=True)  10.8 us
    all_to_all x1, waiting for transfers between devices, shards(): lax.all_to_all(result.reshape(received.shape), EP, split_axis=0, concat_a...  7.59 us
    all_to_all x1, starting transfers between devices, shards(): lax.all_to_all(result.reshape(received.shape), EP, split_axis=0, concat_a...  6.15 us
    dot_general x1, matrix products, shards(): jnp.dot(own_hidden, lax.all_gather(d_down, EP, axis=0, tiled=True), prefe...  5.27 us
  transfers between devices with their start and end apart: 7, of which 5 were waited for; matrix products, arithmetic and copies ran while one was open for 12% of the time, Pallas kernels for 0%

commit v1 on v0

--- a/solution.py
+++ b/solution.py
@@ -1,46 +1,26 @@
+import functools
+
 import jax
 import jax.numpy as jnp
 from jax import lax
+from jax.experimental import pallas as pl
+from jax.experimental.pallas import tpu as pltpu
 from jax.sharding import Mesh
 from jax.sharding import PartitionSpec as P
 
 GROUPS = 4
 TOP_K = 2
 EP = ("ep_0", "ep_1", "ep_2")
-
+Z, Y, CORE, TP = "ep_0", "ep_1", "ep_2", "tp"
 
 norm_eps = 1e-06
 segment_len = 128
-
-
-def copy_for_each(x, axis):
-    devices = lax.axis_size(axis)
-    return lax.all_to_all(jnp.broadcast_to(x[None], (devices, *x.shape)), axis, 0, 0, tiled=True)
-
-
-def over_copies(x, axis):
-    everything = copy_for_each(x, axis)
-    return jnp.sum(everything.astype(jnp.float32), axis=0)
-
-
-def in_order(tiles, dim):
-    lengths = list(tiles.shape[1:])
-    lengths[dim] *= tiles.shape[0]
-    return jnp.moveaxis(tiles, 0, dim).reshape(lengths)
-
-
-def all_blocks(x, axes, sequence):
-    tiles = x[None]
-    for k in sequence:
-        tiles = lax.all_gather(tiles, axes[k], axis=0, tiled=True)
-    current = [lax.axis_size(axes[k]) for k in reversed(sequence)]
-    tiles = tiles.reshape(*current, *x.shape)
-    turned = sorted(range(len(sequence)), key=lambda place: sequence[len(sequence) - 1 - place])
-    return tiles.transpose(*turned, *range(len(sequence), tiles.ndim)).reshape(-1, *x.shape)
-
-
-def whole_of(x, axes, sequence, dim):
-    return in_order(all_blocks(x, axes, sequence), dim)
+NT = (((1,), (1,)), ((), ()))
+
+
+def shifted(x, axis, step):
+    size = lax.axis_size(axis)
+    return lax.ppermute(x, axis, [(i, (i + step) % size) for i in range(size)])
 
 
 def normed(values, gains):
@@ -98,6 +78,123 @@
     position = lax.iota(jnp.int32, count)
     earlier = position[None, :] < position[:, None]
     return jnp.sum(same_expert & earlier, axis=1)
+
+
+def silu(v):
+    return v / (1.0 + jnp.exp(-v))
+
+
+def dense_kernel(here_ref, there_ref, *refs):
+    blocks, out_ref = refs[:-1], refs[-1]
+    units = blocks[0].shape[0] // 3
+    cut = [
+        jnp.concatenate([b[part * units : (part + 1) * units, :] for b in blocks], axis=0)
+        for part in range(3)
+    ]
+    rows = jnp.concatenate([here_ref[...], there_ref[...]], axis=0)
+    gate = lax.dot_general(rows, cut[0], NT, preferred_element_type=jnp.float32)
+    up = lax.dot_general(rows, cut[1], NT, preferred_element_type=jnp.float32)
+    hidden = (silu(gate) * up).astype(jnp.bfloat16)
+    seq, width = out_ref.shape[1], out_ref.shape[2]
+    y, c = lax.axis_index(Y), lax.axis_index(CORE)
+    ys, tps = lax.axis_size(Y), lax.axis_size(TP)
+    for t in range(tps):
+        part = jnp.dot(
+            hidden, cut[2][:, t * width : (t + 1) * width], preferred_element_type=jnp.float32
+        )
+        for other in range(2):
+            core = c if other == 0 else 1 - c
+            for k in range(ys):
+                owner = (lax.rem(y - k + ys, ys) * 2 + core) * tps + t
+                at = (other * ys + k) * seq
+                out_ref[owner] = part[at : at + seq].astype(jnp.bfloat16)
+
+
+def dense_parts(here, there, blocks, seq, width):
+    members = lax.axis_size(Y) * lax.axis_size(CORE) * lax.axis_size(TP)
+    return pl.pallas_call(
+        dense_kernel,
+        out_shape=jax.ShapeDtypeStruct((members, seq, width), jnp.bfloat16),
+        cost_estimate=pl.CostEstimate(
+            flops=1_300_000_000, bytes_accessed=5_000_000, transcendentals=50_000
+        ),
+        name="dense_parts",
+    )(here, there, *blocks)
+
+
+def expert_in_kernel(rows_ref, gate_ref, up_ref, out_ref):
+    t, tps = lax.axis_index(TP), lax.axis_size(TP)
+    width = out_ref.shape[2] // 2
+    rows = rows_ref[...]
+    for u in range(tps):
+        at = slice(u * width, (u + 1) * width)
+        both = jnp.concatenate([gate_ref[:, at], up_ref[:, at]], axis=1)
+        pre = jnp.dot(rows, both, preferred_element_type=jnp.float32)
+        out_ref[lax.rem(u - t + tps, tps)] = pre.astype(jnp.bfloat16)
+
+
+def expert_in(rows, gate, up):
+    tps = lax.axis_size(TP)
+    return pl.pallas_call(
+        expert_in_kernel,
+        out_shape=jax.ShapeDtypeStruct(
+            (tps, rows.shape[0], 2 * gate.shape[1] // tps), jnp.bfloat16
+        ),
+        cost_estimate=pl.CostEstimate(
+            flops=140_000_000, bytes_accessed=1_400_000, transcendentals=0
+        ),
+        name="expert_in",
+    )(rows, gate, up)
+
+
+def expert_out_kernel(*refs):
+    hiddens, down_ref, out_ref = refs[:-2], refs[-2], refs[-1]
+    t, tps = lax.axis_index(TP), lax.axis_size(TP)
+    units = hiddens[0].shape[1]
+    total = None
+    for k in range(tps):
+        at = pl.multiple_of(lax.rem(t - k + tps, tps) * units, units)
+        term = jnp.dot(
+            hiddens[k][...], down_ref[pl.ds(at, units), :], preferred_element_type=jnp.float32
+        )
+        total = term if total is None else total + term
+    out_ref[...] = total.astype(jnp.bfloat16)
+
+
+def expert_out(hiddens, down):
+    return pl.pallas_call(
+        expert_out_kernel,
+        out_shape=jax.ShapeDtypeStruct((hiddens[0].shape[0], down.shape[1]), jnp.bfloat16),
+        cost_estimate=pl.CostEstimate(
+            flops=70_000_000, bytes_accessed=800_000, transcendentals=0
+        ),
+        name="expert_out",
+    )(*hiddens, down)
+
+
+def dense_weights(d_gate, d_up, d_down):
+    tps = lax.axis_size(TP)
+    width, units = d_gate.shape
+    piece = units // tps
+    outgoing = jnp.concatenate(
+        [
+            d_gate.T.reshape(tps, piece, width),
+            d_up.T.reshape(tps, piece, width),
+            d_down.reshape(tps, piece, width),
+        ],
+        axis=1,
+    )
+    arrived = lax.all_to_all(outgoing, TP, split_axis=0, concat_axis=0, tiled=True)
+    own = arrived.transpose(1, 0, 2).reshape(3 * piece, tps * width)
+    blocks = [own]
+    right = left = own
+    for step in range(lax.axis_size(Z) // 2):
+        right = shifted(right, Z, 1)
+        blocks.append(right)
+        if len(blocks) < lax.axis_size(Z):
+            left = shifted(left, Z, -1)
+            blocks.append(left)
+    return blocks
 
 
 def shards(
@@ -125,13 +222,14 @@
 ):
     seq_count = tokens.shape[0]
     width_part = d_gate.shape[0]
-    dense_units = d_gate.shape[1]
-    expert_units = e_gate.shape[2]
     kv_local = key_cache.shape[1]
     head_dim = key_cache.shape[3]
     ep_size = lax.axis_size(EP)
+    tps = lax.axis_size(TP)
     per_group = ep_size // GROUPS
-    capacity = max(2, (seq_count + per_group - 1) // per_group)
+    capacity = 2
+    blocks = dense_weights(d_gate, d_up, d_down)
+
     h_first = normed(tokens, norm_attn).astype(jnp.bfloat16)
     queries = jnp.dot(h_first, w_query, preferred_element_type=jnp.float32).astype(jnp.bfloat16)
     new_keys = jnp.dot(h_first, w_key, preferred_element_type=jnp.float32).astype(jnp.bfloat16)
@@ -143,62 +241,58 @@
     partial_value = jnp.dot(heads_out, w_out, preferred_element_type=jnp.float32).astype(
         jnp.bfloat16
     )
-    attended = over_copies(
-        lax.optimization_barrier(partial_value).astype(jnp.float32).astype(jnp.bfloat16), "tp"
-    ).astype(jnp.float32)
+    partial_value = lax.optimization_barrier(partial_value)
+    attended = partial_value.astype(jnp.float32)
+    for k in range(1, tps):
+        attended = attended + shifted(partial_value, TP, k).astype(jnp.float32)
     resid = tokens.astype(jnp.float32) + attended
     h_second = normed(resid, norm_ffn).astype(jnp.bfloat16)
     column = lax.axis_index("tp") * width_part
     h_slice = lax.dynamic_slice_in_dim(h_second, column, width_part, 1)
     resid_slice = lax.dynamic_slice_in_dim(resid, column, width_part, 1)
-    dense_in = jnp.concatenate([d_gate, d_up], axis=1)
-    expert_in = jnp.concatenate([e_gate[0], e_up[0]], axis=1)
+
+    flat_routes = routes.T.reshape(-1)
+    slot_ids = flat_routes * capacity + slot_ranks(flat_routes)
+    onehot = (lax.iota(jnp.int32, ep_size * capacity)[:, None] == slot_ids[None, :]).astype(
+        jnp.bfloat16
+    )
+    repeated = jnp.concatenate([h_slice] * TOP_K, axis=0)
+    outbound = jnp.dot(onehot, repeated, preferred_element_type=jnp.float32)
+    outbound = outbound.astype(jnp.bfloat16).reshape(ep_size, capacity, width_part)
+    received = lax.all_to_all(outbound, EP, split_axis=0, concat_axis=0, tiled=True)
+
+    here = jnp.concatenate(
+        [h_second] + [shifted(h_second, Y, k) for k in range(1, lax.axis_size(Y))], axis=0
+    )
+    there = shifted(here, CORE, 1)
+    parts = dense_parts(here, there, blocks, seq_count, width_part)
+    dense_all = lax.all_to_all(parts, (Y, CORE, TP), split_axis=0, concat_axis=0, tiled=True)
+    dense_slice = jnp.sum(dense_all.astype(jnp.float32), axis=0)
+
+    flat_rows = received.reshape(-1, width_part)
+    pre = expert_in(flat_rows, e_gate[0], e_up[0])
+    act = pre[0].astype(jnp.float32)
+    for k in range(1, tps):
+        act = act + shifted(pre[k], TP, k).astype(jnp.float32)
+    units = act.shape[1] // 2
+    hidden = (silu(act[:, :units]) * act[:, units:]).astype(jnp.bfloat16)
+    hidden = lax.optimization_barrier(hidden)
+    hiddens = [hidden] + [shifted(hidden, TP, k) for k in range(1, tps)]
+    result = expert_out(hiddens, e_down[0])
+    returned = lax.all_to_all(
+        result.reshape(received.shape), EP, split_axis=0, concat_axis=0, tiled=True
+    )
+
     group_logits = jnp.dot(h_second, w_group, preferred_element_type=jnp.float32)
     fine_logits = jnp.dot(h_second, w_fine, preferred_element_type=jnp.float32)
     shares = route_weights(group_logits, fine_logits, routes, per_group)
     mix_gate = jax.nn.sigmoid(
         jnp.dot(h_second.astype(jnp.float32), w_mix, precision=lax.Precision.HIGHEST)
     )
-    flat_routes = routes.reshape(-1)
-    slot_ids = flat_routes * capacity + slot_ranks(flat_routes)
-    onehot = (lax.iota(jnp.int32, ep_size * capacity)[:, None] == slot_ids[None, :]).astype(
-        jnp.float32
-    )
-    repeated = jnp.repeat(h_slice, TOP_K, axis=0)
-    outbound = jnp.dot(onehot.astype(jnp.bfloat16), repeated, preferred_element_type=jnp.float32)
-    outbound = outbound.astype(jnp.bfloat16).reshape(ep_size, capacity, width_part)
-    received = lax.all_to_all(outbound, EP, split_axis=0, concat_axis=0, tiled=True)
-    flat_rows = received.reshape(-1, width_part)
-    pre_act = over_copies(
-        jnp.dot(flat_rows, expert_in, preferred_element_type=jnp.float32).astype(jnp.bfloat16), "tp"
-    ).astype(jnp.float32)
-    hidden = (jax.nn.silu(pre_act[:, :expert_units]) * pre_act[:, expert_units:]).astype(
-        jnp.bfloat16
-    )
-    result = jnp.dot(hidden, e_down[0], preferred_element_type=jnp.float32).astype(jnp.bfloat16)
-    returned = lax.all_to_all(
-        result.reshape(received.shape), EP, split_axis=0, concat_axis=0, tiled=True
-    )
-    weighted = onehot * shares.reshape(-1)[None, :]
-    moe_rows = jnp.dot(
-        weighted.T,
-        returned.reshape(-1, width_part).astype(jnp.float32),
-        precision=lax.Precision.HIGHEST,
-    )
-    moe_slice = jnp.sum(moe_rows.reshape(seq_count, TOP_K, width_part), axis=1)
-    dense_pre = jnp.dot(
-        whole_of(h_slice, EP, (1, 0, 2), 0), dense_in, preferred_element_type=jnp.float32
-    )
-    dense_pre = over_copies(dense_pre.astype(jnp.bfloat16), "tp").astype(jnp.float32)
-    dense_hidden = (jax.nn.silu(dense_pre[:, :dense_units]) * dense_pre[:, dense_units:]).astype(
-        jnp.bfloat16
-    )
-    own_hidden = lax.all_to_all(dense_hidden, EP, split_axis=0, concat_axis=1, tiled=True)
-    dense_slice = jnp.dot(
-        own_hidden,
-        lax.all_gather(d_down, EP, axis=0, tiled=True),
-        preferred_element_type=jnp.float32,
-    )
+    back = jnp.dot(
+        onehot.T, returned.reshape(-1, width_part), preferred_element_type=jnp.float32
+    ).reshape(TOP_K, seq_count, width_part)
+    moe_slice = jnp.sum(back * shares.T[:, :, None], axis=0)
     mixed = resid_slice + moe_slice + mix_gate[:, None] * dense_slice
     return (
         mixed.astype(jnp.bfloat16),

time: 222 us -> 143 us (0.64)
  blocking collectives: 65.4 us -> 0 us
  starting transfers between devices: 24.6 us -> 60.1 us
  waiting for transfers between devices: 65.6 us -> 30.1 us
  between operations: 14.4 us -> 1.07 us
  matrix products: 27.1 us -> 17.6 us
  Pallas kernels: 0 us -> 8.41 us
  other arithmetic: 9.43 us -> 13 us
  local copies, waits for them, and re-layouts: 14.4 us -> 11.6 us
    all_to_all x4 -> x3, waiting for transfers between devices: 57.3 us -> 14.9 us  [the longest x1 13.3 us: shards(): lax.all_to_all(parts, (Y, CORE, TP), split_axis=0, concat_axis=0, tiled=T...]
    all_gather x2 -> x0, blocking collectives: 36.5 us -> none  [all_blocks(): tiles = lax.all_gather(tiles, axes[k], axis=0, tiled=True)]
    all_to_all x1 -> x0, blocking collectives: 28.8 us -> none  [shards(): lax.all_to_all(outbound, EP, split_axis=0, concat_axis=0, tiled=True)]
    ppermute x0 -> x20, starting transfers between devices: none -> 28.6 us  [shifted(): return lax.ppermute(x, axis, [(i, (i + step) % size) for i in range(size)])]
    dot_general x6 -> x2, matrix products: 10.4 us -> 1.11 us  [the longest x1 0.97 us: shards(): outbound = jnp.dot(onehot, repeated, preferred_element_type=jnp.float32)]
    pallas_call x0 -> x3, Pallas kernels: none -> 8.41 us  [the longest x1 4.11 us: dense_parts(): pl.pallas_call(dense_kernel, out_shape=jax.ShapeDtypeStruct((members, seq...]
    ppermute x0 -> x20, waiting for transfers between devices: none -> 8.25 us  [shifted(): return lax.ppermute(x, axis, [(i, (i + step) % size) for i in range(size)])]
    broadcast_in_dim x4 -> x0, local copies, waits for them, and re-layouts: 5.04 us -> none  [the longest x3 5.01 us: copy_for_each(): jnp.broadcast_to(x[None], (devices, *x.shape))]
  transfers between devices with their start and end apart: 7 -> 24, of which waited for: 5 -> 7; matrix products, arithmetic and copies ran while one was open for 12% -> 13% of each run, Pallas kernels for 0% -> 6%
where the time goes in v1:
time: 143 us; the launch traced here: 142 us
  starting transfers between devices  60.1 us (42%)
  waiting for transfers between devices  30.1 us (21%)
  matrix products  17.6 us (12%)
  other arithmetic  13 us (9%)
  local copies, waits for them, and re-layouts  11.6 us (8%)
  Pallas kernels  8.41 us (6%)
    ppermute x20, starting transfers between devices, shifted(): return lax.ppermute(x, axis, [(i, (i + step) % size) for i in range(size)])  28.6 us
    all_to_all x1, starting transfers between devices, shards(): lax.all_to_all(outbound, EP, split_axis=0, concat_axis=0, tiled=True)  13.4 us
    all_to_all x1, waiting for transfers between devices, shards(): lax.all_to_all(parts, (Y, CORE, TP), split_axis=0, concat_axis=0, tiled=T...  13.3 us
    all_to_all x1, starting transfers between devices, shards(): lax.all_to_all(result.reshape(received.shape), EP, split_axis=0, concat_a...  9.13 us
    ppermute x20, waiting for transfers between devices, shifted(): return lax.ppermute(x, axis, [(i, (i + step) % size) for i in range(size)])  8.25 us
    all_to_all x1, waiting for transfers between devices, shards(): lax.all_to_all(result.reshape(received.shape), EP, split_axis=0, concat_a...  6.89 us
    all_to_all x1, starting transfers between devices, shards(): lax.all_to_all(parts, (Y, CORE, TP), split_axis=0, concat_axis=0, tiled=T...  5.51 us
    pallas_call x1, Pallas kernels, dense_parts(): pl.pallas_call(dense_kernel, out_shape=jax.ShapeDtypeStruct((members, seq...  4.11 us
  transfers between devices with their start and end apart: 24, of which 7 were waited for; matrix products, arithmetic and copies ran while one was open for 13% of the time, Pallas kernels for 6%

profile of v1, /device:TPU:1, one launch (start us, length us, event | category | flops | bytes accessed | tf_op | source)
XLA Modules:
  0.0 141.8 jit_solution(7358523961652823473)
XLA Ops:
  2.4 2.1 %convolution_convert_fusion.2 = bf16[24,512]{1,0:T(8,128)(2,1)S(1)} fusion(bf16[2048,512]{1,0:T(8,128)(2,1)} %param.23, bf16[24,2048]{1,0:T(8,128)(2,1)} %param.21, f32[2048]{0:T(1024)} %param.22, f32[24]{0:T(128)S(1)} %add_rsqrt_fusion.1), kind=kOutput, calls=%fused_computation.15 | convolution fusion | flops 50540544 | bytes 2228320 | tf_op jit(solution)/shard_map/dot_general | solution.py:234
  6.1 1.4 %fusion.54 = (f32[24,8,8]{1,2,0:T(8,128)S(1)}, f32[24,8,8,128]{3,1,2,0:T(8,128)}) fusion(f32[24,8,1024]{2,1,0:T(8,128)S(1)} %fusion.7, pred[24,1024]{1,0:T(8,128)(4,1)S(1)} %iota_compare_fusion), kind=kLoop, calls=%fused_computation.90 | loop fusion | flops 1767936 | bytes 1603584 | tf_op jit(solution)/shard_map/reduce_sum | solution.py:41
  7.9 2.6 %convolution_add_fusion = f32[24,8,8,128]{3,2,1,0:T(8,128)} fusion(f32[24,8,8,128]{3,1,2,0:T(8,128)} %get-tuple-element.6, f32[24,8,8]{2,1,0:T(8,128)S(1)} %copy.45), kind=kOutput, calls=%fused_computation.8 | convolution fusion | flops 302202880 | bytes 1579008 | tf_op jit(solution)/shard_map/...ij,jk->...ik/dot_general | solution.py:37
  10.5 2.1 %reshape.198 = f32[24,8,1024]{2,1,0:T(8,128)} reshape(f32[24,8,8,128]{3,2,1,0:T(8,128)} %convolution_add_fusion) | data formatting | bytes 1572864 | tf_op jit(solution)/shard_map/reshape | solution.py:43
  12.7 3.3 %fusion.10 = bf16[24,8,64]{2,1,0:T(8,128)(2,1)S(1)} fusion(bf16[24,1,1024,64]{2,3,1,0:T(8,128)(2,1)} %param.29, f32[24,8,1024]{2,1,0:T(8,128)} %reshape.198, f32[24,8,1024]{2,1,0:T(8,128)} %copy-done.1, pred[24,1024]{1,0:T(8,128)(4,1)S(1)} %iota_compare_fusion), kind=kOutput, calls=%fused_computation.13 | convolution fusion | flops 27340800 | bytes 4767744 | tf_op jit(solution)/shard_map/bkgs,bksd->bkgd/dot_general | solution.py:53
  16.1 2.6 %convolution_convert_fusion = bf16[24,2048]{1,0:T(8,128)(2,1)} fusion(bf16[24,512]{1,0:T(8,128)(2,1)S(1)} %reshape.200, bf16[512,2048]{1,0:T(8,128)(2,1)} %param.26), kind=kOutput, calls=%fused_computation.6 | convolution fusion | flops 50380800 | bytes 2220032 | tf_op jit(solution)/shard_map/dot_general | solution.py:241
  18.8 3.3 %collective-permute-start.2 = (bf16[24,2048]{1,0:T(8,128)(2,1)}, bf16[24,2048]{1,0:T(8,128)(2,1)}, u32[]{:S(2)}, u32[]{:S(2)}) collective-permute-start(bf16[24,2048]{1,0:T(8,128)(2,1)} %convolution_convert_fusion), channel_id=1, source_target_pairs={{0,3},{1,0},{2,1},{3,2},{4,7},{5,4},{6,5},{7,6},{8,11},{9,8},{10,9... | collective-permute-start | bytes 294920 | tf_op jit(solution)/shard_map/ppermute | solution.py:23
  23.4 1.7 %pad_maximum_fusion.1 = bf16[4,96,512]{2,1,0:T(8,128)(2,1)} fusion(bf16[4,32,512]{2,1,0:T(8,128)(2,1)} %bitcast.91, bf16[4,32,512]{2,1,0:T(8,128)(2,1)S(1)} %bitcast.87, bf16[4,32,512]{2,1,0:T(8,128)(2,1)S(1)} %bitcast.88), kind=kLoop, calls=%fused_computation.35 | loop fusion | flops 1179648 | bytes 786432 | tf_op jit(solution)/shard_map/concatenate | solution.py:179
  25.1 3.5 %all-to-all-start.2 = ((bf16[4,96,512]{2,1,0:T(8,128)(2,1)}), bf16[4,96,512]{2,1,0:T(8,128)(2,1)S(1)}, u32[]{:S(2)}, u32[]{:S(2)}) async-start(bf16[4,96,512]{2,1,0:T(8,128)(2,1)} %pad_maximum_fusion.1), calls=%async_computation.2 | async-start | bytes 786432 | tf_op jit(solution)/shard_map/all_to_all | solution.py:187
  30.0 1.9 %fusion.14 = bf16[24,1,64]{2,0,1:T(8,128)(2,1)} fusion(bf16[2048,64]{0,1:T(8,128)(2,1)} %param.24, bf16[24,2048]{1,0:T(8,128)(2,1)} %param.21, f32[2048]{0:T(1024)S(1)} %copy-done.11, f32[24]{0:T(128)} %copy-done.16), kind=kOutput, calls=%fused_computation.18 | convolution fusion | flops 6489600 | bytes 371808 | tf_op jit(solution)/shard_map/dot_general | solution.py:235
  36.1 1.6 %collective-permute-start.13 = (bf16[96,2048]{1,0:T(8,128)(2,1)}, bf16[96,2048]{1,0:T(8,128)(2,1)}, u32[]{:S(2)}, u32[]{:S(2)}) collective-permute-start(bf16[96,2048]{1,0:T(8,128)(2,1)} %bitcast.32.refs_0_), channel_id=1, source_target_pairs={{0,32},{32,64},{64,96},{96,128},{128,160},{160,192},{192,224},{224... | collective-permute-start | bytes 1179656 | tf_op jit(solution)/shard_map/ppermute | solution.py:23
  39.4 13.4 %all-to-all-start = ((bf16[64,2,512]{2,1,0:T(2,128)(2,1)}), bf16[64,2,512]{2,1,0:T(2,128)(2,1)S(1)}, u32[]{:S(2)}, u32[]{:S(2)}) async-start(bf16[64,2,512]{2,1,0:T(2,128)(2,1)} %reshape.202), calls=%async_computation | async-start | bytes 262144 | tf_op jit(solution)/shard_map/all_to_all | solution.py:262
  52.8 1.9 %fusion.15 = bf16[24,1,64]{2,0,1:T(8,128)(2,1)} fusion(bf16[2048,64]{0,1:T(8,128)(2,1)} %param.25, bf16[24,2048]{1,0:T(8,128)(2,1)} %param.21, f32[2048]{0:T(1024)S(1)} %copy-done.11, f32[24]{0:T(128)} %copy-done.16), kind=kOutput, calls=%fused_computation.19 | convolution fusion | flops 6489600 | bytes 371808 | tf_op jit(solution)/shard_map/dot_general | solution.py:236
  54.7 2.6 %collective-permute-start.11 = (bf16[24,2048]{1,0:T(8,128)(2,1)}, bf16[24,2048]{1,0:T(8,128)(2,1)S(1)}, u32[]{:S(2)}, u32[]{:S(2)}) collective-permute-start(bf16[24,2048]{1,0:T(8,128)(2,1)} %copy-done.2), channel_id=1, source_target_pairs={{0,24},{8,0},{16,8},{24,16},{1,25},{9,1},{17,9},{25,17},{2,26},{10... | collective-permute-start | bytes 294920 | tf_op jit(solution)/shard_map/ppermute | solution.py:23
  59.6 2.7 %collective-permute-start.14 = (bf16[96,2048]{1,0:T(8,128)(2,1)}, bf16[96,2048]{1,0:T(8,128)(2,1)}, u32[]{:S(2)}, u32[]{:S(2)}) collective-permute-start(bf16[96,2048]{1,0:T(8,128)(2,1)} %bitcast.32.refs_0_), channel_id=1, source_target_pairs={{0,224},{32,0},{64,32},{96,64},{128,96},{160,128},{192,160},{224,1... | collective-permute-start | bytes 1179656 | tf_op jit(solution)/shard_map/ppermute | solution.py:23
  62.3 1.6 %all-to-all-done = bf16[64,2,512]{2,1,0:T(2,128)(2,1)S(1)} async-done(((bf16[64,2,512]{2,1,0:T(2,128)(2,1)}), bf16[64,2,512]{2,1,0:T(2,128)(2,1)S(1)}, u32[]{:S(2)}, u32[]{:S(2)}) %all-to-all-start) | async-done | bytes 131104 | tf_op jit(solution)/shard_map/all_to_all | solution.py:262
  64.6 2.3 %expert_in.1 = bf16[4,128,256]{2,1,0:T(8,128)(2,1)} custom-call(bf16[128,512]{1,0:T(8,128)(2,1)} %reshape.203.rows_ref, bf16[512,512]{1,0:T(8,128)(2,1)} %bitcast.89, bf16[512,512]{1,0:T(8,128)(2,1)} %bitcast.90), custom_call_target="tpu_custom_call" | custom-call | flops 140000000 | bytes 1400000 | tf_op jit(solution)/shard_map/expert_in/pallas_call | solution.py:138
  68.2 2.3 %collective-permute-start.5 = (bf16[128,256]{1,0:T(8,128)(2,1)S(1)}, bf16[128,256]{1,0:T(8,128)(2,1)S(1)}, u32[]{:S(2)}, u32[]{:S(2)}) collective-permute-start(bf16[128,256]{1,0:T(8,128)(2,1)S(1)} %get-tuple-element.8), channel_id=1, source_target_pairs={{0,3},{1,0},{2,1},{3,2},{4,7},{5,4},{6,5},{7,6},{8,11},{9,8},{10,9... | collective-permute-start | bytes 196616 | tf_op jit(solution)/shard_map/ppermute | solution.py:23
  71.7 1.7 %pad_maximum_fusion.here_ref = bf16[96,2048]{1,0:T(8,128)(2,1)} fusion(bf16[24,2048]{1,0:T(8,128)(2,1)S(1)} %collective-permute-done.11, bf16[24,2048]{1,0:T(8,128)(2,1)} %collective-permute-done.10, bf16[24,2048]{1,0:T(8,128)(2,1)} %collective-permute-done.9, bf16[24,2048]{1,0:T(8,128)(2,1)S(1)} %copy-done.3), kind=kLoop, calls=%fused_computation.34 | loop fusion | flops 1572864 | bytes 786432 | tf_op jit(solution)/shard_map/concatenate | solution.py:264
  73.4 1.6 %collective-permute-start.12 = (bf16[96,2048]{1,0:T(8,128)(2,1)}, bf16[96,2048]{1,0:T(8,128)(2,1)}, u32[]{:S(2)}, u32[]{:S(2)}) collective-permute-start(bf16[96,2048]{1,0:T(8,128)(2,1)} %pad_maximum_fusion.here_ref), channel_id=1, source_target_pairs={{0,4},{4,0},{1,5},{5,1},{2,6},{6,2},{3,7},{7,3},{8,12},{12,8},{9,1... | collective-permute-start | bytes 1179656 | tf_op jit(solution)/shard_map/ppermute | solution.py:23
  75.0 2.2 %collective-permute-start.16 = (bf16[96,2048]{1,0:T(8,128)(2,1)}, bf16[96,2048]{1,0:T(8,128)(2,1)}, u32[]{:S(2)}, u32[]{:S(2)}) collective-permute-start(bf16[96,2048]{1,0:T(8,128)(2,1)} %collective-permute-done.14.refs_2_), channel_id=1, source_target_pairs={{0,224},{32,0},{64,32},{96,64},{128,96},{160,128},{192,160},{224,1... | collective-permute-start | bytes 1179656 | tf_op jit(solution)/shard_map/ppermute | solution.py:23
  80.7 5.2 %collective-permute-done.16.refs_4_ = bf16[96,2048]{1,0:T(8,128)(2,1)} collective-permute-done((bf16[96,2048]{1,0:T(8,128)(2,1)}, bf16[96,2048]{1,0:T(8,128)(2,1)}, u32[]{:S(2)}, u32[]{:S(2)}) %collective-permute-start.16) | collective-permute-done | bytes 393248 | tf_op jit(solution)/shard_map/ppermute | solution.py:23
  85.9 3.4 %collective-permute-start.18 = (bf16[96,2048]{1,0:T(8,128)(2,1)}, bf16[96,2048]{1,0:T(8,128)(2,1)}, u32[]{:S(2)}, u32[]{:S(2)}) collective-permute-start(bf16[96,2048]{1,0:T(8,128)(2,1)} %collective-permute-done.16.refs_4_), channel_id=1, source_target_pairs={{0,224},{32,0},{64,32},{96,64},{128,96},{160,128},{192,160},{224,1... | collective-permute-start | bytes 1179656 | tf_op jit(solution)/shard_map/ppermute | solution.py:23
  89.5 2.5 %collective-permute-start.7 = (bf16[128,128]{1,0:T(8,128)(2,1)S(1)}, bf16[128,128]{1,0:T(8,128)(2,1)S(1)}, u32[]{:S(2)}, u32[]{:S(2)}) collective-permute-start(bf16[128,128]{1,0:T(8,128)(2,1)S(1)} %fusion.37.refs_0_), channel_id=1, source_target_pairs={{0,2},{1,3},{2,0},{3,1},{4,6},{5,7},{6,4},{7,5},{8,10},{9,11},{10,... | collective-permute-start | bytes 98312 | tf_op jit(solution)/shard_map/ppermute | solution.py:23
  95.8 2.0 %expert_out.1 = bf16[128,512]{1,0:T(8,128)(2,1)} custom-call(bf16[128,128]{1,0:T(8,128)(2,1)} %copy-done.5, bf16[128,128]{1,0:T(8,128)(2,1)} %copy-done.8, bf16[128,128]{1,0:T(8,128)(2,1)} %copy-done.9, bf16[128,128]{1,0:T(8,128)(2,1)} %copy-done.10, bf16[512,512]{1,0:T(8,128)(2,1)} %bitcast.86), custom_call_target="tpu_custom_call" | custom-call | flops 70000000 | bytes 800000 | tf_op jit(solution)/shard_map/expert_out/pallas_call | solution.py:165
  97.9 1.6 %reshape.204 = bf16[64,2,512]{2,1,0:T(2,128)(2,1)} reshape(bf16[128,512]{1,0:T(8,128)(2,1)} %expert_out.1) | data formatting | bytes 262144 | tf_op jit(solution)/shard_map/reshape | solution.py:283
  99.5 9.1 %all-to-all-start.1 = ((bf16[64,2,512]{2,1,0:T(2,128)(2,1)}), bf16[64,2,512]{2,1,0:T(2,128)(2,1)S(1)}, u32[]{:S(2)}, u32[]{:S(2)}) async-start(bf16[64,2,512]{2,1,0:T(2,128)(2,1)} %reshape.204), calls=%async_computation.1 | async-start | bytes 262144 | tf_op jit(solution)/shard_map/all_to_all | solution.py:282
  108.7 4.1 %dense_parts.1 = bf16[32,24,512]{2,1,0:T(8,128)(2,1)} custom-call(bf16[96,2048]{1,0:T(8,128)(2,1)} %pad_maximum_fusion.here_ref, bf16[96,2048]{1,0:T(8,128)(2,1)} %collective-permute-done.12.there_ref, bf16[96,2048]{1,0:T(8,128)(2,1)} %bitcast.32.refs_0_, bf16[96,2048]{1,0:T(8,128)(2,1)} %collective-permute-done.13.refs_1_, ...), custom_call_target="tpu_custom_call" | custom-call | flops 1300000000 | bytes 5000000 | tf_op jit(solution)/shard_map/dense_parts/pallas_call | solution.py:115
  112.8 6.9 %all-to-all-done.1 = bf16[64,2,512]{2,1,0:T(2,128)(2,1)S(1)} async-done(((bf16[64,2,512]{2,1,0:T(2,128)(2,1)}), bf16[64,2,512]{2,1,0:T(2,128)(2,1)S(1)}, u32[]{:S(2)}, u32[]{:S(2)}) %all-to-all-start.1) | async-done | bytes 131104 | tf_op jit(solution)/shard_map/all_to_all | solution.py:282
  119.7 5.5 %all-to-all-start.3 = ((bf16[32,24,512]{2,1,0:T(8,128)(2,1)}), bf16[32,24,512]{2,1,0:T(8,128)(2,1)}, u32[]{:S(2)}, u32[]{:S(2)}) async-start(bf16[32,24,512]{2,1,0:T(8,128)(2,1)} %dense_parts.1), calls=%async_computation.3 | async-start | bytes 1572864 | tf_op jit(solution)/shard_map/all_to_all | solution.py:269
  125.7 13.3 %all-to-all-done.3 = bf16[32,24,512]{2,1,0:T(8,128)(2,1)} async-done(((bf16[32,24,512]{2,1,0:T(8,128)(2,1)}), bf16[32,24,512]{2,1,0:T(8,128)(2,1)}, u32[]{:S(2)}, u32[]{:S(2)}) %all-to-all-start.3) | async-done | bytes 786464 | tf_op jit(solution)/shard_map/all_to_all | solution.py:269
  140.3 1.5 %add_convert_fusion = bf16[24,512]{1,0:T(8,128)(2,1)} fusion(f32[24,512]{1,0:T(8,128)S(1)} %convert_reduce_fusion, f32[24,512]{1,0:T(8,128)S(1)} %fusion.13, f32[24,2048]{1,0:T(8,128)} %copy-done.4, s32[]{:T(128)S(6)} %select_n.41, f32[24]{0:T(128)S(1)} %fusion.19), kind=kLoop, calls=%fused_computation.62 | loop fusion | flops 49152 | bytes 172132 | tf_op jit(solution)/shard_map/convert_element_type | solution.py:298
  (113 shorter events, 27.1 us)
Async XLA Ops:
  16.1 13.9 %copy-start.11 = (f32[2048]{0:T(1024)S(1)}, f32[2048]{0:T(1024)}, u32[]{:S(2)}) copy-start(f32[2048]{0:T(1024)} %param.22) | copy-start | bytes 24580
  18.8 13.1 %collective-permute-start.2 = (bf16[24,2048]{1,0:T(8,128)(2,1)}, bf16[24,2048]{1,0:T(8,128)(2,1)}, u32[]{:S(2)}, u32[]{:S(2)}) collective-permute-start(bf16[24,2048]{1,0:T(8,128)(2,1)} %convolution_convert_fusion), channel_id=1, source_target_pairs={{0,3},{1,0},{2,1},{3,2},{4,7},{5,4},{6,5},{7,6},{8,11},{9,8},{10,9... | collective-permute-start | bytes 294920 | tf_op jit(solution)/shard_map/ppermute | solution.py:23
  22.1 9.8 %collective-permute-start.1 = (bf16[24,2048]{1,0:T(8,128)(2,1)}, bf16[24,2048]{1,0:T(8,128)(2,1)}, u32[]{:S(2)}, u32[]{:S(2)}) collective-permute-start(bf16[24,2048]{1,0:T(8,128)(2,1)} %convolution_convert_fusion), channel_id=1, source_target_pairs={{0,2},{1,3},{2,0},{3,1},{4,6},{5,7},{6,4},{7,5},{8,10},{9,11},{10,... | collective-permute-start | bytes 294920 | tf_op jit(solution)/shard_map/ppermute | solution.py:23
  22.6 9.3 %collective-permute-start = (bf16[24,2048]{1,0:T(8,128)(2,1)}, bf16[24,2048]{1,0:T(8,128)(2,1)}, u32[]{:S(2)}, u32[]{:S(2)}) collective-permute-start(bf16[24,2048]{1,0:T(8,128)(2,1)} %convolution_convert_fusion), channel_id=1, source_target_pairs={{0,1},{1,2},{2,3},{3,0},{4,5},{5,6},{6,7},{7,4},{8,9},{9,10},{10,1... | collective-permute-start | bytes 294920 | tf_op jit(solution)/shard_map/ppermute | solution.py:23
  25.1 10.1 %all-to-all-start.2 = ((bf16[4,96,512]{2,1,0:T(8,128)(2,1)}), bf16[4,96,512]{2,1,0:T(8,128)(2,1)S(1)}, u32[]{:S(2)}, u32[]{:S(2)}) async-start(bf16[4,96,512]{2,1,0:T(8,128)(2,1)} %pad_maximum_fusion.1), calls=%async_computation.2 | async-start | bytes 786432 | tf_op jit(solution)/shard_map/all_to_all | solution.py:187
  36.1 35.6 %copy-start.3 = (bf16[24,2048]{1,0:T(8,128)(2,1)S(1)}, bf16[24,2048]{1,0:T(8,128)(2,1)}, u32[]{:S(2)}) copy-start(bf16[24,2048]{1,0:T(8,128)(2,1)} %copy-done.2) | copy-start | bytes 294916
  36.1 30.8 %collective-permute-start.13 = (bf16[96,2048]{1,0:T(8,128)(2,1)}, bf16[96,2048]{1,0:T(8,128)(2,1)}, u32[]{:S(2)}, u32[]{:S(2)}) collective-permute-start(bf16[96,2048]{1,0:T(8,128)(2,1)} %bitcast.32.refs_0_), channel_id=1, source_target_pairs={{0,32},{32,64},{64,96},{96,128},{128,160},{160,192},{192,224},{224... | collective-permute-start | bytes 1179656 | tf_op jit(solution)/shard_map/ppermute | solution.py:23
  39.4 24.5 %all-to-all-start = ((bf16[64,2,512]{2,1,0:T(2,128)(2,1)}), bf16[64,2,512]{2,1,0:T(2,128)(2,1)S(1)}, u32[]{:S(2)}, u32[]{:S(2)}) async-start(bf16[64,2,512]{2,1,0:T(2,128)(2,1)} %reshape.202), calls=%async_computation | async-start | bytes 262144 | tf_op jit(solution)/shard_map/all_to_all | solution.py:262
  52.8 36.5 %copy-start.19 = (bf16[2048,4]{0,1:T(4,128)(2,1)S(1)}, bf16[2048,4]{0,1:T(4,128)(2,1)}, u32[]{:S(2)}) copy-start(bf16[2048,4]{0,1:T(4,128)(2,1)} %param.32) | copy-start | bytes 49156
  52.8 36.5 %copy-start.21 = (s32[24]{0:T(128)S(1)}, s32[24]{0:T(128)}, u32[]{:S(2)}) copy-start(s32[24]{0:T(128)} %fusion.48) | copy-start | bytes 292
  52.8 40.6 %copy-start.14 = (s32[24,2]{0,1:T(2,128)S(1)}, s32[24,2]{0,1:T(2,128)}, u32[]{:S(2)}) copy-start(s32[24,2]{0,1:T(2,128)} %param.34) | copy-start | bytes 580
  54.7 13.5 %collective-permute-start.11 = (bf16[24,2048]{1,0:T(8,128)(2,1)}, bf16[24,2048]{1,0:T(8,128)(2,1)S(1)}, u32[]{:S(2)}, u32[]{:S(2)}) collective-permute-start(bf16[24,2048]{1,0:T(8,128)(2,1)} %copy-done.2), channel_id=1, source_target_pairs={{0,24},{8,0},{16,8},{24,16},{1,25},{9,1},{17,9},{25,17},{2,26},{10... | collective-permute-start | bytes 294920 | tf_op jit(solution)/shard_map/ppermute | solution.py:23
  57.3 13.3 %collective-permute-start.10 = (bf16[24,2048]{1,0:T(8,128)(2,1)}, bf16[24,2048]{1,0:T(8,128)(2,1)}, u32[]{:S(2)}, u32[]{:S(2)}) collective-permute-start(bf16[24,2048]{1,0:T(8,128)(2,1)} %copy-done.2), channel_id=1, source_target_pairs={{0,16},{8,24},{16,0},{24,8},{1,17},{9,25},{17,1},{25,9},{2,18},{10... | collective-permute-start | bytes 294920 | tf_op jit(solution)/shard_map/ppermute | solution.py:23
  57.8 13.3 %collective-permute-start.9 = (bf16[24,2048]{1,0:T(8,128)(2,1)}, bf16[24,2048]{1,0:T(8,128)(2,1)}, u32[]{:S(2)}, u32[]{:S(2)}) collective-permute-start(bf16[24,2048]{1,0:T(8,128)(2,1)} %copy-done.2), channel_id=1, source_target_pairs={{0,8},{8,16},{16,24},{24,0},{1,9},{9,17},{17,25},{25,1},{2,10},{10... | collective-permute-start | bytes 294920 | tf_op jit(solution)/shard_map/ppermute | solution.py:23
  59.6 15.4 %collective-permute-start.14 = (bf16[96,2048]{1,0:T(8,128)(2,1)}, bf16[96,2048]{1,0:T(8,128)(2,1)}, u32[]{:S(2)}, u32[]{:S(2)}) collective-permute-start(bf16[96,2048]{1,0:T(8,128)(2,1)} %bitcast.32.refs_0_), channel_id=1, source_target_pairs={{0,224},{32,0},{64,32},{96,64},{128,96},{160,128},{192,160},{224,1... | collective-permute-start | bytes 1179656 | tf_op jit(solution)/shard_map/ppermute | solution.py:23
  66.9 11.7 %collective-permute-start.15 = (bf16[96,2048]{1,0:T(8,128)(2,1)}, bf16[96,2048]{1,0:T(8,128)(2,1)S(1)}, u32[]{:S(2)}, u32[]{:S(2)}) collective-permute-start(bf16[96,2048]{1,0:T(8,128)(2,1)} %collective-permute-done.13.refs_1_), channel_id=1, source_target_pairs={{0,32},{32,64},{64,96},{96,128},{128,160},{160,192},{192,224},{224... | collective-permute-start | bytes 1179656 | tf_op jit(solution)/shard_map/ppermute | solution.py:23
  68.2 5.2 %collective-permute-start.5 = (bf16[128,256]{1,0:T(8,128)(2,1)S(1)}, bf16[128,256]{1,0:T(8,128)(2,1)S(1)}, u32[]{:S(2)}, u32[]{:S(2)}) collective-permute-start(bf16[128,256]{1,0:T(8,128)(2,1)S(1)} %get-tuple-element.8), channel_id=1, source_target_pairs={{0,3},{1,0},{2,1},{3,2},{4,7},{5,4},{6,5},{7,6},{8,11},{9,8},{10,9... | collective-permute-start | bytes 196616 | tf_op jit(solution)/shard_map/ppermute | solution.py:23
  70.5 8.1 %collective-permute-start.4 = (bf16[128,256]{1,0:T(8,128)(2,1)S(1)}, bf16[128,256]{1,0:T(8,128)(2,1)S(1)}, u32[]{:S(2)}, u32[]{:S(2)}) collective-permute-start(bf16[128,256]{1,0:T(8,128)(2,1)S(1)} %get-tuple-element.9), channel_id=1, source_target_pairs={{0,2},{1,3},{2,0},{3,1},{4,6},{5,7},{6,4},{7,5},{8,10},{9,11},{10,... | collective-permute-start | bytes 196616 | tf_op jit(solution)/shard_map/ppermute | solution.py:23
  71.1 7.5 %collective-permute-start.3 = (bf16[128,256]{1,0:T(8,128)(2,1)S(1)}, bf16[128,256]{1,0:T(8,128)(2,1)S(1)}, u32[]{:S(2)}, u32[]{:S(2)}) collective-permute-start(bf16[128,256]{1,0:T(8,128)(2,1)S(1)} %get-tuple-element.7), channel_id=1, source_target_pairs={{0,1},{1,2},{2,3},{3,0},{4,5},{5,6},{6,7},{7,4},{8,9},{9,10},{10,1... | collective-permute-start | bytes 196616 | tf_op jit(solution)/shard_map/ppermute | solution.py:23
  73.4 35.3 %collective-permute-start.12 = (bf16[96,2048]{1,0:T(8,128)(2,1)}, bf16[96,2048]{1,0:T(8,128)(2,1)}, u32[]{:S(2)}, u32[]{:S(2)}) collective-permute-start(bf16[96,2048]{1,0:T(8,128)(2,1)} %pad_maximum_fusion.here_ref), channel_id=1, source_target_pairs={{0,4},{4,0},{1,5},{5,1},{2,6},{6,2},{3,7},{7,3},{8,12},{12,8},{9,1... | collective-permute-start | bytes 1179656 | tf_op jit(solution)/shard_map/ppermute | solution.py:23
  75.0 10.9 %collective-permute-start.16 = (bf16[96,2048]{1,0:T(8,128)(2,1)}, bf16[96,2048]{1,0:T(8,128)(2,1)}, u32[]{:S(2)}, u32[]{:S(2)}) collective-permute-start(bf16[96,2048]{1,0:T(8,128)(2,1)} %collective-permute-done.14.refs_2_), channel_id=1, source_target_pairs={{0,224},{32,0},{64,32},{96,64},{128,96},{160,128},{192,160},{224,1... | collective-permute-start | bytes 1179656 | tf_op jit(solution)/shard_map/ppermute | solution.py:23
  78.6 16.6 %copy-start.18 = (bf16[96,2048]{1,0:T(8,128)(2,1)}, bf16[96,2048]{1,0:T(8,128)(2,1)S(1)}, u32[]{:S(2)}) copy-start(bf16[96,2048]{1,0:T(8,128)(2,1)S(1)} %collective-permute-done.15.refs_3_) | copy-start | bytes 1179652
  78.6 10.7 %collective-permute-start.17 = (bf16[96,2048]{1,0:T(8,128)(2,1)S(1)}, bf16[96,2048]{1,0:T(8,128)(2,1)}, u32[]{:S(2)}, u32[]{:S(2)}) collective-permute-start(bf16[96,2048]{1,0:T(8,128)(2,1)S(1)} %collective-permute-done.15.refs_3_), channel_id=1, source_target_pairs={{0,32},{32,64},{64,96},{96,128},{128,160},{160,192},{192,224},{224... | collective-permute-start | bytes 1179656 | tf_op jit(solution)/shard_map/ppermute | solution.py:23
  79.6 15.6 %copy-start.5 = (bf16[128,128]{1,0:T(8,128)(2,1)}, bf16[128,128]{1,0:T(8,128)(2,1)S(1)}, u32[]{:S(2)}) copy-start(bf16[128,128]{1,0:T(8,128)(2,1)S(1)} %fusion.37.refs_0_) | copy-start | bytes 98308
  79.6 12.4 %collective-permute-start.6 = (bf16[128,128]{1,0:T(8,128)(2,1)S(1)}, bf16[128,128]{1,0:T(8,128)(2,1)S(1)}, u32[]{:S(2)}, u32[]{:S(2)}) collective-permute-start(bf16[128,128]{1,0:T(8,128)(2,1)S(1)} %fusion.37.refs_0_), channel_id=1, source_target_pairs={{0,1},{1,2},{2,3},{3,0},{4,5},{5,6},{6,7},{7,4},{8,9},{9,10},{10,1... | collective-permute-start | bytes 98312 | tf_op jit(solution)/shard_map/ppermute | solution.py:23
  85.9 22.8 %collective-permute-start.18 = (bf16[96,2048]{1,0:T(8,128)(2,1)}, bf16[96,2048]{1,0:T(8,128)(2,1)}, u32[]{:S(2)}, u32[]{:S(2)}) collective-permute-start(bf16[96,2048]{1,0:T(8,128)(2,1)} %collective-permute-done.16.refs_4_), channel_id=1, source_target_pairs={{0,224},{32,0},{64,32},{96,64},{128,96},{160,128},{192,160},{224,1... | collective-permute-start | bytes 1179656 | tf_op jit(solution)/shard_map/ppermute | solution.py:23
  89.3 19.4 %collective-permute-start.19 = (bf16[96,2048]{1,0:T(8,128)(2,1)}, bf16[96,2048]{1,0:T(8,128)(2,1)}, u32[]{:S(2)}, u32[]{:S(2)}) collective-permute-start(bf16[96,2048]{1,0:T(8,128)(2,1)} %collective-permute-done.17.refs_5_), channel_id=1, source_target_pairs={{0,32},{32,64},{64,96},{96,128},{128,160},{160,192},{192,224},{224... | collective-permute-start | bytes 1179656 | tf_op jit(solution)/shard_map/ppermute | solution.py:23
  89.5 4.3 %collective-permute-start.7 = (bf16[128,128]{1,0:T(8,128)(2,1)S(1)}, bf16[128,128]{1,0:T(8,128)(2,1)S(1)}, u32[]{:S(2)}, u32[]{:S(2)}) collective-permute-start(bf16[128,128]{1,0:T(8,128)(2,1)S(1)} %fusion.37.refs_0_), channel_id=1, source_target_pairs={{0,2},{1,3},{2,0},{3,1},{4,6},{5,7},{6,4},{7,5},{8,10},{9,11},{10,... | collective-permute-start | bytes 98312 | tf_op jit(solution)/shard_map/ppermute | solution.py:23
  92.0 3.2 %collective-permute-start.8 = (bf16[128,128]{1,0:T(8,128)(2,1)S(1)}, bf16[128,128]{1,0:T(8,128)(2,1)S(1)}, u32[]{:S(2)}, u32[]{:S(2)}) collective-permute-start(bf16[128,128]{1,0:T(8,128)(2,1)S(1)} %fusion.37.refs_0_), channel_id=1, source_target_pairs={{0,3},{1,0},{2,1},{3,2},{4,7},{5,4},{6,5},{7,6},{8,11},{9,8},{10,9... | collective-permute-start | bytes 98312 | tf_op jit(solution)/shard_map/ppermute | solution.py:23
  99.5 20.2 %all-to-all-start.1 = ((bf16[64,2,512]{2,1,0:T(2,128)(2,1)}), bf16[64,2,512]{2,1,0:T(2,128)(2,1)S(1)}, u32[]{:S(2)}, u32[]{:S(2)}) async-start(bf16[64,2,512]{2,1,0:T(2,128)(2,1)} %reshape.204), calls=%async_computation.1 | async-start | bytes 262144 | tf_op jit(solution)/shard_map/all_to_all | solution.py:282
  108.7 16.6 %copy-start.20 = (f32[2048]{0:T(1024)S(1)}, f32[2048]{0:T(1024)}, u32[]{:S(2)}) copy-start(f32[2048]{0:T(1024)} %param.41) | copy-start | bytes 24580
  119.7 19.3 %all-to-all-start.3 = ((bf16[32,24,512]{2,1,0:T(8,128)(2,1)}), bf16[32,24,512]{2,1,0:T(8,128)(2,1)}, u32[]{:S(2)}, u32[]{:S(2)}) async-start(bf16[32,24,512]{2,1,0:T(8,128)(2,1)} %dense_parts.1), calls=%async_computation.3 | async-start | bytes 1572864 | tf_op jit(solution)/shard_map/all_to_all | solution.py:269
  (14 other events, 47.7 us)

commit v2 on v0

v2 whole, which is shorter than its diff:
```python
import jax
import jax.numpy as jnp
from jax import lax
from jax.experimental import pallas as pl
from jax.experimental.pallas import tpu as pltpu
from jax.sharding import Mesh
from jax.sharding import PartitionSpec as P


EP = ("ep_0", "ep_1", "ep_2")
Z, Y, CORE, TP = "ep_0", "ep_1", "ep_2", "tp"

norm_eps = 1e-06
PIECE = 128
CHUNK = 8
EXTRA = 128
SLOTS = 16
VMEM_LIMIT = 12 * 2**20
NT = (((1,), (1,)), ((), ()))
F32 = jnp.float32
BF16 = jnp.bfloat16


def shifted(x, axis, step):
    size = lax.axis_size(axis)
    return lax.ppermute(x, axis, [(i, (i + step) % size) for i in range(size)])


def all_shifts(x, axis):
    return [x] + [shifted(x, axis, k) for k in range(1, lax.axis_size(axis))]


def silu(v):
    return v / (1.0 + jnp.exp(-v))


def dot(a, b):
    return jnp.dot(a, b, preferred_element_type=F32)


def dot_nt(a, b):
    return lax.dot_general(a, b, NT, preferred_element_type=F32)


def behind(axis, k):
    size = lax.axis_size(axis)
    return lax.rem(lax.axis_index(axis) - k + size, size)


def span(index, size):
    return pl.ds(pl.multiple_of(index * size, size), size)


def call(kernel, out, flops, moved, *operands, near=True, **more):
    if near:
        more["compiler_params"] = pltpu.CompilerParams(vmem_limit_bytes=VMEM_LIMIT)
    return pl.pallas_call(
        kernel,
        out_shape=out,
        cost_estimate=pl.CostEstimate(flops=flops, bytes_accessed=moved, transcendentals=0),
        **more,
    )(*operands)


def attention_kernel(
    lengths_ref, tokens_ref, gain_ref, bias_ref, wk_ref, wv_ref,
    wq_hbm, keys_hbm, values_hbm, wo_hbm,
    partial_ref, new_keys_ref, new_values_ref,
    wq_ref, keys_ref, values_ref, wo_ref,
    q_ref, split_ref, reach_ref, stop_ref, mixed_ref, heads_ref, sems,
):
    seq, heads, dim = q_ref.shape
    length = keys_ref.shape[2]
    pieces = length // PIECE
    chunks = seq // CHUNK

    def fetch(source, target, number):
        return pltpu.make_async_copy(source, target, sems.at[number])

    query_copy = fetch(wq_hbm, wq_ref, 0)
    key_copies = [
        fetch(keys_hbm.at[pl.ds(c * CHUNK, CHUNK)], keys_ref.at[pl.ds(c * CHUNK, CHUNK)], 2 + c)
        for c in range(chunks)
    ]
    value_copies = [
        fetch(
            values_hbm.at[pl.ds(c * CHUNK, CHUNK)],
            values_ref.at[pl.ds(c * CHUNK, CHUNK)],
            2 + chunks + c,
        )
        for c in range(chunks)
    ]
    out_copy = fetch(wo_hbm, wo_ref, 1)
    query_copy.start()
    for c in range(chunks):
        key_copies[c].start()
        value_copies[c].start()
    out_copy.start()

    wide = tokens_ref[...].astype(jnp.float32)
    scale = lax.rsqrt(jnp.mean(wide * wide, axis=-1, keepdims=True) + norm_eps)
    h_first = (wide * scale * gain_ref[...]).astype(jnp.bfloat16)
    for weight, target in ((wk_ref, new_keys_ref), (wv_ref, new_values_ref)):
        target[...] = lax.dot_general(
            h_first, weight[...], NT, preferred_element_type=jnp.float32
        ).astype(jnp.bfloat16)
    query_copy.wait()
    queries = jnp.dot(h_first, wq_ref[...], preferred_element_type=jnp.float32)
    for g in range(heads):
        q_ref[:, g, :] = queries[:, g * dim : (g + 1) * dim]

    row = lax.broadcasted_iota(jnp.int32, (2 * PIECE, 2 * PIECE), 0) % PIECE
    column = lax.broadcasted_iota(jnp.int32, (2 * PIECE, 2 * PIECE), 1)
    later = ((row > column) | (column >= PIECE)).astype(jnp.bfloat16)
    position = lax.broadcasted_iota(jnp.int32, (heads, PIECE), 1)
    head = lax.broadcasted_iota(jnp.int32, (heads, PIECE), 0)
    bias = jnp.full((heads, PIECE), bias_ref[0], jnp.float32)
    for g in range(1, heads):
        bias = jnp.where(head == g, bias_ref[g], bias)

    for c in range(chunks):
        key_copies[c].wait()
        for i in range(CHUNK):
            b = c * CHUNK + i
            scores = jnp.dot(
                q_ref[b].astype(jnp.bfloat16), keys_ref[b], preferred_element_type=jnp.float32
            )
            for p in range(pieces):
                s = scores[:, p * PIECE : (p + 1) * PIECE] * dim ** (-0.5) + bias
                inside = position < lengths_ref[b] - p * PIECE
                rest = jnp.log(1.0 + jnp.exp(-jnp.abs(s)))
                fail = jnp.where(inside, -(jnp.maximum(s, 0.0) + rest), 0.0)
                stop_ref[i, p] = jnp.where(inside, jnp.minimum(s, 0.0) - rest, -jnp.inf)
                high = fail.astype(jnp.bfloat16)
                low = (fail - high.astype(jnp.float32)).astype(jnp.bfloat16)
                at = (i * pieces + p) * heads
                split_ref[at : at + heads, :PIECE] = high.astype(jnp.float32)
                split_ref[at : at + heads, PIECE:] = low.astype(jnp.float32)
        reach_ref[...] = jnp.dot(
            split_ref[...].astype(jnp.bfloat16), later, preferred_element_type=jnp.float32
        )
        value_copies[c].wait()
        for i in range(CHUNK):
            b = c * CHUNK + i
            carried = None
            weights = [None] * pieces
            for p in reversed(range(pieces)):
                at = (i * pieces + p) * heads
                within = reach_ref[at : at + heads, :PIECE]
                whole = reach_ref[at : at + heads, PIECE:]
                exponent = stop_ref[i, p] + within
                if carried is not None:
                    exponent = exponent + carried
                weights[p] = jnp.exp(exponent)
                carried = whole if carried is None else carried + whole
            stick = jnp.concatenate(weights, axis=1).astype(jnp.bfloat16)
            mixed_ref[b] = lax.dot_general(
                stick, values_ref[b], NT, preferred_element_type=jnp.float32
            )
    for g in range(heads):
        heads_ref[:, g * dim : (g + 1) * dim] = mixed_ref[:, g, :]
    out_copy.wait()
    partial_ref[...] = jnp.dot(
        heads_ref[...].astype(jnp.bfloat16), wo_ref[...], preferred_element_type=jnp.float32
    ).astype(jnp.bfloat16)


def attention(tokens, gain, wq, wk, wv, wo, bias, keys, values, lengths):
    seq, width = tokens.shape
    dim, length = keys.shape[2], keys.shape[3]
    heads = bias.shape[0]
    keys, values = keys[:, 0], values[:, 0]
    pieces = length // PIECE
    rows = CHUNK * pieces * heads
    vmem = pl.BlockSpec(memory_space=pltpu.VMEM)
    anywhere = pl.BlockSpec(memory_space=pltpu.HBM)
    smem = pl.BlockSpec(memory_space=pltpu.SMEM)
    return pl.pallas_call(
        attention_kernel,
        out_shape=(
            jax.ShapeDtypeStruct((seq, width), jnp.bfloat16),
            jax.ShapeDtypeStruct((seq, dim), jnp.bfloat16),
            jax.ShapeDtypeStruct((seq, dim), jnp.bfloat16),
        ),
        in_specs=[smem, vmem, vmem, smem, vmem, vmem] + [anywhere] * 4,
        out_specs=(vmem, vmem, vmem),
        scratch_shapes=[
            pltpu.VMEM(wq.shape, jnp.bfloat16),
            pltpu.VMEM(keys.shape, jnp.bfloat16),
            pltpu.VMEM(values.shape, jnp.bfloat16),
            pltpu.VMEM(wo.shape, jnp.bfloat16),
            pltpu.VMEM((seq, heads, dim), jnp.float32),
            pltpu.VMEM((rows, 2 * PIECE), jnp.float32),
            pltpu.VMEM((rows, 2 * PIECE), jnp.float32),
            pltpu.VMEM((CHUNK, pieces, heads, PIECE), jnp.float32),
            pltpu.VMEM((seq, heads, dim), jnp.float32),
            pltpu.VMEM((seq, heads * dim), jnp.float32),
            pltpu.SemaphoreType.DMA((2 + 2 * (seq // CHUNK),)),
        ],
        cost_estimate=pl.CostEstimate(
            flops=400_000_000, bytes_accessed=11_000_000, transcendentals=600_000
        ),
        name="attention",
    )(lengths, tokens, gain[None, :], bias, wk, wv, wq, keys, values, wo)


def prepare_kernel(gate_ref, up_ref, *outs_and_scratch):
    outs, (gates, ups) = outs_and_scratch[:-2], outs_and_scratch[-2:]
    units = outs[0].shape[0] // 2
    gates[...] = gate_ref[...].T
    ups[...] = up_ref[...].T
    for k, out in enumerate(outs):
        at = span(behind(TP, -k), units)
        out[:units, :] = gates[at, :]
        out[units:, :] = ups[at, :]


def prepare(d_gate, d_up):
    tps = lax.axis_size(TP)
    width, units = d_gate.shape
    one = jax.ShapeDtypeStruct((2 * units // tps, width), BF16)
    turned = pltpu.VMEM((units, width), BF16)
    return call(
        prepare_kernel, (one,) * tps, 0, 600_000, d_gate, d_up,
        scratch_shapes=[turned, turned],
    )


def norm_kernel(tokens_ref, gain_ref, routes_ref, *refs):
    parts, (payload_ref, slice_ref, resid_ref) = refs[:-3], refs[-3:]
    seq, width = tokens_ref.shape
    attended = parts[0][...].astype(F32)
    for part in parts[1:]:
        attended = attended + part[...].astype(F32)
    resid = tokens_ref[...].astype(F32) + attended
    resid_ref[...] = resid
    scale = lax.rsqrt(jnp.mean(resid * resid, axis=-1, keepdims=True) + norm_eps)
    payload_ref[:, :width] = (resid * scale * gain_ref[...]).astype(BF16)
    lane = lax.broadcasted_iota(jnp.int32, (seq, EXTRA), 1)
    routes = routes_ref[...]
    named = jnp.where(lane == 0, routes[:, 0:1], jnp.where(lane == 1, routes[:, 1:2], 0))
    payload_ref[:, width:] = named.astype(F32).astype(BF16)
    slice_ref[...] = resid_ref[:, span(lax.axis_index(TP), slice_ref.shape[1])]


def norm_payload(tokens, gain, routes, parts):
    seq, width = tokens.shape
    return call(
        norm_kernel,
        (
            jax.ShapeDtypeStruct((seq, width + EXTRA), BF16),
            jax.ShapeDtypeStruct((seq, width // lax.axis_size(TP)), F32),
        ),
        1_000_000, 600_000, tokens, gain[None, :], routes, *parts,
        scratch_shapes=[pltpu.VMEM((seq, width), F32)],
    )


def group_routes(tokens):
    width = tokens[0].shape[1] - EXTRA
    extra = jnp.concatenate([ref[:, width:].astype(F32) for ref in tokens], axis=0)
    first, second = extra[:, 0:1], extra[:, 1:2]
    slots = lax.axis_size(Z) * SLOTS
    lane = lax.broadcasted_iota(jnp.int32, (extra.shape[0], slots), 1)
    plane = lax.axis_size(Y) * lax.axis_size(CORE)
    place = lax.axis_index(Y) * lax.axis_size(CORE) + lax.axis_index(CORE)
    expert = ((lane // SLOTS) * plane + place).astype(F32)
    return first, second, expert, (lane % SLOTS).astype(F32)


def select_kernel(*refs):
    tokens, (rows_ref, hot_ref) = refs[:-2], refs[-2:]
    part = rows_ref.shape[1]
    first, second, expert, slot = group_routes(tokens)
    match = ((first == expert) | (second == expert)).astype(F32)
    count = match.shape[0]
    row = lax.broadcasted_iota(jnp.int32, (count, count), 0)
    column = lax.broadcasted_iota(jnp.int32, (count, count), 1)
    rank = dot((column < row).astype(BF16), match.astype(BF16))
    hot = jnp.where(rank == slot, match, 0.0)
    hot_ref[...] = hot.astype(BF16)
    mine = jnp.concatenate(
        [ref[:, span(lax.axis_index(TP), part)].astype(F32) for ref in tokens], axis=0
    ).astype(BF16)
    rows_ref[...] = dot(hot.T.astype(BF16), mine).astype(BF16)


def select(tokens, part):
    slots = lax.axis_size(Z) * SLOTS
    count = len(tokens) * tokens[0].shape[0]
    return call(
        select_kernel,
        (
            jax.ShapeDtypeStruct((slots, part), BF16),
            jax.ShapeDtypeStruct((count, slots), BF16),
        ),
        40_000_000, 1_000_000, *tokens,
    )


def share_kernel(hot_ref, group_ref, fine_ref, mix_ref, *refs):
    tokens, (high_ref, low_ref, gate_ref) = refs[:-3], refs[-3:]
    width = group_ref.shape[1]
    per_group = fine_ref.shape[0] // group_ref.shape[0]
    rows = jnp.concatenate([ref[:, :width].astype(F32) for ref in tokens], axis=0)
    narrow = rows.astype(BF16)
    group_logits = dot_nt(narrow, group_ref[...])
    fine_logits = dot_nt(narrow, fine_ref[...])
    first, second, expert, _ = group_routes(tokens)
    group = lax.broadcasted_iota(jnp.int32, group_logits.shape, 1)
    own = (first.astype(jnp.int32) // per_group) == group
    own_logit = jnp.sum(jnp.where(own, group_logits, 0.0), axis=1, keepdims=True)
    group_share = 1.0 / jnp.sum(jnp.exp(group_logits - own_logit), axis=1, keepdims=True)
    fine = lax.broadcasted_iota(jnp.int32, fine_logits.shape, 1).astype(F32)
    picked = [
        jnp.sum(jnp.where(fine == chosen, fine_logits, 0.0), axis=1, keepdims=True)
        for chosen in (first, second)
    ]
    weight = 0.0
    for chosen, here, there in ((first, 0, 1), (second, 1, 0)):
        share = group_share * (1.0 / (1.0 + jnp.exp(picked[there] - picked[here])))
        weight = weight + jnp.where(chosen == expert, share, 0.0)
    weight = weight * hot_ref[...].astype(F32)
    high = weight.astype(BF16)
    high_ref[...] = high
    low_ref[...] = (weight - high.astype(F32)).astype(BF16)
    mix = jnp.sum(rows * mix_ref[...], axis=1, keepdims=True)
    gate_ref[...] = jnp.broadcast_to(1.0 / (1.0 + jnp.exp(-mix)), gate_ref.shape)


def share_weights(hot, w_group, w_fine, w_mix, tokens):
    table = jax.ShapeDtypeStruct(hot.shape, BF16)
    return call(
        share_kernel,
        (table, table, jax.ShapeDtypeStruct((hot.shape[0], EXTRA), F32)),
        60_000_000, 1_500_000, hot, w_group.T, w_fine.T, w_mix[None, :], *tokens, near=False,
    )


def expert_in_kernel(rows_ref, gate_ref, up_ref, out_ref):
    units = gate_ref.shape[1]
    rows = rows_ref[...]
    out_ref[:, :units] = dot(rows, gate_ref[...]).astype(BF16)
    out_ref[:, units:] = dot(rows, up_ref[...]).astype(BF16)


def expert_in(rows, gate, up):
    return call(
        expert_in_kernel,
        jax.ShapeDtypeStruct((rows.shape[0], 2 * gate.shape[1]), BF16),
        140_000_000, 1_400_000, rows, gate, up,
    )


def expert_out_kernel(*refs):
    parts, (down_ref, out_ref) = refs[:-2], refs[-2:]
    units = down_ref.shape[0]
    act = parts[0][...].astype(F32)
    for part in parts[1:]:
        act = act + part[...].astype(F32)
    hidden = (silu(act[:, :units]) * act[:, units:]).astype(BF16)
    out_ref[...] = dot(hidden, down_ref[...]).astype(BF16)


def expert_out(parts, down):
    return call(
        expert_out_kernel,
        jax.ShapeDtypeStruct((parts[0].shape[0], down.shape[1]), BF16),
        70_000_000, 1_800_000, *parts, down,
    )


def dense_in_kernel(*refs):
    out_ref = refs[-1]
    planes, tps = lax.axis_size(Z), lax.axis_size(TP)
    tokens, blocks = refs[: -planes - 1], refs[-planes - 1 : -1]
    width = blocks[0].shape[1]
    units = out_ref.shape[1] // planes
    gate = up = 0.0
    for k in range(tps):
        at = span(behind(TP, k), width)
        rows = jnp.concatenate([ref[:, at].astype(F32) for ref in tokens], axis=0).astype(BF16)
        low, mid, top = 2 * k * units, (2 * k + 1) * units, (2 * k + 2) * units
        gate = gate + dot_nt(rows, jnp.concatenate([b[low:mid, :] for b in blocks], axis=0))
        up = up + dot_nt(rows, jnp.concatenate([b[mid:top, :] for b in blocks], axis=0))
    out_ref[...] = (silu(gate) * up).astype(BF16)


def dense_in(tokens, blocks):
    count = len(tokens) * tokens[0].shape[0]
    rows, width = blocks[0].shape
    whole = pl.BlockSpec(memory_space=pltpu.VMEM)
    upper = pl.BlockSpec((rows * 2 // 3, width), lambda i: (0, 0))
    kept = lambda shape: pl.BlockSpec(shape, lambda i: (0, 0))
    return call(
        dense_in_kernel,
        jax.ShapeDtypeStruct((count, rows * 2 // 3), BF16),
        400_000_000, 3_000_000, *tokens, *blocks, near=False,
        grid=(1,),
        in_specs=[kept(x.shape) for x in tokens] + [upper] * len(blocks),
        out_specs=kept((count, rows * 2 // 3)),
    )


def dense_out_kernel(*refs):
    gate_ref, out_ref = refs[-2:]
    planes, tps = lax.axis_size(Z), lax.axis_size(TP)
    hiddens, blocks = refs[:tps], refs[tps : tps + planes]
    units = blocks[0].shape[0] // tps
    total = 0.0
    for k in range(tps):
        at = span(behind(TP, k), units)
        total = total + dot(
            hiddens[k][...], jnp.concatenate([b[at, :] for b in blocks], axis=0)
        )
    out_ref[...] = total * gate_ref[:, 0:1]


def dense_out(hiddens, blocks, gate):
    count = hiddens[0].shape[0]
    rows, width = blocks[0].shape
    kept = lambda shape: pl.BlockSpec(shape, lambda i: (0, 0))
    lower = pl.BlockSpec((rows // 3, width), lambda i: (2, 0))
    return call(
        dense_out_kernel,
        jax.ShapeDtypeStruct((count, width), F32),
        400_000_000, 2_000_000, *hiddens, *blocks, gate, near=False,
        grid=(1,),
        in_specs=[kept(x.shape) for x in hiddens] + [lower] * len(blocks) + [kept(gate.shape)],
        out_specs=kept((count, width)),
    )


def gather_kernel(dense_ref, rows_ref, high_ref, low_ref, out_ref):
    rows = rows_ref[...]
    total = dense_ref[...] + (dot(high_ref[...], rows) + dot(low_ref[...], rows))
    seq = out_ref.shape[1]
    ys, c = lax.axis_size(Y), lax.axis_index(CORE)
    for other in range(2):
        core = c if other == 0 else 1 - c
        for j in range(ys):
            at = (other * ys + j) * seq
            out_ref[behind(Y, j) * 2 + core] = total[at : at + seq].astype(BF16)


def gather_rows(dense, rows, high, low, seq):
    return call(
        gather_kernel,
        jax.ShapeDtypeStruct((dense.shape[0] // seq, seq, dense.shape[1]), BF16),
        60_000_000, 1_000_000, dense, rows, high, low, near=False,
    )


def finish_kernel(resid_ref, parts_ref, out_ref):
    total = resid_ref[...]
    for i in range(parts_ref.shape[0]):
        total = total + parts_ref[i].astype(F32)
    out_ref[...] = total.astype(BF16)


def finish(resid, parts):
    return call(finish_kernel, jax.ShapeDtypeStruct(resid.shape, BF16), 0, 400_000, resid, parts)


def along_z(own):
    blocks = [own]
    right = left = own
    for _ in range(1, lax.axis_size(Z) // 2 + 1):
        right = shifted(right, Z, 1)
        blocks.append(right)
        if len(blocks) < lax.axis_size(Z):
            left = shifted(left, Z, -1)
            blocks.append(left)
    return blocks


def over_z(rows):
    planes = lax.axis_size(Z)
    shaped = rows.reshape(planes, -1, rows.shape[1])
    return lax.all_to_all(shaped, Z, split_axis=0, concat_axis=0, tiled=True).reshape(rows.shape)


def shards(
    tokens,
    norm_attn,
    w_query,
    w_key,
    w_value,
    w_out,
    head_bias,
    key_cache,
    value_cache,
    lengths,
    norm_ffn,
    w_group,
    w_fine,
    routes,
    e_gate,
    e_up,
    e_down,
    d_gate,
    d_up,
    d_down,
    w_mix,
):
    seq_count = tokens.shape[0]
    width_part = d_gate.shape[0]
    kv_local = key_cache.shape[1]
    head_dim = key_cache.shape[3]
    wide = prepare(d_gate, d_up)
    arrived = [wide[0]] + [shifted(wide[k], TP, k) for k in range(1, len(wide))]
    partial_value, new_keys, new_values = attention(
        tokens,
        norm_attn,
        w_query,
        w_key.T,
        w_value.T,
        w_out,
        head_bias,
        key_cache.transpose(0, 1, 3, 2),
        value_cache.transpose(0, 1, 3, 2),
        lengths,
    )
    parts = all_shifts(partial_value, TP)
    own = jnp.concatenate([*arrived, d_down], axis=0)
    blocks = along_z(own)
    payload, resid = norm_payload(tokens, norm_ffn, routes, parts)
    here = all_shifts(payload, Y)
    group = here + [shifted(x, CORE, 1) for x in here]
    rows, hot = select(group, width_part)
    rows = over_z(rows)
    pre = expert_in(rows, e_gate[0], e_up[0])
    pres = all_shifts(pre, TP)
    result = expert_out(pres, e_down[0])
    returned = over_z(result)
    high, low, gate = share_weights(hot, w_group, w_fine, w_mix, group)
    hidden = dense_in(group, blocks)
    hiddens = all_shifts(hidden, TP)
    dense = dense_out(hiddens, blocks, gate)
    parts = gather_rows(dense, returned, high, low, seq_count)
    parts = lax.all_to_all(parts, (Y, CORE), split_axis=0, concat_axis=0, tiled=True)
    mixed = finish(resid, parts)
    return (
        mixed,
        new_keys.reshape(seq_count, kv_local, head_dim),
        new_values.reshape(seq_count, kv_local, head_dim),
    )


def solution(mesh):
    torus = Mesh(mesh.devices.reshape(8, 4, 2, mesh.shape["tp"]), ("ep_0", "ep_1", "ep_2", "tp"))
    placed = (
        P(EP, None),
        P(),
        P(None, "tp"),
        P(None, "tp"),
        P(None, "tp"),
        P("tp", None),
        P("tp"),
        P(EP, "tp", None, None),
        P(EP, "tp", None, None),
        P(EP),
        P(),
        P(),
        P(),
        P(EP, None),
        P(EP, "tp", None),
        P(EP, "tp", None),
        P(EP, None, "tp"),
        P("tp", EP),
        P("tp", EP),
        P(EP, "tp"),
        P(),
    )
    return jax.shard_map(
        shards,
        mesh=torus,
        in_specs=placed,
        out_specs=(P(EP, "tp"), P(EP, "tp", None), P(EP, "tp", None)),
        check_vma=False,
    )
```

time: 222 us -> 126 us (0.57)
  blocking collectives: 65.4 us -> 11.9 us
  matrix products: 27.1 us -> 0 us
  waiting for transfers between devices: 65.6 us -> 40.5 us
  Pallas kernels: 0 us -> 21.6 us
  starting transfers between devices: 24.6 us -> 44.6 us
  between operations: 14.4 us -> 0.93 us
  other arithmetic: 9.43 us -> 0 us
  local copies, waits for them, and re-layouts: 14.4 us -> 5.71 us
    all_to_all x5 -> x2, waiting for transfers between devices: 64.9 us -> 5.19 us  [over_z(): lax.all_to_all(shaped, Z, split_axis=0, concat_axis=0, tiled=True)]
    all_gather x2 -> x0, blocking collectives: 36.5 us -> none  [all_blocks(): tiles = lax.all_gather(tiles, axes[k], axis=0, tiled=True)]
    ppermute x0 -> x26, starting transfers between devices: none -> 35.7 us  [shifted(): return lax.ppermute(x, axis, [(i, (i + step) % size) for i in range(size)])]
    ppermute x0 -> x26, waiting for transfers between devices: none -> 35.3 us  [shifted(): return lax.ppermute(x, axis, [(i, (i + step) % size) for i in range(size)])]
    dot_general x17 -> x0, matrix products: 27.1 us -> none  [the longest x1 5.27 us: shards(): jnp.dot(own_hidden, lax.all_gather(d_down, EP, axis=0, tiled=True), prefe...]
    pallas_call x0 -> x11, Pallas kernels: none -> 21.6 us  [the longest x10 14 us: call(): pl.pallas_call(kernel, out_shape=out, cost_estimate=pl.CostEstimate(flops...]
    all_to_all x1, blocking collectives: 28.8 us -> 11.9 us  [shards(): lax.all_to_all(parts, (Y, CORE), split_axis=0, concat_axis=0, tiled=True)]
    all_to_all x5 -> x2, starting transfers between devices: 24.6 us -> 8.93 us  [over_z(): lax.all_to_all(shaped, Z, split_axis=0, concat_axis=0, tiled=True)]
  transfers between devices with their start and end apart: 7 -> 28, of which waited for: 5 -> 15; matrix products, arithmetic and copies ran while one was open for 12% -> 0% of each run, Pallas kernels for 0% -> 15%
where the time goes in v2:
time: 126 us; the launch traced here: 125 us
  starting transfers between devices  44.6 us (35%)
  waiting for transfers between devices  40.5 us (32%)
  Pallas kernels  21.6 us (17%)
  blocking collectives  11.9 us (9%)
  local copies, waits for them, and re-layouts  5.71 us (5%)
    ppermute x26, starting transfers between devices, shifted(): return lax.ppermute(x, axis, [(i, (i + step) % size) for i in range(size)])  35.7 us
    ppermute x26, waiting for transfers between devices, shifted(): return lax.ppermute(x, axis, [(i, (i + step) % size) for i in range(size)])  35.3 us
    pallas_call x10, Pallas kernels, call(): pl.pallas_call(kernel, out_shape=out, cost_estimate=pl.CostEstimate(flops...  14 us
    all_to_all x1, blocking collectives, shards(): lax.all_to_all(parts, (Y, CORE), split_axis=0, concat_axis=0, tiled=True)  11.9 us
    all_to_all x2, starting transfers between devices, over_z(): lax.all_to_all(shaped, Z, split_axis=0, concat_axis=0, tiled=True)  8.93 us
    pallas_call x1, Pallas kernels, attention(): pl.pallas_call(attention_kernel, out_shape=(jax.ShapeDtypeStruct((seq, wi...  7.57 us
    all_to_all x2, waiting for transfers between devices, over_z(): lax.all_to_all(shaped, Z, split_axis=0, concat_axis=0, tiled=True)  5.19 us
    unnamed x57, local copies, waits for them, and re-layouts  4.8 us
  transfers between devices with their start and end apart: 28, of which 15 were waited for; matrix products, arithmetic and copies ran while one was open for 0% of the time, Pallas kernels for 15%

profile of v2, /device:TPU:1, one launch (start us, length us, event | category | flops | bytes accessed | tf_op | source)
XLA Modules:
  0.0 125.3 jit_solution(7197909165656191900)
XLA Ops:
  2.6 2.1 %collective-permute-start.10 = (bf16[64,512]{1,0:T(8,128)(2,1)S(1)}, bf16[64,512]{1,0:T(8,128)(2,1)S(1)}, u32[]{:S(2)}, u32[]{:S(2)}) collective-permute-start(bf16[64,512]{1,0:T(8,128)(2,1)S(1)} %get-tuple-element.21), channel_id=1, source_target_pairs={{0,1},{1,2},{2,3},{3,0},{4,5},{5,6},{6,7},{7,4},{8,9},{9,10},{10,1... | collective-permute-start | bytes 196616 | tf_op jit(solution)/shard_map/ppermute | solution.py:26
  4.7 2.5 %collective-permute-start.11 = (bf16[64,512]{1,0:T(8,128)(2,1)S(1)}, bf16[64,512]{1,0:T(8,128)(2,1)S(1)}, u32[]{:S(2)}, u32[]{:S(2)}) collective-permute-start(bf16[64,512]{1,0:T(8,128)(2,1)S(1)} %get-tuple-element.22), channel_id=1, source_target_pairs={{0,2},{1,3},{2,0},{3,1},{4,6},{5,7},{6,4},{7,5},{8,10},{9,11},{10,... | collective-permute-start | bytes 196616 | tf_op jit(solution)/shard_map/ppermute | solution.py:26
  7.1 1.2 collective-permute-start.12
  8.3 1.4 %collective-permute-done.11 = bf16[64,512]{1,0:T(8,128)(2,1)S(1)} collective-permute-done((bf16[64,512]{1,0:T(8,128)(2,1)S(1)}, bf16[64,512]{1,0:T(8,128)(2,1)S(1)}, u32[]{:S(2)}, u32[]{:S(2)}) %collective-permute-start.11) | collective-permute-done | bytes 65568 | tf_op jit(solution)/shard_map/ppermute | solution.py:26
  11.5 2.0 %collective-permute-start.13 = (bf16[384,512]{1,0:T(8,128)(2,1)S(1)}, bf16[384,512]{1,0:T(8,128)(2,1)S(1)}, u32[]{:S(2)}, u32[]{:S(2)}) collective-permute-start(bf16[384,512]{1,0:T(8,128)(2,1)S(1)} %constant_dynamic-update-slice_fusion.refs_8_.refs_4_), channel_id=1, source_target_pairs={{0,32},{32,64},{64,96},{96,128},{128,160},{160,192},{192,224},{224... | collective-permute-start | bytes 1179656 | tf_op jit(solution)/shard_map/ppermute | solution.py:26
  13.4 4.0 %collective-permute-start.14 = (bf16[384,512]{1,0:T(8,128)(2,1)S(1)}, bf16[384,512]{1,0:T(8,128)(2,1)}, u32[]{:S(2)}, u32[]{:S(2)}) collective-permute-start(bf16[384,512]{1,0:T(8,128)(2,1)S(1)} %constant_dynamic-update-slice_fusion.refs_8_.refs_4_), channel_id=1, source_target_pairs={{0,224},{32,0},{64,32},{96,64},{128,96},{160,128},{192,160},{224,1... | collective-permute-start | bytes 1179656 | tf_op jit(solution)/shard_map/ppermute | solution.py:26
  17.5 7.6 %collective-permute-done.13.refs_9_.refs_5_ = bf16[384,512]{1,0:T(8,128)(2,1)S(1)} collective-permute-done((bf16[384,512]{1,0:T(8,128)(2,1)S(1)}, bf16[384,512]{1,0:T(8,128)(2,1)S(1)}, u32[]{:S(2)}, u32[]{:S(2)}) %collective-permute-start.13) | collective-permute-done | bytes 393248 | tf_op jit(solution)/shard_map/ppermute | solution.py:26
  25.1 7.6 %attention.1 = (bf16[24,2048]{1,0:T(8,128)(2,1)}, bf16[24,64]{1,0:T(8,128)(2,1)}, bf16[24,64]{1,0:T(8,128)(2,1)}) custom-call(s32[24]{0:T(128)} %lengths_ref.1, bf16[24,2048]{1,0:T(8,128)(2,1)} %tokens_ref.3, f32[1,2048]{1,0:T(1,128)} %bitcast.38, f32[8]{0:T(128)} %bias_ref.1, bf16[64,2048]{1,0:T(8,128)(2,1)} %bitcast.34, bf16[64,2048]{1,0:T(8,128)(2,1)} %bitcast.35, ...), custom_call_target="tpu_custom_call" | custom-call | flops 400000000 | bytes 11000000 | tf_op jit(solution)/shard_map/attention/pallas_call | solution.py:178
  32.7 1.9 %collective-permute-start.2 = (bf16[24,2048]{1,0:T(8,128)(2,1)}, bf16[24,2048]{1,0:T(8,128)(2,1)S(1)}, u32[]{:S(2)}, u32[]{:S(2)}) collective-permute-start(bf16[24,2048]{1,0:T(8,128)(2,1)} %get-tuple-element.17.refs_0_), channel_id=1, source_target_pairs={{0,3},{1,0},{2,1},{3,2},{4,7},{5,4},{6,5},{7,6},{8,11},{9,8},{10,9... | collective-permute-start | bytes 294920 | tf_op jit(solution)/shard_map/ppermute | solution.py:26
  35.4 2.2 %collective-permute-done.2.refs_3_ = bf16[24,2048]{1,0:T(8,128)(2,1)S(1)} collective-permute-done((bf16[24,2048]{1,0:T(8,128)(2,1)}, bf16[24,2048]{1,0:T(8,128)(2,1)S(1)}, u32[]{:S(2)}, u32[]{:S(2)}) %collective-permute-start.2) | collective-permute-done | bytes 98336 | tf_op jit(solution)/shard_map/ppermute | solution.py:26
  37.6 2.3 %collective-permute-done.1.refs_2_ = bf16[24,2048]{1,0:T(8,128)(2,1)S(1)} collective-permute-done((bf16[24,2048]{1,0:T(8,128)(2,1)}, bf16[24,2048]{1,0:T(8,128)(2,1)S(1)}, u32[]{:S(2)}, u32[]{:S(2)}) %collective-permute-start.1) | collective-permute-done | bytes 98336 | tf_op jit(solution)/shard_map/ppermute | solution.py:26
  41.6 4.2 %collective-permute-start.6 = (bf16[24,2176]{1,0:T(8,128)(2,1)S(1)}, bf16[24,2176]{1,0:T(8,128)(2,1)S(1)}, u32[]{:S(2)}, u32[]{:S(2)}) collective-permute-start(bf16[24,2176]{1,0:T(8,128)(2,1)S(1)} %get-tuple-element.19.refs_0_), channel_id=1, source_target_pairs={{0,4},{4,0},{1,5},{5,1},{2,6},{6,2},{3,7},{7,3},{8,12},{12,8},{9,1... | collective-permute-start | bytes 313352 | tf_op jit(solution)/shard_map/ppermute | solution.py:26
  45.8 2.8 %collective-permute-start.16 = (bf16[384,512]{1,0:T(8,128)(2,1)}, bf16[384,512]{1,0:T(8,128)(2,1)S(1)}, u32[]{:S(2)}, u32[]{:S(2)}) collective-permute-start(bf16[384,512]{1,0:T(8,128)(2,1)} %collective-permute-done.14.refs_10_.refs_6_), channel_id=1, source_target_pairs={{0,224},{32,0},{64,32},{96,64},{128,96},{160,128},{192,160},{224,1... | collective-permute-start | bytes 1179656 | tf_op jit(solution)/shard_map/ppermute | solution.py:26
  48.7 2.7 %collective-permute-start.5 = (bf16[24,2176]{1,0:T(8,128)(2,1)S(1)}, bf16[24,2176]{1,0:T(8,128)(2,1)S(1)}, u32[]{:S(2)}, u32[]{:S(2)}) collective-permute-start(bf16[24,2176]{1,0:T(8,128)(2,1)S(1)} %get-tuple-element.19.refs_0_), channel_id=1, source_target_pairs={{0,24},{8,0},{16,8},{24,16},{1,25},{9,1},{17,9},{25,17},{2,26},{10... | collective-permute-start | bytes 313352 | tf_op jit(solution)/shard_map/ppermute | solution.py:26
  52.4 3.0 %collective-permute-done.5.refs_3_ = bf16[24,2176]{1,0:T(8,128)(2,1)S(1)} collective-permute-done((bf16[24,2176]{1,0:T(8,128)(2,1)S(1)}, bf16[24,2176]{1,0:T(8,128)(2,1)S(1)}, u32[]{:S(2)}, u32[]{:S(2)}) %collective-permute-start.5) | collective-permute-done | bytes 104480 | tf_op jit(solution)/shard_map/ppermute | solution.py:26
  55.4 1.4 %collective-permute-start.9 = (bf16[24,2176]{1,0:T(8,128)(2,1)S(1)}, bf16[24,2176]{1,0:T(8,128)(2,1)S(1)}, u32[]{:S(2)}, u32[]{:S(2)}) collective-permute-start(bf16[24,2176]{1,0:T(8,128)(2,1)S(1)} %collective-permute-done.5.refs_3_), channel_id=1, source_target_pairs={{0,4},{4,0},{1,5},{5,1},{2,6},{6,2},{3,7},{7,3},{8,12},{12,8},{9,1... | collective-permute-start | bytes 313352 | tf_op jit(solution)/shard_map/ppermute | solution.py:26
  56.8 2.6 %collective-permute-start.8 = (bf16[24,2176]{1,0:T(8,128)(2,1)S(1)}, bf16[24,2176]{1,0:T(8,128)(2,1)S(1)}, u32[]{:S(2)}, u32[]{:S(2)}) collective-permute-start(bf16[24,2176]{1,0:T(8,128)(2,1)S(1)} %collective-permute-done.4.refs_2_), channel_id=1, source_target_pairs={{0,4},{4,0},{1,5},{5,1},{2,6},{6,2},{3,7},{7,3},{8,12},{12,8},{9,1... | collective-permute-start | bytes 313352 | tf_op jit(solution)/shard_map/ppermute | solution.py:26
  61.4 1.1 shard_map.223
  63.2 5.6 %all-to-all-start = ((bf16[8,16,512]{2,1,0:T(8,128)(2,1)}), bf16[8,16,512]{2,1,0:T(8,128)(2,1)S(1)}, u32[]{:S(2)}, u32[]{:S(2)}) async-start(bf16[8,16,512]{2,1,0:T(8,128)(2,1)} %bitcast.13), calls=%async_computation | async-start | bytes 262144 | tf_op jit(solution)/shard_map/all_to_all | solution.py:480
  68.8 2.7 %collective-permute-start.18 = (bf16[384,512]{1,0:T(8,128)(2,1)S(1)}, bf16[384,512]{1,0:T(8,128)(2,1)}, u32[]{:S(2)}, u32[]{:S(2)}) collective-permute-start(bf16[384,512]{1,0:T(8,128)(2,1)S(1)} %collective-permute-done.16.refs_12_.refs_8_), channel_id=1, source_target_pairs={{0,224},{32,0},{64,32},{96,64},{128,96},{160,128},{192,160},{224,1... | collective-permute-start | bytes 1179656 | tf_op jit(solution)/shard_map/ppermute | solution.py:26
  71.5 5.2 %all-to-all-done = bf16[8,16,512]{2,1,0:T(8,128)(2,1)S(1)} async-done(((bf16[8,16,512]{2,1,0:T(8,128)(2,1)}), bf16[8,16,512]{2,1,0:T(8,128)(2,1)S(1)}, u32[]{:S(2)}, u32[]{:S(2)}) %all-to-all-start) | async-done | bytes 131104 | tf_op jit(solution)/shard_map/all_to_all | solution.py:480
  78.9 3.8 %collective-permute-done.25.refs_3_ = bf16[128,1024]{1,0:T(8,128)(2,1)S(1)} collective-permute-done((bf16[128,1024]{1,0:T(8,128)(2,1)S(1)}, bf16[128,1024]{1,0:T(8,128)(2,1)S(1)}, u32[]{:S(2)}, u32[]{:S(2)}) %collective-permute-start.25) | collective-permute-done | bytes 262176 | tf_op jit(solution)/shard_map/ppermute | solution.py:26
  82.7 1.8 %collective-permute-done.24.refs_2_ = bf16[128,1024]{1,0:T(8,128)(2,1)S(1)} collective-permute-done((bf16[128,1024]{1,0:T(8,128)(2,1)S(1)}, bf16[128,1024]{1,0:T(8,128)(2,1)S(1)}, u32[]{:S(2)}, u32[]{:S(2)}) %collective-permute-start.24) | collective-permute-done | bytes 262176 | tf_op jit(solution)/shard_map/ppermute | solution.py:26
  84.5 7.9 %collective-permute-done.23.refs_1_ = bf16[128,1024]{1,0:T(8,128)(2,1)S(1)} collective-permute-done((bf16[128,1024]{1,0:T(8,128)(2,1)S(1)}, bf16[128,1024]{1,0:T(8,128)(2,1)S(1)}, u32[]{:S(2)}, u32[]{:S(2)}) %collective-permute-start.23) | collective-permute-done | bytes 262176 | tf_op jit(solution)/shard_map/ppermute | solution.py:26
  93.4 3.4 %all-to-all-start.1 = ((bf16[8,16,512]{2,1,0:T(8,128)(2,1)}), bf16[8,16,512]{2,1,0:T(8,128)(2,1)S(1)}, u32[]{:S(2)}, u32[]{:S(2)}) async-start(bf16[8,16,512]{2,1,0:T(8,128)(2,1)} %bitcast.18), calls=%async_computation.1 | async-start | bytes 262144 | tf_op jit(solution)/shard_map/all_to_all | solution.py:480
  96.9 3.3 %shard_map.222.refs_0_ = bf16[192,256]{1,0:T(8,128)(2,1)} custom-call(bf16[24,2176]{1,0:T(8,128)(2,1)} %copy-done, bf16[24,2176]{1,0:T(8,128)(2,1)} %copy-done.4, bf16[24,2176]{1,0:T(8,128)(2,1)} %copy-done.3, bf16[24,2176]{1,0:T(8,128)(2,1)} %copy-done.2, bf16[24,2176]{1,0:T(8,128)(2,1)} %copy-done.1, bf16[24,2176]{1,0:T(8,128)(2,1)} %copy-done.7, ...), custom_call_target="tpu_custom_call" | custom-call | flops 400000000 | bytes 3000000 | tf_op jit(solution)/shard_map/pallas_call | solution.py:57
  100.4 1.3 %collective-permute-start.20 = (bf16[192,256]{1,0:T(8,128)(2,1)}, bf16[192,256]{1,0:T(8,128)(2,1)S(1)}, u32[]{:S(2)}, u32[]{:S(2)}) collective-permute-start(bf16[192,256]{1,0:T(8,128)(2,1)} %shard_map.222.refs_0_), channel_id=1, source_target_pairs={{0,1},{1,2},{2,3},{3,0},{4,5},{5,6},{6,7},{7,4},{8,9},{9,10},{10,1... | collective-permute-start | bytes 294920 | tf_op jit(solution)/shard_map/ppermute | solution.py:26
  101.7 2.7 %shard_map.224 = (bf16[192,128]{1,0:T(8,128)(2,1)}, bf16[192,128]{1,0:T(8,128)(2,1)}, f32[192,128]{1,0:T(8,128)}) custom-call(bf16[192,128]{1,0:T(8,128)(2,1)} %copy-done.15, bf16[4,2048]{1,0:T(4,128)(2,1)} %bitcast.37, bf16[64,2048]{1,0:T(8,128)(2,1)} %bitcast.36, f32[1,2048]{1,0:T(1,128)} %bitcast.39, bf16[24,2176]{1,0:T(8,128)(2,1)} %copy-done, ...), custom_call_target="tpu_custom_call" | custom-call | flops 60000000 | bytes 1500000 | tf_op jit(solution)/shard_map/pallas_call | solution.py:57
  104.5 1.3 %collective-permute-done.21.refs_2_ = bf16[192,256]{1,0:T(8,128)(2,1)S(1)} collective-permute-done((bf16[192,256]{1,0:T(8,128)(2,1)}, bf16[192,256]{1,0:T(8,128)(2,1)S(1)}, u32[]{:S(2)}, u32[]{:S(2)}) %collective-permute-start.21) | collective-permute-done | bytes 98336 | tf_op jit(solution)/shard_map/ppermute | solution.py:26
  107.5 2.6 %shard_map.225.dense_ref = f32[192,512]{1,0:T(8,128)} custom-call(bf16[192,256]{1,0:T(8,128)(2,1)} %shard_map.222.refs_0_, bf16[192,256]{1,0:T(8,128)(2,1)} %copy-done.24, bf16[192,256]{1,0:T(8,128)(2,1)} %copy-done.23, bf16[192,256]{1,0:T(8,128)(2,1)} %copy-done.22, bf16[384,512]{1,0:T(8,128)(2,1)} %copy-done.17, bf16[384,512]{1,0:T(8,128)(2,1)} %copy-done.18, ...), custom_call_target="tpu_custom_call" | custom-call | flops 400000000 | bytes 2000000 | tf_op jit(solution)/shard_map/pallas_call | solution.py:57
  110.8 2.0 %shard_map.228 = bf16[8,24,512]{2,1,0:T(8,128)(2,1)} custom-call(f32[192,512]{1,0:T(8,128)} %shard_map.225.dense_ref, bf16[128,512]{1,0:T(8,128)(2,1)} %bitcast.33, bf16[192,128]{1,0:T(8,128)(2,1)} %get-tuple-element.27.high_ref, bf16[192,128]{1,0:T(8,128)(2,1)} %get-tuple-element.28.low_ref), custom_call_target="tpu_custom_call" | custom-call | flops 60000000 | bytes 1000000 | tf_op jit(solution)/shard_map/pallas_call | solution.py:57
  112.8 11.9 %all_to_all.15.parts_ref = bf16[8,24,512]{2,1,0:T(8,128)(2,1)S(1)} all-to-all(bf16[8,24,512]{2,1,0:T(8,128)(2,1)} %shard_map.228), channel_id=1, replica_groups=mesh['ep_0'=8,'ep_1'=4,'ep_2'=2,'tp'=4] {'ep_1','ep_2'}, dimensions={0} | all-to-all | bytes 393216 | tf_op jit(solution)/shard_map/all_to_all | solution.py:541
  (94 shorter events, 16.4 us)
Async XLA Ops:
  2.6 5.7 %collective-permute-start.10 = (bf16[64,512]{1,0:T(8,128)(2,1)S(1)}, bf16[64,512]{1,0:T(8,128)(2,1)S(1)}, u32[]{:S(2)}, u32[]{:S(2)}) collective-permute-start(bf16[64,512]{1,0:T(8,128)(2,1)S(1)} %get-tuple-element.21), channel_id=1, source_target_pairs={{0,1},{1,2},{2,3},{3,0},{4,5},{5,6},{6,7},{7,4},{8,9},{9,10},{10,1... | collective-permute-start | bytes 196616 | tf_op jit(solution)/shard_map/ppermute | solution.py:26
  4.7 5.1 %collective-permute-start.11 = (bf16[64,512]{1,0:T(8,128)(2,1)S(1)}, bf16[64,512]{1,0:T(8,128)(2,1)S(1)}, u32[]{:S(2)}, u32[]{:S(2)}) collective-permute-start(bf16[64,512]{1,0:T(8,128)(2,1)S(1)} %get-tuple-element.22), channel_id=1, source_target_pairs={{0,2},{1,3},{2,0},{3,1},{4,6},{5,7},{6,4},{7,5},{8,10},{9,11},{10,... | collective-permute-start | bytes 196616 | tf_op jit(solution)/shard_map/ppermute | solution.py:26
  7.1 3.4 %collective-permute-start.12 = (bf16[64,512]{1,0:T(8,128)(2,1)S(1)}, bf16[64,512]{1,0:T(8,128)(2,1)S(1)}, u32[]{:S(2)}, u32[]{:S(2)}) collective-permute-start(bf16[64,512]{1,0:T(8,128)(2,1)S(1)} %get-tuple-element.23), channel_id=1, source_target_pairs={{0,3},{1,0},{2,1},{3,2},{4,7},{5,4},{6,5},{7,6},{8,11},{9,8},{10,9... | collective-permute-start | bytes 196616 | tf_op jit(solution)/shard_map/ppermute | solution.py:26
  11.5 13.5 %collective-permute-start.13 = (bf16[384,512]{1,0:T(8,128)(2,1)S(1)}, bf16[384,512]{1,0:T(8,128)(2,1)S(1)}, u32[]{:S(2)}, u32[]{:S(2)}) collective-permute-start(bf16[384,512]{1,0:T(8,128)(2,1)S(1)} %constant_dynamic-update-slice_fusion.refs_8_.refs_4_), channel_id=1, source_target_pairs={{0,32},{32,64},{64,96},{96,128},{128,160},{160,192},{192,224},{224... | collective-permute-start | bytes 1179656 | tf_op jit(solution)/shard_map/ppermute | solution.py:26
  13.4 32.4 %collective-permute-start.14 = (bf16[384,512]{1,0:T(8,128)(2,1)S(1)}, bf16[384,512]{1,0:T(8,128)(2,1)}, u32[]{:S(2)}, u32[]{:S(2)}) collective-permute-start(bf16[384,512]{1,0:T(8,128)(2,1)S(1)} %constant_dynamic-update-slice_fusion.refs_8_.refs_4_), channel_id=1, source_target_pairs={{0,224},{32,0},{64,32},{96,64},{128,96},{160,128},{192,160},{224,1... | collective-permute-start | bytes 1179656 | tf_op jit(solution)/shard_map/ppermute | solution.py:26
  25.0 23.6 %collective-permute-start.15 = (bf16[384,512]{1,0:T(8,128)(2,1)S(1)}, bf16[384,512]{1,0:T(8,128)(2,1)}, u32[]{:S(2)}, u32[]{:S(2)}) collective-permute-start(bf16[384,512]{1,0:T(8,128)(2,1)S(1)} %collective-permute-done.13.refs_9_.refs_5_), channel_id=1, source_target_pairs={{0,32},{32,64},{64,96},{96,128},{128,160},{160,192},{192,224},{224... | collective-permute-start | bytes 1179656 | tf_op jit(solution)/shard_map/ppermute | solution.py:26
  25.0 51.7 %copy-start.9 = (bf16[1,512,512]{2,1,0:T(8,128)(2,1)S(1)}, bf16[1,512,512]{2,1,0:T(8,128)(2,1)}, u32[]{:S(2)}) copy-start(bf16[1,512,512]{2,1,0:T(8,128)(2,1)} %param.35) | copy-start | bytes 1572868
  25.1 51.7 %copy-start.10 = (bf16[1,512,512]{2,1,0:T(8,128)(2,1)S(1)}, bf16[1,512,512]{2,1,0:T(8,128)(2,1)}, u32[]{:S(2)}) copy-start(bf16[1,512,512]{2,1,0:T(8,128)(2,1)} %param.36) | copy-start | bytes 1572868
  32.7 59.8 %copy-start.8 = (bf16[1,512,512]{2,1,0:T(8,128)(2,1)S(1)}, bf16[1,512,512]{2,1,0:T(8,128)(2,1)}, u32[]{:S(2)}) copy-start(bf16[1,512,512]{2,1,0:T(8,128)(2,1)} %param.37) | copy-start | bytes 1572868
  32.7 4.9 %collective-permute-start.2 = (bf16[24,2048]{1,0:T(8,128)(2,1)}, bf16[24,2048]{1,0:T(8,128)(2,1)S(1)}, u32[]{:S(2)}, u32[]{:S(2)}) collective-permute-start(bf16[24,2048]{1,0:T(8,128)(2,1)} %get-tuple-element.17.refs_0_), channel_id=1, source_target_pairs={{0,3},{1,0},{2,1},{3,2},{4,7},{5,4},{6,5},{7,6},{8,11},{9,8},{10,9... | collective-permute-start | bytes 294920 | tf_op jit(solution)/shard_map/ppermute | solution.py:26
  34.6 5.3 %collective-permute-start.1 = (bf16[24,2048]{1,0:T(8,128)(2,1)}, bf16[24,2048]{1,0:T(8,128)(2,1)S(1)}, u32[]{:S(2)}, u32[]{:S(2)}) collective-permute-start(bf16[24,2048]{1,0:T(8,128)(2,1)} %get-tuple-element.17.refs_0_), channel_id=1, source_target_pairs={{0,2},{1,3},{2,0},{3,1},{4,6},{5,7},{6,4},{7,5},{8,10},{9,11},{10,... | collective-permute-start | bytes 294920 | tf_op jit(solution)/shard_map/ppermute | solution.py:26
  34.6 5.9 %collective-permute-start = (bf16[24,2048]{1,0:T(8,128)(2,1)}, bf16[24,2048]{1,0:T(8,128)(2,1)S(1)}, u32[]{:S(2)}, u32[]{:S(2)}) collective-permute-start(bf16[24,2048]{1,0:T(8,128)(2,1)} %get-tuple-element.17.refs_0_), channel_id=1, source_target_pairs={{0,1},{1,2},{2,3},{3,0},{4,5},{5,6},{6,7},{7,4},{8,9},{9,10},{10,1... | collective-permute-start | bytes 294920 | tf_op jit(solution)/shard_map/ppermute | solution.py:26
  41.6 55.2 %copy-start = (bf16[24,2176]{1,0:T(8,128)(2,1)}, bf16[24,2176]{1,0:T(8,128)(2,1)S(1)}, u32[]{:S(2)}) copy-start(bf16[24,2176]{1,0:T(8,128)(2,1)S(1)} %get-tuple-element.19.refs_0_) | copy-start | bytes 313348
  41.6 10.1 %collective-permute-start.6 = (bf16[24,2176]{1,0:T(8,128)(2,1)S(1)}, bf16[24,2176]{1,0:T(8,128)(2,1)S(1)}, u32[]{:S(2)}, u32[]{:S(2)}) collective-permute-start(bf16[24,2176]{1,0:T(8,128)(2,1)S(1)} %get-tuple-element.19.refs_0_), channel_id=1, source_target_pairs={{0,4},{4,0},{1,5},{5,1},{2,6},{6,2},{3,7},{7,3},{8,12},{12,8},{9,1... | collective-permute-start | bytes 313352 | tf_op jit(solution)/shard_map/ppermute | solution.py:26
  45.8 22.9 %collective-permute-start.16 = (bf16[384,512]{1,0:T(8,128)(2,1)}, bf16[384,512]{1,0:T(8,128)(2,1)S(1)}, u32[]{:S(2)}, u32[]{:S(2)}) collective-permute-start(bf16[384,512]{1,0:T(8,128)(2,1)} %collective-permute-done.14.refs_10_.refs_6_), channel_id=1, source_target_pairs={{0,224},{32,0},{64,32},{96,64},{128,96},{160,128},{192,160},{224,1... | collective-permute-start | bytes 1179656 | tf_op jit(solution)/shard_map/ppermute | solution.py:26
  48.6 22.9 %collective-permute-start.17 = (bf16[384,512]{1,0:T(8,128)(2,1)}, bf16[384,512]{1,0:T(8,128)(2,1)S(1)}, u32[]{:S(2)}, u32[]{:S(2)}) collective-permute-start(bf16[384,512]{1,0:T(8,128)(2,1)} %collective-permute-done.15.refs_11_.refs_7_), channel_id=1, source_target_pairs={{0,32},{32,64},{64,96},{96,128},{128,160},{160,192},{192,224},{224... | collective-permute-start | bytes 1179656 | tf_op jit(solution)/shard_map/ppermute | solution.py:26
  48.7 6.7 %collective-permute-start.5 = (bf16[24,2176]{1,0:T(8,128)(2,1)S(1)}, bf16[24,2176]{1,0:T(8,128)(2,1)S(1)}, u32[]{:S(2)}, u32[]{:S(2)}) collective-permute-start(bf16[24,2176]{1,0:T(8,128)(2,1)S(1)} %get-tuple-element.19.refs_0_), channel_id=1, source_target_pairs={{0,24},{8,0},{16,8},{24,16},{1,25},{9,1},{17,9},{25,17},{2,26},{10... | collective-permute-start | bytes 313352 | tf_op jit(solution)/shard_map/ppermute | solution.py:26
  51.4 5.4 %collective-permute-start.4 = (bf16[24,2176]{1,0:T(8,128)(2,1)S(1)}, bf16[24,2176]{1,0:T(8,128)(2,1)S(1)}, u32[]{:S(2)}, u32[]{:S(2)}) collective-permute-start(bf16[24,2176]{1,0:T(8,128)(2,1)S(1)} %get-tuple-element.19.refs_0_), channel_id=1, source_target_pairs={{0,16},{8,24},{16,0},{24,8},{1,17},{9,25},{17,1},{25,9},{2,18},{10... | collective-permute-start | bytes 313352 | tf_op jit(solution)/shard_map/ppermute | solution.py:26
  51.7 8.2 %collective-permute-start.3 = (bf16[24,2176]{1,0:T(8,128)(2,1)S(1)}, bf16[24,2176]{1,0:T(8,128)(2,1)S(1)}, u32[]{:S(2)}, u32[]{:S(2)}) collective-permute-start(bf16[24,2176]{1,0:T(8,128)(2,1)S(1)} %get-tuple-element.19.refs_0_), channel_id=1, source_target_pairs={{0,8},{8,16},{16,24},{24,0},{1,9},{9,17},{17,25},{25,1},{2,10},{10... | collective-permute-start | bytes 313352 | tf_op jit(solution)/shard_map/ppermute | solution.py:26
  55.4 5.1 %collective-permute-start.9 = (bf16[24,2176]{1,0:T(8,128)(2,1)S(1)}, bf16[24,2176]{1,0:T(8,128)(2,1)S(1)}, u32[]{:S(2)}, u32[]{:S(2)}) collective-permute-start(bf16[24,2176]{1,0:T(8,128)(2,1)S(1)} %collective-permute-done.5.refs_3_), channel_id=1, source_target_pairs={{0,4},{4,0},{1,5},{5,1},{2,6},{6,2},{3,7},{7,3},{8,12},{12,8},{9,1... | collective-permute-start | bytes 313352 | tf_op jit(solution)/shard_map/ppermute | solution.py:26
  56.8 3.7 %collective-permute-start.8 = (bf16[24,2176]{1,0:T(8,128)(2,1)S(1)}, bf16[24,2176]{1,0:T(8,128)(2,1)S(1)}, u32[]{:S(2)}, u32[]{:S(2)}) collective-permute-start(bf16[24,2176]{1,0:T(8,128)(2,1)S(1)} %collective-permute-done.4.refs_2_), channel_id=1, source_target_pairs={{0,4},{4,0},{1,5},{5,1},{2,6},{6,2},{3,7},{7,3},{8,12},{12,8},{9,1... | collective-permute-start | bytes 313352 | tf_op jit(solution)/shard_map/ppermute | solution.py:26
  59.9 1.5 %collective-permute-start.7 = (bf16[24,2176]{1,0:T(8,128)(2,1)S(1)}, bf16[24,2176]{1,0:T(8,128)(2,1)S(1)}, u32[]{:S(2)}, u32[]{:S(2)}) collective-permute-start(bf16[24,2176]{1,0:T(8,128)(2,1)S(1)} %collective-permute-done.3.refs_1_), channel_id=1, source_target_pairs={{0,4},{4,0},{1,5},{5,1},{2,6},{6,2},{3,7},{7,3},{8,12},{12,8},{9,1... | collective-permute-start | bytes 313352 | tf_op jit(solution)/shard_map/ppermute | solution.py:26
  63.2 13.5 %all-to-all-start = ((bf16[8,16,512]{2,1,0:T(8,128)(2,1)}), bf16[8,16,512]{2,1,0:T(8,128)(2,1)S(1)}, u32[]{:S(2)}, u32[]{:S(2)}) async-start(bf16[8,16,512]{2,1,0:T(8,128)(2,1)} %bitcast.13), calls=%async_computation | async-start | bytes 262144 | tf_op jit(solution)/shard_map/all_to_all | solution.py:480
  68.8 28.1 %collective-permute-start.18 = (bf16[384,512]{1,0:T(8,128)(2,1)S(1)}, bf16[384,512]{1,0:T(8,128)(2,1)}, u32[]{:S(2)}, u32[]{:S(2)}) collective-permute-start(bf16[384,512]{1,0:T(8,128)(2,1)S(1)} %collective-permute-done.16.refs_12_.refs_8_), channel_id=1, source_target_pairs={{0,224},{32,0},{64,32},{96,64},{128,96},{160,128},{192,160},{224,1... | collective-permute-start | bytes 1179656 | tf_op jit(solution)/shard_map/ppermute | solution.py:26
  71.5 25.3 %collective-permute-start.19 = (bf16[384,512]{1,0:T(8,128)(2,1)S(1)}, bf16[384,512]{1,0:T(8,128)(2,1)}, u32[]{:S(2)}, u32[]{:S(2)}) collective-permute-start(bf16[384,512]{1,0:T(8,128)(2,1)S(1)} %collective-permute-done.17.refs_13_.refs_9_), channel_id=1, source_target_pairs={{0,32},{32,64},{64,96},{96,128},{128,160},{160,192},{192,224},{224... | collective-permute-start | bytes 1179656 | tf_op jit(solution)/shard_map/ppermute | solution.py:26
  77.0 5.7 %collective-permute-start.25 = (bf16[128,1024]{1,0:T(8,128)(2,1)S(1)}, bf16[128,1024]{1,0:T(8,128)(2,1)S(1)}, u32[]{:S(2)}, u32[]{:S(2)}) collective-permute-start(bf16[128,1024]{1,0:T(8,128)(2,1)S(1)} %shard_map.226.refs_0_), channel_id=1, source_target_pairs={{0,3},{1,0},{2,1},{3,2},{4,7},{5,4},{6,5},{7,6},{8,11},{9,8},{10,9... | collective-permute-start | bytes 786440 | tf_op jit(solution)/shard_map/ppermute | solution.py:26
  77.7 6.8 %collective-permute-start.24 = (bf16[128,1024]{1,0:T(8,128)(2,1)S(1)}, bf16[128,1024]{1,0:T(8,128)(2,1)S(1)}, u32[]{:S(2)}, u32[]{:S(2)}) collective-permute-start(bf16[128,1024]{1,0:T(8,128)(2,1)S(1)} %shard_map.226.refs_0_), channel_id=1, source_target_pairs={{0,2},{1,3},{2,0},{3,1},{4,6},{5,7},{6,4},{7,5},{8,10},{9,11},{10,... | collective-permute-start | bytes 786440 | tf_op jit(solution)/shard_map/ppermute | solution.py:26
  78.2 14.3 %collective-permute-start.23 = (bf16[128,1024]{1,0:T(8,128)(2,1)S(1)}, bf16[128,1024]{1,0:T(8,128)(2,1)S(1)}, u32[]{:S(2)}, u32[]{:S(2)}) collective-permute-start(bf16[128,1024]{1,0:T(8,128)(2,1)S(1)} %shard_map.226.refs_0_), channel_id=1, source_target_pairs={{0,1},{1,2},{2,3},{3,0},{4,5},{5,6},{6,7},{7,4},{8,9},{9,10},{10,1... | collective-permute-start | bytes 786440 | tf_op jit(solution)/shard_map/ppermute | solution.py:26
  93.4 16.7 %all-to-all-start.1 = ((bf16[8,16,512]{2,1,0:T(8,128)(2,1)}), bf16[8,16,512]{2,1,0:T(8,128)(2,1)S(1)}, u32[]{:S(2)}, u32[]{:S(2)}) async-start(bf16[8,16,512]{2,1,0:T(8,128)(2,1)} %bitcast.18), calls=%async_computation.1 | async-start | bytes 262144 | tf_op jit(solution)/shard_map/all_to_all | solution.py:480
  100.3 4.2 %collective-permute-start.22 = (bf16[192,256]{1,0:T(8,128)(2,1)}, bf16[192,256]{1,0:T(8,128)(2,1)S(1)}, u32[]{:S(2)}, u32[]{:S(2)}) collective-permute-start(bf16[192,256]{1,0:T(8,128)(2,1)} %shard_map.222.refs_0_), channel_id=1, source_target_pairs={{0,3},{1,0},{2,1},{3,2},{4,7},{5,4},{6,5},{7,6},{8,11},{9,8},{10,9... | collective-permute-start | bytes 294920 | tf_op jit(solution)/shard_map/ppermute | solution.py:26
  100.3 5.6 %collective-permute-start.21 = (bf16[192,256]{1,0:T(8,128)(2,1)}, bf16[192,256]{1,0:T(8,128)(2,1)S(1)}, u32[]{:S(2)}, u32[]{:S(2)}) collective-permute-start(bf16[192,256]{1,0:T(8,128)(2,1)} %shard_map.222.refs_0_), channel_id=1, source_target_pairs={{0,2},{1,3},{2,0},{3,1},{4,6},{5,7},{6,4},{7,5},{8,10},{9,11},{10,... | collective-permute-start | bytes 294920 | tf_op jit(solution)/shard_map/ppermute | solution.py:26
  100.4 6.4 %collective-permute-start.20 = (bf16[192,256]{1,0:T(8,128)(2,1)}, bf16[192,256]{1,0:T(8,128)(2,1)S(1)}, u32[]{:S(2)}, u32[]{:S(2)}) collective-permute-start(bf16[192,256]{1,0:T(8,128)(2,1)} %shard_map.222.refs_0_), channel_id=1, source_target_pairs={{0,1},{1,2},{2,3},{3,0},{4,5},{5,6},{6,7},{7,4},{8,9},{9,10},{10,1... | collective-permute-start | bytes 294920 | tf_op jit(solution)/shard_map/ppermute | solution.py:26
  (22 other events, 403.7 us)

commit v3 on v2

--- a/solution.py
+++ b/solution.py
@@ -337,36 +337,53 @@
     )
 
 
-def expert_in_kernel(rows_ref, gate_ref, up_ref, out_ref):
-    units = gate_ref.shape[1]
+def expert_in_kernel(rows_ref, gate_ref, up_ref, *outs):
+    units = outs[0].shape[1] // 2
     rows = rows_ref[...]
-    out_ref[:, :units] = dot(rows, gate_ref[...]).astype(BF16)
-    out_ref[:, units:] = dot(rows, up_ref[...]).astype(BF16)
+    for k, out in enumerate(outs):
+        at = span(behind(TP, -k), units)
+        both = jnp.concatenate([gate_ref[:, at], up_ref[:, at]], axis=1)
+        out[...] = dot(rows, both).astype(BF16)
 
 
 def expert_in(rows, gate, up):
-    return call(
-        expert_in_kernel,
-        jax.ShapeDtypeStruct((rows.shape[0], 2 * gate.shape[1]), BF16),
-        140_000_000, 1_400_000, rows, gate, up,
-    )
-
-
-def expert_out_kernel(*refs):
-    parts, (down_ref, out_ref) = refs[:-2], refs[-2:]
-    units = down_ref.shape[0]
+    tps = lax.axis_size(TP)
+    one = jax.ShapeDtypeStruct((rows.shape[0], 2 * gate.shape[1] // tps), BF16)
+    return call(expert_in_kernel, (one,) * tps, 140_000_000, 1_400_000, rows, gate, up)
+
+
+def expert_act_kernel(*refs):
+    parts, out_ref = refs[:-1], refs[-1]
+    units = out_ref.shape[1]
     act = parts[0][...].astype(F32)
     for part in parts[1:]:
         act = act + part[...].astype(F32)
-    hidden = (silu(act[:, :units]) * act[:, units:]).astype(BF16)
-    out_ref[...] = dot(hidden, down_ref[...]).astype(BF16)
-
-
-def expert_out(parts, down):
+    out_ref[...] = (silu(act[:, :units]) * act[:, units:]).astype(BF16)
+
+
+def expert_act(parts):
+    rows, width = parts[0].shape
+    return call(
+        expert_act_kernel,
+        jax.ShapeDtypeStruct((rows, width // 2), BF16),
+        1_000_000, 300_000, *parts,
+    )
+
+
+def expert_out_kernel(*refs):
+    hiddens, (down_ref, out_ref) = refs[:-2], refs[-2:]
+    units = hiddens[0].shape[1]
+    total = 0.0
+    for k, hidden in enumerate(hiddens):
+        total = total + dot(hidden[...], down_ref[span(behind(TP, k), units), :])
+    out_ref[...] = total.astype(BF16)
+
+
+def expert_out(hiddens, down):
     return call(
         expert_out_kernel,
-        jax.ShapeDtypeStruct((parts[0].shape[0], down.shape[1]), BF16),
-        70_000_000, 1_800_000, *parts, down,
+        jax.ShapeDtypeStruct((hiddens[0].shape[0], down.shape[1]), BF16),
+        70_000_000, 800_000, *hiddens, down,
     )
 
 
@@ -403,9 +420,9 @@
 
 
 def dense_out_kernel(*refs):
-    gate_ref, out_ref = refs[-2:]
     planes, tps = lax.axis_size(Z), lax.axis_size(TP)
     hiddens, blocks = refs[:tps], refs[tps : tps + planes]
+    gate_ref, rows_ref, high_ref, low_ref, home_ref, away_ref = refs[tps + planes :]
     units = blocks[0].shape[0] // tps
     total = 0.0
     for k in range(tps):
@@ -413,53 +430,59 @@
         total = total + dot(
             hiddens[k][...], jnp.concatenate([b[at, :] for b in blocks], axis=0)
         )
-    out_ref[...] = total * gate_ref[:, 0:1]
-
-
-def dense_out(hiddens, blocks, gate):
-    count = hiddens[0].shape[0]
+    rows = rows_ref[...]
+    total = total * gate_ref[:, 0:1] + (dot(high_ref[...], rows) + dot(low_ref[...], rows))
+    half = home_ref.shape[0]
+    home_ref[...] = total[:half]
+    away_ref[...] = total[half:].astype(BF16)
+
+
+def dense_out(hiddens, blocks, gate, returned, high, low):
+    half = hiddens[0].shape[0] // 2
     rows, width = blocks[0].shape
     kept = lambda shape: pl.BlockSpec(shape, lambda i: (0, 0))
     lower = pl.BlockSpec((rows // 3, width), lambda i: (2, 0))
+    others = (gate, returned, high, low)
     return call(
         dense_out_kernel,
-        jax.ShapeDtypeStruct((count, width), F32),
-        400_000_000, 2_000_000, *hiddens, *blocks, gate, near=False,
+        (
+            jax.ShapeDtypeStruct((half, width), F32),
+            jax.ShapeDtypeStruct((half, width), BF16),
+        ),
+        400_000_000, 2_000_000, *hiddens, *blocks, *others, near=False,
         grid=(1,),
-        in_specs=[kept(x.shape) for x in hiddens] + [lower] * len(blocks) + [kept(gate.shape)],
-        out_specs=kept((count, width)),
-    )
-
-
-def gather_kernel(dense_ref, rows_ref, high_ref, low_ref, out_ref):
-    rows = rows_ref[...]
-    total = dense_ref[...] + (dot(high_ref[...], rows) + dot(low_ref[...], rows))
-    seq = out_ref.shape[1]
-    ys, c = lax.axis_size(Y), lax.axis_index(CORE)
-    for other in range(2):
-        core = c if other == 0 else 1 - c
-        for j in range(ys):
-            at = (other * ys + j) * seq
-            out_ref[behind(Y, j) * 2 + core] = total[at : at + seq].astype(BF16)
-
-
-def gather_rows(dense, rows, high, low, seq):
-    return call(
-        gather_kernel,
-        jax.ShapeDtypeStruct((dense.shape[0] // seq, seq, dense.shape[1]), BF16),
-        60_000_000, 1_000_000, dense, rows, high, low, near=False,
-    )
-
-
-def finish_kernel(resid_ref, parts_ref, out_ref):
-    total = resid_ref[...]
-    for i in range(parts_ref.shape[0]):
-        total = total + parts_ref[i].astype(F32)
+        in_specs=[kept(x.shape) for x in hiddens]
+        + [lower] * len(blocks)
+        + [kept(x.shape) for x in others],
+        out_specs=(kept((half, width)), kept((half, width))),
+    )
+
+
+def fold_kernel(home_ref, come_ref, resid_ref, *outs):
+    seq = resid_ref.shape[0]
+    total = home_ref[...] + come_ref[...].astype(F32)
+    outs[0][...] = resid_ref[...] + total[:seq]
+    for j in range(1, len(outs)):
+        outs[j][...] = total[j * seq : (j + 1) * seq].astype(BF16)
+
+
+def fold(home, come, resid):
+    keep = jax.ShapeDtypeStruct(resid.shape, F32)
+    sent = jax.ShapeDtypeStruct(resid.shape, BF16)
+    outs = (keep,) + (sent,) * (lax.axis_size(Y) - 1)
+    return call(fold_kernel, outs, 100_000, 500_000, home, come, resid)
+
+
+def finish_kernel(keep_ref, *refs):
+    parts, out_ref = refs[:-1], refs[-1]
+    total = keep_ref[...]
+    for part in parts:
+        total = total + part[...].astype(F32)
     out_ref[...] = total.astype(BF16)
 
 
-def finish(resid, parts):
-    return call(finish_kernel, jax.ShapeDtypeStruct(resid.shape, BF16), 0, 400_000, resid, parts)
+def finish(keep, parts):
+    return call(finish_kernel, jax.ShapeDtypeStruct(keep.shape, BF16), 0, 200_000, keep, *parts)
 
 
 def along_z(own):
@@ -530,16 +553,19 @@
     rows, hot = select(group, width_part)
     rows = over_z(rows)
     pre = expert_in(rows, e_gate[0], e_up[0])
-    pres = all_shifts(pre, TP)
-    result = expert_out(pres, e_down[0])
+    pres = [pre[0]] + [shifted(pre[k], TP, k) for k in range(1, len(pre))]
+    act = expert_act(pres)
+    acts = all_shifts(act, TP)
+    result = expert_out(acts, e_down[0])
     returned = over_z(result)
     high, low, gate = share_weights(hot, w_group, w_fine, w_mix, group)
     hidden = dense_in(group, blocks)
     hiddens = all_shifts(hidden, TP)
-    dense = dense_out(hiddens, blocks, gate)
-    parts = gather_rows(dense, returned, high, low, seq_count)
-    parts = lax.all_to_all(parts, (Y, CORE), split_axis=0, concat_axis=0, tiled=True)
-    mixed = finish(resid, parts)
+    home, away = dense_out(hiddens, blocks, gate, returned, high, low)
+    come = shifted(away, CORE, 1)
+    folded = fold(home, come, resid)
+    parts = [shifted(folded[j], Y, -j) for j in range(1, len(folded))]
+    mixed = finish(folded[0], parts)
     return (
         mixed,
         new_keys.reshape(seq_count, kv_local, head_dim),

time: 126 us -> 120 us (0.952)
  starting transfers between devices: 44.6 us -> 57 us
  blocking collectives: 11.9 us -> 0 us
  waiting for transfers between devices: 40.5 us -> 36 us
  Pallas kernels: 21.6 us -> 19.7 us
    ppermute x26 -> x33, starting transfers between devices: 35.7 us -> 47.9 us  [shifted(): return lax.ppermute(x, axis, [(i, (i + step) % size) for i in range(size)])]
    all_to_all x1 -> x0, blocking collectives: 11.9 us -> none  [shards(): lax.all_to_all(parts, (Y, CORE), split_axis=0, concat_axis=0, tiled=True)]
    ppermute x26 -> x33, waiting for transfers between devices: 35.3 us -> 30.8 us  [shifted(): return lax.ppermute(x, axis, [(i, (i + step) % size) for i in range(size)])]
    pallas_call x10 -> x11, Pallas kernels: 14 us -> 12.1 us  [call(): pl.pallas_call(kernel, out_shape=out, cost_estimate=pl.CostEstimate(flops...]
    unnamed x57 -> x59, local copies, waits for them, and re-layouts: 4.8 us -> 5.06 us
  transfers between devices with their start and end apart: 28 -> 35, of which waited for: 15 -> 21; matrix products, arithmetic and copies ran while one was open for 0% -> 0% of each run, Pallas kernels for 15% -> 14%
where the time goes in v3:
time: 120 us
  starting transfers between devices  57 us (48%)
  waiting for transfers between devices  36 us (30%)
  Pallas kernels  19.7 us (16%)
  local copies, waits for them, and re-layouts  5.98 us (5%)
    ppermute x33, starting transfers between devices, shifted(): return lax.ppermute(x, axis, [(i, (i + step) % size) for i in range(size)])  47.9 us
    ppermute x33, waiting for transfers between devices, shifted(): return lax.ppermute(x, axis, [(i, (i + step) % size) for i in range(size)])  30.8 us
    pallas_call x11, Pallas kernels, call(): pl.pallas_call(kernel, out_shape=out, cost_estimate=pl.CostEstimate(flops...  12.1 us
    all_to_all x2, starting transfers between devices, over_z(): lax.all_to_all(shaped, Z, split_axis=0, concat_axis=0, tiled=True)  9.07 us
    pallas_call x1, Pallas kernels, attention(): pl.pallas_call(attention_kernel, out_shape=(jax.ShapeDtypeStruct((seq, wi...  7.58 us
    all_to_all x2, waiting for transfers between devices, over_z(): lax.all_to_all(shaped, Z, split_axis=0, concat_axis=0, tiled=True)  5.19 us
    unnamed x59, local copies, waits for them, and re-layouts  5.06 us
  transfers between devices with their start and end apart: 35, of which 21 were waited for; matrix products, arithmetic and copies ran while one was open for 0% of the time, Pallas kernels for 14%

profile of v3, /device:TPU:1, one launch (start us, length us, event | category | flops | bytes accessed | tf_op | source)
XLA Modules:
  0.0 119.6 jit_solution(15614523219581056441)
XLA Ops:
  2.6 2.1 %collective-permute-start.10 = (bf16[64,512]{1,0:T(8,128)(2,1)S(1)}, bf16[64,512]{1,0:T(8,128)(2,1)S(1)}, u32[]{:S(2)}, u32[]{:S(2)}) collective-permute-start(bf16[64,512]{1,0:T(8,128)(2,1)S(1)} %get-tuple-element.30), channel_id=1, source_target_pairs={{0,1},{1,2},{2,3},{3,0},{4,5},{5,6},{6,7},{7,4},{8,9},{9,10},{10,1... | collective-permute-start | bytes 196616 | tf_op jit(solution)/shard_map/ppermute | solution.py:26
  4.7 2.5 %collective-permute-start.11 = (bf16[64,512]{1,0:T(8,128)(2,1)S(1)}, bf16[64,512]{1,0:T(8,128)(2,1)S(1)}, u32[]{:S(2)}, u32[]{:S(2)}) collective-permute-start(bf16[64,512]{1,0:T(8,128)(2,1)S(1)} %get-tuple-element.31), channel_id=1, source_target_pairs={{0,2},{1,3},{2,0},{3,1},{4,6},{5,7},{6,4},{7,5},{8,10},{9,11},{10,... | collective-permute-start | bytes 196616 | tf_op jit(solution)/shard_map/ppermute | solution.py:26
  7.1 1.2 collective-permute-start.12
  8.3 1.4 %collective-permute-done.11 = bf16[64,512]{1,0:T(8,128)(2,1)S(1)} collective-permute-done((bf16[64,512]{1,0:T(8,128)(2,1)S(1)}, bf16[64,512]{1,0:T(8,128)(2,1)S(1)}, u32[]{:S(2)}, u32[]{:S(2)}) %collective-permute-start.11) | collective-permute-done | bytes 65568 | tf_op jit(solution)/shard_map/ppermute | solution.py:26
  11.5 2.0 %collective-permute-start.13 = (bf16[384,512]{1,0:T(8,128)(2,1)S(1)}, bf16[384,512]{1,0:T(8,128)(2,1)S(1)}, u32[]{:S(2)}, u32[]{:S(2)}) collective-permute-start(bf16[384,512]{1,0:T(8,128)(2,1)S(1)} %constant_dynamic-update-slice_fusion.refs_8_.refs_4_), channel_id=1, source_target_pairs={{0,32},{32,64},{64,96},{96,128},{128,160},{160,192},{192,224},{224... | collective-permute-start | bytes 1179656 | tf_op jit(solution)/shard_map/ppermute | solution.py:26
  13.4 4.0 %collective-permute-start.14 = (bf16[384,512]{1,0:T(8,128)(2,1)S(1)}, bf16[384,512]{1,0:T(8,128)(2,1)}, u32[]{:S(2)}, u32[]{:S(2)}) collective-permute-start(bf16[384,512]{1,0:T(8,128)(2,1)S(1)} %constant_dynamic-update-slice_fusion.refs_8_.refs_4_), channel_id=1, source_target_pairs={{0,224},{32,0},{64,32},{96,64},{128,96},{160,128},{192,160},{224,1... | collective-permute-start | bytes 1179656 | tf_op jit(solution)/shard_map/ppermute | solution.py:26
  17.5 7.6 %collective-permute-done.13.refs_9_.refs_5_ = bf16[384,512]{1,0:T(8,128)(2,1)S(1)} collective-permute-done((bf16[384,512]{1,0:T(8,128)(2,1)S(1)}, bf16[384,512]{1,0:T(8,128)(2,1)S(1)}, u32[]{:S(2)}, u32[]{:S(2)}) %collective-permute-start.13) | collective-permute-done | bytes 393248 | tf_op jit(solution)/shard_map/ppermute | solution.py:26
  25.1 7.6 %attention.1 = (bf16[24,2048]{1,0:T(8,128)(2,1)}, bf16[24,64]{1,0:T(8,128)(2,1)}, bf16[24,64]{1,0:T(8,128)(2,1)}) custom-call(s32[24]{0:T(128)} %lengths_ref.1, bf16[24,2048]{1,0:T(8,128)(2,1)} %tokens_ref.3, f32[1,2048]{1,0:T(1,128)} %bitcast.38, f32[8]{0:T(128)} %bias_ref.1, bf16[64,2048]{1,0:T(8,128)(2,1)} %bitcast.34, bf16[64,2048]{1,0:T(8,128)(2,1)} %bitcast.35, ...), custom_call_target="tpu_custom_call" | custom-call | flops 400000000 | bytes 11000000 | tf_op jit(solution)/shard_map/attention/pallas_call | solution.py:178
  32.7 1.9 %collective-permute-start.2 = (bf16[24,2048]{1,0:T(8,128)(2,1)}, bf16[24,2048]{1,0:T(8,128)(2,1)S(1)}, u32[]{:S(2)}, u32[]{:S(2)}) collective-permute-start(bf16[24,2048]{1,0:T(8,128)(2,1)} %get-tuple-element.27.refs_0_), channel_id=1, source_target_pairs={{0,3},{1,0},{2,1},{3,2},{4,7},{5,4},{6,5},{7,6},{8,11},{9,8},{10,9... | collective-permute-start | bytes 294920 | tf_op jit(solution)/shard_map/ppermute | solution.py:26
  35.3 2.5 %collective-permute-start.16 = (bf16[384,512]{1,0:T(8,128)(2,1)}, bf16[384,512]{1,0:T(8,128)(2,1)S(1)}, u32[]{:S(2)}, u32[]{:S(2)}) collective-permute-start(bf16[384,512]{1,0:T(8,128)(2,1)} %collective-permute-done.14.refs_10_.refs_6_), channel_id=1, source_target_pairs={{0,224},{32,0},{64,32},{96,64},{128,96},{160,128},{192,160},{224,1... | collective-permute-start | bytes 1179656 | tf_op jit(solution)/shard_map/ppermute | solution.py:26
  37.9 2.0 %collective-permute-done.1.refs_2_ = bf16[24,2048]{1,0:T(8,128)(2,1)S(1)} collective-permute-done((bf16[24,2048]{1,0:T(8,128)(2,1)}, bf16[24,2048]{1,0:T(8,128)(2,1)S(1)}, u32[]{:S(2)}, u32[]{:S(2)}) %collective-permute-start.1) | collective-permute-done | bytes 98336 | tf_op jit(solution)/shard_map/ppermute | solution.py:26
  41.6 4.2 %collective-permute-start.6 = (bf16[24,2176]{1,0:T(8,128)(2,1)S(1)}, bf16[24,2176]{1,0:T(8,128)(2,1)S(1)}, u32[]{:S(2)}, u32[]{:S(2)}) collective-permute-start(bf16[24,2176]{1,0:T(8,128)(2,1)S(1)} %get-tuple-element.28.refs_0_), channel_id=1, source_target_pairs={{0,4},{4,0},{1,5},{5,1},{2,6},{6,2},{3,7},{7,3},{8,12},{12,8},{9,1... | collective-permute-start | bytes 313352 | tf_op jit(solution)/shard_map/ppermute | solution.py:26
  45.8 2.7 %collective-permute-start.5 = (bf16[24,2176]{1,0:T(8,128)(2,1)S(1)}, bf16[24,2176]{1,0:T(8,128)(2,1)S(1)}, u32[]{:S(2)}, u32[]{:S(2)}) collective-permute-start(bf16[24,2176]{1,0:T(8,128)(2,1)S(1)} %get-tuple-element.28.refs_0_), channel_id=1, source_target_pairs={{0,24},{8,0},{16,8},{24,16},{1,25},{9,1},{17,9},{25,17},{2,26},{10... | collective-permute-start | bytes 313352 | tf_op jit(solution)/shard_map/ppermute | solution.py:26
  49.6 3.1 %collective-permute-done.5.refs_3_ = bf16[24,2176]{1,0:T(8,128)(2,1)S(1)} collective-permute-done((bf16[24,2176]{1,0:T(8,128)(2,1)S(1)}, bf16[24,2176]{1,0:T(8,128)(2,1)S(1)}, u32[]{:S(2)}, u32[]{:S(2)}) %collective-permute-start.5) | collective-permute-done | bytes 104480 | tf_op jit(solution)/shard_map/ppermute | solution.py:26
  52.7 1.3 %collective-permute-start.9 = (bf16[24,2176]{1,0:T(8,128)(2,1)S(1)}, bf16[24,2176]{1,0:T(8,128)(2,1)S(1)}, u32[]{:S(2)}, u32[]{:S(2)}) collective-permute-start(bf16[24,2176]{1,0:T(8,128)(2,1)S(1)} %collective-permute-done.5.refs_3_), channel_id=1, source_target_pairs={{0,4},{4,0},{1,5},{5,1},{2,6},{6,2},{3,7},{7,3},{8,12},{12,8},{9,1... | collective-permute-start | bytes 313352 | tf_op jit(solution)/shard_map/ppermute | solution.py:26
  54.0 2.4 %collective-permute-start.8 = (bf16[24,2176]{1,0:T(8,128)(2,1)S(1)}, bf16[24,2176]{1,0:T(8,128)(2,1)S(1)}, u32[]{:S(2)}, u32[]{:S(2)}) collective-permute-start(bf16[24,2176]{1,0:T(8,128)(2,1)S(1)} %collective-permute-done.4.refs_2_), channel_id=1, source_target_pairs={{0,4},{4,0},{1,5},{5,1},{2,6},{6,2},{3,7},{7,3},{8,12},{12,8},{9,1... | collective-permute-start | bytes 313352 | tf_op jit(solution)/shard_map/ppermute | solution.py:26
  60.4 5.7 %all-to-all-start = ((bf16[8,16,512]{2,1,0:T(8,128)(2,1)}), bf16[8,16,512]{2,1,0:T(8,128)(2,1)S(1)}, u32[]{:S(2)}, u32[]{:S(2)}) async-start(bf16[8,16,512]{2,1,0:T(8,128)(2,1)} %bitcast.13), calls=%async_computation | async-start | bytes 262144 | tf_op jit(solution)/shard_map/all_to_all | solution.py:503
  66.1 2.7 %collective-permute-start.18 = (bf16[384,512]{1,0:T(8,128)(2,1)S(1)}, bf16[384,512]{1,0:T(8,128)(2,1)}, u32[]{:S(2)}, u32[]{:S(2)}) collective-permute-start(bf16[384,512]{1,0:T(8,128)(2,1)S(1)} %collective-permute-done.16.refs_12_.refs_8_), channel_id=1, source_target_pairs={{0,224},{32,0},{64,32},{96,64},{128,96},{160,128},{192,160},{224,1... | collective-permute-start | bytes 1179656 | tf_op jit(solution)/shard_map/ppermute | solution.py:26
  68.9 5.2 %all-to-all-done = bf16[8,16,512]{2,1,0:T(8,128)(2,1)S(1)} async-done(((bf16[8,16,512]{2,1,0:T(8,128)(2,1)}), bf16[8,16,512]{2,1,0:T(8,128)(2,1)S(1)}, u32[]{:S(2)}, u32[]{:S(2)}) %all-to-all-start) | async-done | bytes 131104 | tf_op jit(solution)/shard_map/all_to_all | solution.py:503
  74.5 1.8 %collective-permute-start.24 = (bf16[128,256]{1,0:T(8,128)(2,1)S(1)}, bf16[128,256]{1,0:T(8,128)(2,1)S(1)}, u32[]{:S(2)}, u32[]{:S(2)}) collective-permute-start(bf16[128,256]{1,0:T(8,128)(2,1)S(1)} %get-tuple-element.38), channel_id=1, source_target_pairs={{0,2},{1,3},{2,0},{3,1},{4,6},{5,7},{6,4},{7,5},{8,10},{9,11},{10,... | collective-permute-start | bytes 196616 | tf_op jit(solution)/shard_map/ppermute | solution.py:26
  76.2 1.3 %collective-permute-start.25 = (bf16[128,256]{1,0:T(8,128)(2,1)S(1)}, bf16[128,256]{1,0:T(8,128)(2,1)S(1)}, u32[]{:S(2)}, u32[]{:S(2)}) collective-permute-start(bf16[128,256]{1,0:T(8,128)(2,1)S(1)} %get-tuple-element.39), channel_id=1, source_target_pairs={{0,3},{1,0},{2,1},{3,2},{4,7},{5,4},{6,5},{7,6},{8,11},{9,8},{10,9... | collective-permute-start | bytes 196616 | tf_op jit(solution)/shard_map/ppermute | solution.py:26
  77.5 2.4 %collective-permute-done.23.refs_1_ = bf16[128,256]{1,0:T(8,128)(2,1)S(1)} collective-permute-done((bf16[128,256]{1,0:T(8,128)(2,1)S(1)}, bf16[128,256]{1,0:T(8,128)(2,1)S(1)}, u32[]{:S(2)}, u32[]{:S(2)}) %collective-permute-start.23) | collective-permute-done | bytes 65568 | tf_op jit(solution)/shard_map/ppermute | solution.py:26
  80.5 2.3 %collective-permute-start.28 = (bf16[128,128]{1,0:T(8,128)(2,1)S(1)}, bf16[128,128]{1,0:T(8,128)(2,1)S(1)}, u32[]{:S(2)}, u32[]{:S(2)}) collective-permute-start(bf16[128,128]{1,0:T(8,128)(2,1)S(1)} %shard_map.226.refs_0_), channel_id=1, source_target_pairs={{0,3},{1,0},{2,1},{3,2},{4,7},{5,4},{6,5},{7,6},{8,11},{9,8},{10,9... | collective-permute-start | bytes 98312 | tf_op jit(solution)/shard_map/ppermute | solution.py:26
  84.0 3.2 %collective-permute-done.27.refs_2_ = bf16[128,128]{1,0:T(8,128)(2,1)S(1)} collective-permute-done((bf16[128,128]{1,0:T(8,128)(2,1)S(1)}, bf16[128,128]{1,0:T(8,128)(2,1)S(1)}, u32[]{:S(2)}, u32[]{:S(2)}) %collective-permute-start.27) | collective-permute-done | bytes 32800 | tf_op jit(solution)/shard_map/ppermute | solution.py:26
  88.4 3.4 %all-to-all-start.1 = ((bf16[8,16,512]{2,1,0:T(8,128)(2,1)}), bf16[8,16,512]{2,1,0:T(8,128)(2,1)S(1)}, u32[]{:S(2)}, u32[]{:S(2)}) async-start(bf16[8,16,512]{2,1,0:T(8,128)(2,1)} %bitcast.18), calls=%async_computation.1 | async-start | bytes 262144 | tf_op jit(solution)/shard_map/all_to_all | solution.py:503
  91.9 3.3 %shard_map.222.refs_0_ = bf16[192,256]{1,0:T(8,128)(2,1)} custom-call(bf16[24,2176]{1,0:T(8,128)(2,1)} %copy-done, bf16[24,2176]{1,0:T(8,128)(2,1)} %copy-done.4, bf16[24,2176]{1,0:T(8,128)(2,1)} %copy-done.3, bf16[24,2176]{1,0:T(8,128)(2,1)} %copy-done.2, bf16[24,2176]{1,0:T(8,128)(2,1)} %copy-done.1, bf16[24,2176]{1,0:T(8,128)(2,1)} %copy-done.7, ...), custom_call_target="tpu_custom_call" | custom-call | flops 400000000 | bytes 3000000 | tf_op jit(solution)/shard_map/pallas_call | solution.py:57
  97.2 2.7 %shard_map.224 = (bf16[192,128]{1,0:T(8,128)(2,1)}, bf16[192,128]{1,0:T(8,128)(2,1)}, f32[192,128]{1,0:T(8,128)}) custom-call(bf16[192,128]{1,0:T(8,128)(2,1)} %copy-done.16, bf16[4,2048]{1,0:T(4,128)(2,1)} %bitcast.37, bf16[64,2048]{1,0:T(8,128)(2,1)} %bitcast.36, f32[1,2048]{1,0:T(1,128)} %bitcast.39, bf16[24,2176]{1,0:T(8,128)(2,1)} %copy-done, ...), custom_call_target="tpu_custom_call" | custom-call | flops 60000000 | bytes 1500000 | tf_op jit(solution)/shard_map/pallas_call | solution.py:57
  102.5 2.6 %shard_map.228 = (f32[96,512]{1,0:T(8,128)}, bf16[96,512]{1,0:T(8,128)(2,1)}) custom-call(bf16[192,256]{1,0:T(8,128)(2,1)} %shard_map.222.refs_0_, bf16[192,256]{1,0:T(8,128)(2,1)} %copy-done.25, bf16[192,256]{1,0:T(8,128)(2,1)} %copy-done.24, bf16[192,256]{1,0:T(8,128)(2,1)} %copy-done.23, bf16[384,512]{1,0:T(8,128)(2,1)} %copy-done.18, ...), custom_call_target="tpu_custom_call" | custom-call | flops 400000000 | bytes 2000000 | tf_op jit(solution)/shard_map/pallas_call | solution.py:57
  105.2 6.5 %collective-permute-start.29 = (bf16[96,512]{1,0:T(8,128)(2,1)}, bf16[96,512]{1,0:T(8,128)(2,1)S(1)}, u32[]{:S(2)}, u32[]{:S(2)}) collective-permute-start(bf16[96,512]{1,0:T(8,128)(2,1)} %get-tuple-element.43), channel_id=1, source_target_pairs={{0,4},{4,0},{1,5},{5,1},{2,6},{6,2},{3,7},{7,3},{8,12},{12,8},{9,1... | collective-permute-start | bytes 294920 | tf_op jit(solution)/shard_map/ppermute | solution.py:26
  111.7 1.2 collective-permute-done.29.come_ref
  115.4 1.2 %collective-permute-done.30.refs_0_ = bf16[24,512]{1,0:T(8,128)(2,1)S(1)} collective-permute-done((bf16[24,512]{1,0:T(8,128)(2,1)S(1)}, bf16[24,512]{1,0:T(8,128)(2,1)S(1)}, u32[]{:S(2)}, u32[]{:S(2)}) %collective-permute-start.30) | collective-permute-done | bytes 24608 | tf_op jit(solution)/shard_map/ppermute | solution.py:26
  116.6 1.8 %collective-permute-done.31.refs_1_ = bf16[24,512]{1,0:T(8,128)(2,1)S(1)} collective-permute-done((bf16[24,512]{1,0:T(8,128)(2,1)S(1)}, bf16[24,512]{1,0:T(8,128)(2,1)S(1)}, u32[]{:S(2)}, u32[]{:S(2)}) %collective-permute-start.31) | collective-permute-done | bytes 24608 | tf_op jit(solution)/shard_map/ppermute | solution.py:26
  (110 shorter events, 22.9 us)
Async XLA Ops:
  2.6 5.7 %collective-permute-start.10 = (bf16[64,512]{1,0:T(8,128)(2,1)S(1)}, bf16[64,512]{1,0:T(8,128)(2,1)S(1)}, u32[]{:S(2)}, u32[]{:S(2)}) collective-permute-start(bf16[64,512]{1,0:T(8,128)(2,1)S(1)} %get-tuple-element.30), channel_id=1, source_target_pairs={{0,1},{1,2},{2,3},{3,0},{4,5},{5,6},{6,7},{7,4},{8,9},{9,10},{10,1... | collective-permute-start | bytes 196616 | tf_op jit(solution)/shard_map/ppermute | solution.py:26
  4.7 5.1 %collective-permute-start.11 = (bf16[64,512]{1,0:T(8,128)(2,1)S(1)}, bf16[64,512]{1,0:T(8,128)(2,1)S(1)}, u32[]{:S(2)}, u32[]{:S(2)}) collective-permute-start(bf16[64,512]{1,0:T(8,128)(2,1)S(1)} %get-tuple-element.31), channel_id=1, source_target_pairs={{0,2},{1,3},{2,0},{3,1},{4,6},{5,7},{6,4},{7,5},{8,10},{9,11},{10,... | collective-permute-start | bytes 196616 | tf_op jit(solution)/shard_map/ppermute | solution.py:26
  11.5 13.5 %collective-permute-start.13 = (bf16[384,512]{1,0:T(8,128)(2,1)S(1)}, bf16[384,512]{1,0:T(8,128)(2,1)S(1)}, u32[]{:S(2)}, u32[]{:S(2)}) collective-permute-start(bf16[384,512]{1,0:T(8,128)(2,1)S(1)} %constant_dynamic-update-slice_fusion.refs_8_.refs_4_), channel_id=1, source_target_pairs={{0,32},{32,64},{64,96},{96,128},{128,160},{160,192},{192,224},{224... | collective-permute-start | bytes 1179656 | tf_op jit(solution)/shard_map/ppermute | solution.py:26
  13.4 21.8 %collective-permute-start.14 = (bf16[384,512]{1,0:T(8,128)(2,1)S(1)}, bf16[384,512]{1,0:T(8,128)(2,1)}, u32[]{:S(2)}, u32[]{:S(2)}) collective-permute-start(bf16[384,512]{1,0:T(8,128)(2,1)S(1)} %constant_dynamic-update-slice_fusion.refs_8_.refs_4_), channel_id=1, source_target_pairs={{0,224},{32,0},{64,32},{96,64},{128,96},{160,128},{192,160},{224,1... | collective-permute-start | bytes 1179656 | tf_op jit(solution)/shard_map/ppermute | solution.py:26
  25.0 12.8 %collective-permute-start.15 = (bf16[384,512]{1,0:T(8,128)(2,1)S(1)}, bf16[384,512]{1,0:T(8,128)(2,1)}, u32[]{:S(2)}, u32[]{:S(2)}) collective-permute-start(bf16[384,512]{1,0:T(8,128)(2,1)S(1)} %collective-permute-done.13.refs_9_.refs_5_), channel_id=1, source_target_pairs={{0,32},{32,64},{64,96},{96,128},{128,160},{160,192},{192,224},{224... | collective-permute-start | bytes 1179656 | tf_op jit(solution)/shard_map/ppermute | solution.py:26
  32.7 5.2 %collective-permute-start.2 = (bf16[24,2048]{1,0:T(8,128)(2,1)}, bf16[24,2048]{1,0:T(8,128)(2,1)S(1)}, u32[]{:S(2)}, u32[]{:S(2)}) collective-permute-start(bf16[24,2048]{1,0:T(8,128)(2,1)} %get-tuple-element.27.refs_0_), channel_id=1, source_target_pairs={{0,3},{1,0},{2,1},{3,2},{4,7},{5,4},{6,5},{7,6},{8,11},{9,8},{10,9... | collective-permute-start | bytes 294920 | tf_op jit(solution)/shard_map/ppermute | solution.py:26
  34.6 5.3 %collective-permute-start.1 = (bf16[24,2048]{1,0:T(8,128)(2,1)}, bf16[24,2048]{1,0:T(8,128)(2,1)S(1)}, u32[]{:S(2)}, u32[]{:S(2)}) collective-permute-start(bf16[24,2048]{1,0:T(8,128)(2,1)} %get-tuple-element.27.refs_0_), channel_id=1, source_target_pairs={{0,2},{1,3},{2,0},{3,1},{4,6},{5,7},{6,4},{7,5},{8,10},{9,11},{10,... | collective-permute-start | bytes 294920 | tf_op jit(solution)/shard_map/ppermute | solution.py:26
  34.6 5.9 %collective-permute-start = (bf16[24,2048]{1,0:T(8,128)(2,1)}, bf16[24,2048]{1,0:T(8,128)(2,1)S(1)}, u32[]{:S(2)}, u32[]{:S(2)}) collective-permute-start(bf16[24,2048]{1,0:T(8,128)(2,1)} %get-tuple-element.27.refs_0_), channel_id=1, source_target_pairs={{0,1},{1,2},{2,3},{3,0},{4,5},{5,6},{6,7},{7,4},{8,9},{9,10},{10,1... | collective-permute-start | bytes 294920 | tf_op jit(solution)/shard_map/ppermute | solution.py:26
  35.3 30.8 %collective-permute-start.16 = (bf16[384,512]{1,0:T(8,128)(2,1)}, bf16[384,512]{1,0:T(8,128)(2,1)S(1)}, u32[]{:S(2)}, u32[]{:S(2)}) collective-permute-start(bf16[384,512]{1,0:T(8,128)(2,1)} %collective-permute-done.14.refs_10_.refs_6_), channel_id=1, source_target_pairs={{0,224},{32,0},{64,32},{96,64},{128,96},{160,128},{192,160},{224,1... | collective-permute-start | bytes 1179656 | tf_op jit(solution)/shard_map/ppermute | solution.py:26
  37.8 31.0 %collective-permute-start.17 = (bf16[384,512]{1,0:T(8,128)(2,1)}, bf16[384,512]{1,0:T(8,128)(2,1)S(1)}, u32[]{:S(2)}, u32[]{:S(2)}) collective-permute-start(bf16[384,512]{1,0:T(8,128)(2,1)} %collective-permute-done.15.refs_11_.refs_7_), channel_id=1, source_target_pairs={{0,32},{32,64},{64,96},{96,128},{128,160},{160,192},{192,224},{224... | collective-permute-start | bytes 1179656 | tf_op jit(solution)/shard_map/ppermute | solution.py:26
  41.6 7.3 %collective-permute-start.6 = (bf16[24,2176]{1,0:T(8,128)(2,1)S(1)}, bf16[24,2176]{1,0:T(8,128)(2,1)S(1)}, u32[]{:S(2)}, u32[]{:S(2)}) collective-permute-start(bf16[24,2176]{1,0:T(8,128)(2,1)S(1)} %get-tuple-element.28.refs_0_), channel_id=1, source_target_pairs={{0,4},{4,0},{1,5},{5,1},{2,6},{6,2},{3,7},{7,3},{8,12},{12,8},{9,1... | collective-permute-start | bytes 313352 | tf_op jit(solution)/shard_map/ppermute | solution.py:26
  45.8 6.8 %collective-permute-start.5 = (bf16[24,2176]{1,0:T(8,128)(2,1)S(1)}, bf16[24,2176]{1,0:T(8,128)(2,1)S(1)}, u32[]{:S(2)}, u32[]{:S(2)}) collective-permute-start(bf16[24,2176]{1,0:T(8,128)(2,1)S(1)} %get-tuple-element.28.refs_0_), channel_id=1, source_target_pairs={{0,24},{8,0},{16,8},{24,16},{1,25},{9,1},{17,9},{25,17},{2,26},{10... | collective-permute-start | bytes 313352 | tf_op jit(solution)/shard_map/ppermute | solution.py:26
  48.6 5.4 %collective-permute-start.4 = (bf16[24,2176]{1,0:T(8,128)(2,1)S(1)}, bf16[24,2176]{1,0:T(8,128)(2,1)S(1)}, u32[]{:S(2)}, u32[]{:S(2)}) collective-permute-start(bf16[24,2176]{1,0:T(8,128)(2,1)S(1)} %get-tuple-element.28.refs_0_), channel_id=1, source_target_pairs={{0,16},{8,24},{16,0},{24,8},{1,17},{9,25},{17,1},{25,9},{2,18},{10... | collective-permute-start | bytes 313352 | tf_op jit(solution)/shard_map/ppermute | solution.py:26
  48.9 8.2 %collective-permute-start.3 = (bf16[24,2176]{1,0:T(8,128)(2,1)S(1)}, bf16[24,2176]{1,0:T(8,128)(2,1)S(1)}, u32[]{:S(2)}, u32[]{:S(2)}) collective-permute-start(bf16[24,2176]{1,0:T(8,128)(2,1)S(1)} %get-tuple-element.28.refs_0_), channel_id=1, source_target_pairs={{0,8},{8,16},{16,24},{24,0},{1,9},{9,17},{17,25},{25,1},{2,10},{10... | collective-permute-start | bytes 313352 | tf_op jit(solution)/shard_map/ppermute | solution.py:26
  52.7 5.0 %collective-permute-start.9 = (bf16[24,2176]{1,0:T(8,128)(2,1)S(1)}, bf16[24,2176]{1,0:T(8,128)(2,1)S(1)}, u32[]{:S(2)}, u32[]{:S(2)}) collective-permute-start(bf16[24,2176]{1,0:T(8,128)(2,1)S(1)} %collective-permute-done.5.refs_3_), channel_id=1, source_target_pairs={{0,4},{4,0},{1,5},{5,1},{2,6},{6,2},{3,7},{7,3},{8,12},{12,8},{9,1... | collective-permute-start | bytes 313352 | tf_op jit(solution)/shard_map/ppermute | solution.py:26
  54.0 3.7 %collective-permute-start.8 = (bf16[24,2176]{1,0:T(8,128)(2,1)S(1)}, bf16[24,2176]{1,0:T(8,128)(2,1)S(1)}, u32[]{:S(2)}, u32[]{:S(2)}) collective-permute-start(bf16[24,2176]{1,0:T(8,128)(2,1)S(1)} %collective-permute-done.4.refs_2_), channel_id=1, source_target_pairs={{0,4},{4,0},{1,5},{5,1},{2,6},{6,2},{3,7},{7,3},{8,12},{12,8},{9,1... | collective-permute-start | bytes 313352 | tf_op jit(solution)/shard_map/ppermute | solution.py:26
  60.4 13.7 %all-to-all-start = ((bf16[8,16,512]{2,1,0:T(8,128)(2,1)}), bf16[8,16,512]{2,1,0:T(8,128)(2,1)S(1)}, u32[]{:S(2)}, u32[]{:S(2)}) async-start(bf16[8,16,512]{2,1,0:T(8,128)(2,1)} %bitcast.13), calls=%async_computation | async-start | bytes 262144 | tf_op jit(solution)/shard_map/all_to_all | solution.py:503
  66.1 25.7 %collective-permute-start.18 = (bf16[384,512]{1,0:T(8,128)(2,1)S(1)}, bf16[384,512]{1,0:T(8,128)(2,1)}, u32[]{:S(2)}, u32[]{:S(2)}) collective-permute-start(bf16[384,512]{1,0:T(8,128)(2,1)S(1)} %collective-permute-done.16.refs_12_.refs_8_), channel_id=1, source_target_pairs={{0,224},{32,0},{64,32},{96,64},{128,96},{160,128},{192,160},{224,1... | collective-permute-start | bytes 1179656 | tf_op jit(solution)/shard_map/ppermute | solution.py:26
  68.8 22.9 %collective-permute-start.19 = (bf16[384,512]{1,0:T(8,128)(2,1)S(1)}, bf16[384,512]{1,0:T(8,128)(2,1)}, u32[]{:S(2)}, u32[]{:S(2)}) collective-permute-start(bf16[384,512]{1,0:T(8,128)(2,1)S(1)} %collective-permute-done.17.refs_13_.refs_9_), channel_id=1, source_target_pairs={{0,32},{32,64},{64,96},{96,128},{128,160},{160,192},{192,224},{224... | collective-permute-start | bytes 1179656 | tf_op jit(solution)/shard_map/ppermute | solution.py:26
  74.4 5.5 %collective-permute-start.23 = (bf16[128,256]{1,0:T(8,128)(2,1)S(1)}, bf16[128,256]{1,0:T(8,128)(2,1)S(1)}, u32[]{:S(2)}, u32[]{:S(2)}) collective-permute-start(bf16[128,256]{1,0:T(8,128)(2,1)S(1)} %get-tuple-element.37), channel_id=1, source_target_pairs={{0,1},{1,2},{2,3},{3,0},{4,5},{5,6},{6,7},{7,4},{8,9},{9,10},{10,1... | collective-permute-start | bytes 196616 | tf_op jit(solution)/shard_map/ppermute | solution.py:26
  74.5 5.4 %collective-permute-start.24 = (bf16[128,256]{1,0:T(8,128)(2,1)S(1)}, bf16[128,256]{1,0:T(8,128)(2,1)S(1)}, u32[]{:S(2)}, u32[]{:S(2)}) collective-permute-start(bf16[128,256]{1,0:T(8,128)(2,1)S(1)} %get-tuple-element.38), channel_id=1, source_target_pairs={{0,2},{1,3},{2,0},{3,1},{4,6},{5,7},{6,4},{7,5},{8,10},{9,11},{10,... | collective-permute-start | bytes 196616 | tf_op jit(solution)/shard_map/ppermute | solution.py:26
  76.2 4.2 %collective-permute-start.25 = (bf16[128,256]{1,0:T(8,128)(2,1)S(1)}, bf16[128,256]{1,0:T(8,128)(2,1)S(1)}, u32[]{:S(2)}, u32[]{:S(2)}) collective-permute-start(bf16[128,256]{1,0:T(8,128)(2,1)S(1)} %get-tuple-element.39), channel_id=1, source_target_pairs={{0,3},{1,0},{2,1},{3,2},{4,7},{5,4},{6,5},{7,6},{8,11},{9,8},{10,9... | collective-permute-start | bytes 196616 | tf_op jit(solution)/shard_map/ppermute | solution.py:26
  80.5 3.5 %collective-permute-start.28 = (bf16[128,128]{1,0:T(8,128)(2,1)S(1)}, bf16[128,128]{1,0:T(8,128)(2,1)S(1)}, u32[]{:S(2)}, u32[]{:S(2)}) collective-permute-start(bf16[128,128]{1,0:T(8,128)(2,1)S(1)} %shard_map.226.refs_0_), channel_id=1, source_target_pairs={{0,3},{1,0},{2,1},{3,2},{4,7},{5,4},{6,5},{7,6},{8,11},{9,8},{10,9... | collective-permute-start | bytes 98312 | tf_op jit(solution)/shard_map/ppermute | solution.py:26
  82.9 4.4 %collective-permute-start.27 = (bf16[128,128]{1,0:T(8,128)(2,1)S(1)}, bf16[128,128]{1,0:T(8,128)(2,1)S(1)}, u32[]{:S(2)}, u32[]{:S(2)}) collective-permute-start(bf16[128,128]{1,0:T(8,128)(2,1)S(1)} %shard_map.226.refs_0_), channel_id=1, source_target_pairs={{0,2},{1,3},{2,0},{3,1},{4,6},{5,7},{6,4},{7,5},{8,10},{9,11},{10,... | collective-permute-start | bytes 98312 | tf_op jit(solution)/shard_map/ppermute | solution.py:26
  83.1 4.3 %collective-permute-start.26 = (bf16[128,128]{1,0:T(8,128)(2,1)S(1)}, bf16[128,128]{1,0:T(8,128)(2,1)S(1)}, u32[]{:S(2)}, u32[]{:S(2)}) collective-permute-start(bf16[128,128]{1,0:T(8,128)(2,1)S(1)} %shard_map.226.refs_0_), channel_id=1, source_target_pairs={{0,1},{1,2},{2,3},{3,0},{4,5},{5,6},{6,7},{7,4},{8,9},{9,10},{10,1... | collective-permute-start | bytes 98312 | tf_op jit(solution)/shard_map/ppermute | solution.py:26
  88.4 11.6 %all-to-all-start.1 = ((bf16[8,16,512]{2,1,0:T(8,128)(2,1)}), bf16[8,16,512]{2,1,0:T(8,128)(2,1)S(1)}, u32[]{:S(2)}, u32[]{:S(2)}) async-start(bf16[8,16,512]{2,1,0:T(8,128)(2,1)} %bitcast.18), calls=%async_computation.1 | async-start | bytes 262144 | tf_op jit(solution)/shard_map/all_to_all | solution.py:503
  95.2 4.7 %collective-permute-start.22 = (bf16[192,256]{1,0:T(8,128)(2,1)}, bf16[192,256]{1,0:T(8,128)(2,1)S(1)}, u32[]{:S(2)}, u32[]{:S(2)}) collective-permute-start(bf16[192,256]{1,0:T(8,128)(2,1)} %shard_map.222.refs_0_), channel_id=1, source_target_pairs={{0,3},{1,0},{2,1},{3,2},{4,7},{5,4},{6,5},{7,6},{8,11},{9,8},{10,9... | collective-permute-start | bytes 294920 | tf_op jit(solution)/shard_map/ppermute | solution.py:26
  95.5 5.2 %collective-permute-start.21 = (bf16[192,256]{1,0:T(8,128)(2,1)}, bf16[192,256]{1,0:T(8,128)(2,1)S(1)}, u32[]{:S(2)}, u32[]{:S(2)}) collective-permute-start(bf16[192,256]{1,0:T(8,128)(2,1)} %shard_map.222.refs_0_), channel_id=1, source_target_pairs={{0,2},{1,3},{2,0},{3,1},{4,6},{5,7},{6,4},{7,5},{8,10},{9,11},{10,... | collective-permute-start | bytes 294920 | tf_op jit(solution)/shard_map/ppermute | solution.py:26
  96.4 5.5 %collective-permute-start.20 = (bf16[192,256]{1,0:T(8,128)(2,1)}, bf16[192,256]{1,0:T(8,128)(2,1)S(1)}, u32[]{:S(2)}, u32[]{:S(2)}) collective-permute-start(bf16[192,256]{1,0:T(8,128)(2,1)} %shard_map.222.refs_0_), channel_id=1, source_target_pairs={{0,1},{1,2},{2,3},{3,0},{4,5},{5,6},{6,7},{7,4},{8,9},{9,10},{10,1... | collective-permute-start | bytes 294920 | tf_op jit(solution)/shard_map/ppermute | solution.py:26
  105.2 7.7 %collective-permute-start.29 = (bf16[96,512]{1,0:T(8,128)(2,1)}, bf16[96,512]{1,0:T(8,128)(2,1)S(1)}, u32[]{:S(2)}, u32[]{:S(2)}) collective-permute-start(bf16[96,512]{1,0:T(8,128)(2,1)} %get-tuple-element.43), channel_id=1, source_target_pairs={{0,4},{4,0},{1,5},{5,1},{2,6},{6,2},{3,7},{7,3},{8,12},{12,8},{9,1... | collective-permute-start | bytes 294920 | tf_op jit(solution)/shard_map/ppermute | solution.py:26
  114.2 4.2 %collective-permute-start.31 = (bf16[24,512]{1,0:T(8,128)(2,1)S(1)}, bf16[24,512]{1,0:T(8,128)(2,1)S(1)}, u32[]{:S(2)}, u32[]{:S(2)}) collective-permute-start(bf16[24,512]{1,0:T(8,128)(2,1)S(1)} %get-tuple-element.47), channel_id=1, source_target_pairs={{0,16},{8,24},{16,0},{24,8},{1,17},{9,25},{17,1},{25,9},{2,18},{10... | collective-permute-start | bytes 73736 | tf_op jit(solution)/shard_map/ppermute | solution.py:26
  114.5 4.4 %collective-permute-start.32 = (bf16[24,512]{1,0:T(8,128)(2,1)S(1)}, bf16[24,512]{1,0:T(8,128)(2,1)S(1)}, u32[]{:S(2)}, u32[]{:S(2)}) collective-permute-start(bf16[24,512]{1,0:T(8,128)(2,1)S(1)} %get-tuple-element.48), channel_id=1, source_target_pairs={{0,8},{8,16},{16,24},{24,0},{1,9},{9,17},{17,25},{25,1},{2,10},{10... | collective-permute-start | bytes 73736 | tf_op jit(solution)/shard_map/ppermute | solution.py:26
  (30 other events, 598.1 us)

commit v4 on v3

--- a/solution.py
+++ b/solution.py
@@ -371,12 +371,10 @@
 
 
 def expert_out_kernel(*refs):
-    hiddens, (down_ref, out_ref) = refs[:-2], refs[-2:]
-    units = hiddens[0].shape[1]
-    total = 0.0
+    hiddens, (down_ref, out_ref, hidden_ref) = refs[:-3], refs[-3:]
     for k, hidden in enumerate(hiddens):
-        total = total + dot(hidden[...], down_ref[span(behind(TP, k), units), :])
-    out_ref[...] = total.astype(BF16)
+        hidden_ref[:, span(behind(TP, k), hidden.shape[1])] = hidden[...]
+    out_ref[...] = dot(hidden_ref[...], down_ref[...]).astype(BF16)
 
 
 def expert_out(hiddens, down):
@@ -384,6 +382,7 @@
         expert_out_kernel,
         jax.ShapeDtypeStruct((hiddens[0].shape[0], down.shape[1]), BF16),
         70_000_000, 800_000, *hiddens, down,
+        scratch_shapes=[pltpu.VMEM((hiddens[0].shape[0], down.shape[0]), BF16)],
     )
 
 

time: 120 us -> 120 us (level)
  no operation moved by 1% of the time
where the time goes in v4:
time: 120 us
  starting transfers between devices  57 us (48%)
  waiting for transfers between devices  36 us (30%)
  Pallas kernels  19.6 us (16%)
  local copies, waits for them, and re-layouts  5.98 us (5%)
    ppermute x33, starting transfers between devices, shifted(): return lax.ppermute(x, axis, [(i, (i + step) % size) for i in range(size)])  47.9 us
    ppermute x33, waiting for transfers between devices, shifted(): return lax.ppermute(x, axis, [(i, (i + step) % size) for i in range(size)])  30.8 us
    pallas_call x11, Pallas kernels, call(): pl.pallas_call(kernel, out_shape=out, cost_estimate=pl.CostEstimate(flops...  12.1 us
    all_to_all x2, starting transfers between devices, over_z(): lax.all_to_all(shaped, Z, split_axis=0, concat_axis=0, tiled=True)  9.07 us
    pallas_call x1, Pallas kernels, attention(): pl.pallas_call(attention_kernel, out_shape=(jax.ShapeDtypeStruct((seq, wi...  7.58 us
    all_to_all x2, waiting for transfers between devices, over_z(): lax.all_to_all(shaped, Z, split_axis=0, concat_axis=0, tiled=True)  5.19 us
    unnamed x59, local copies, waits for them, and re-layouts  5.06 us
  transfers between devices with their start and end apart: 35, of which 21 were waited for; matrix products, arithmetic and copies ran while one was open for 0% of the time, Pallas kernels for 14%

profile of v4, /device:TPU:1, one launch (start us, length us, event | category | flops | bytes accessed | tf_op | source)
XLA Modules:
  0.0 119.5 jit_solution(17998425308092613055)
XLA Ops:
  2.6 2.1 %collective-permute-start.10 = (bf16[64,512]{1,0:T(8,128)(2,1)S(1)}, bf16[64,512]{1,0:T(8,128)(2,1)S(1)}, u32[]{:S(2)}, u32[]{:S(2)}) collective-permute-start(bf16[64,512]{1,0:T(8,128)(2,1)S(1)} %get-tuple-element.30), channel_id=1, source_target_pairs={{0,1},{1,2},{2,3},{3,0},{4,5},{5,6},{6,7},{7,4},{8,9},{9,10},{10,1... | collective-permute-start | bytes 196616 | tf_op jit(solution)/shard_map/ppermute | solution.py:26
  4.7 2.5 %collective-permute-start.11 = (bf16[64,512]{1,0:T(8,128)(2,1)S(1)}, bf16[64,512]{1,0:T(8,128)(2,1)S(1)}, u32[]{:S(2)}, u32[]{:S(2)}) collective-permute-start(bf16[64,512]{1,0:T(8,128)(2,1)S(1)} %get-tuple-element.31), channel_id=1, source_target_pairs={{0,2},{1,3},{2,0},{3,1},{4,6},{5,7},{6,4},{7,5},{8,10},{9,11},{10,... | collective-permute-start | bytes 196616 | tf_op jit(solution)/shard_map/ppermute | solution.py:26
  7.1 1.2 collective-permute-start.12
  8.3 1.4 %collective-permute-done.11 = bf16[64,512]{1,0:T(8,128)(2,1)S(1)} collective-permute-done((bf16[64,512]{1,0:T(8,128)(2,1)S(1)}, bf16[64,512]{1,0:T(8,128)(2,1)S(1)}, u32[]{:S(2)}, u32[]{:S(2)}) %collective-permute-start.11) | collective-permute-done | bytes 65568 | tf_op jit(solution)/shard_map/ppermute | solution.py:26
  11.5 2.0 %collective-permute-start.13 = (bf16[384,512]{1,0:T(8,128)(2,1)S(1)}, bf16[384,512]{1,0:T(8,128)(2,1)S(1)}, u32[]{:S(2)}, u32[]{:S(2)}) collective-permute-start(bf16[384,512]{1,0:T(8,128)(2,1)S(1)} %constant_dynamic-update-slice_fusion.refs_8_.refs_4_), channel_id=1, source_target_pairs={{0,32},{32,64},{64,96},{96,128},{128,160},{160,192},{192,224},{224... | collective-permute-start | bytes 1179656 | tf_op jit(solution)/shard_map/ppermute | solution.py:26
  13.4 4.0 %collective-permute-start.14 = (bf16[384,512]{1,0:T(8,128)(2,1)S(1)}, bf16[384,512]{1,0:T(8,128)(2,1)}, u32[]{:S(2)}, u32[]{:S(2)}) collective-permute-start(bf16[384,512]{1,0:T(8,128)(2,1)S(1)} %constant_dynamic-update-slice_fusion.refs_8_.refs_4_), channel_id=1, source_target_pairs={{0,224},{32,0},{64,32},{96,64},{128,96},{160,128},{192,160},{224,1... | collective-permute-start | bytes 1179656 | tf_op jit(solution)/shard_map/ppermute | solution.py:26
  17.5 7.6 %collective-permute-done.13.refs_9_.refs_5_ = bf16[384,512]{1,0:T(8,128)(2,1)S(1)} collective-permute-done((bf16[384,512]{1,0:T(8,128)(2,1)S(1)}, bf16[384,512]{1,0:T(8,128)(2,1)S(1)}, u32[]{:S(2)}, u32[]{:S(2)}) %collective-permute-start.13) | collective-permute-done | bytes 393248 | tf_op jit(solution)/shard_map/ppermute | solution.py:26
  25.1 7.6 %attention.1 = (bf16[24,2048]{1,0:T(8,128)(2,1)}, bf16[24,64]{1,0:T(8,128)(2,1)}, bf16[24,64]{1,0:T(8,128)(2,1)}) custom-call(s32[24]{0:T(128)} %lengths_ref.1, bf16[24,2048]{1,0:T(8,128)(2,1)} %tokens_ref.3, f32[1,2048]{1,0:T(1,128)} %bitcast.38, f32[8]{0:T(128)} %bias_ref.1, bf16[64,2048]{1,0:T(8,128)(2,1)} %bitcast.34, bf16[64,2048]{1,0:T(8,128)(2,1)} %bitcast.35, ...), custom_call_target="tpu_custom_call" | custom-call | flops 400000000 | bytes 11000000 | tf_op jit(solution)/shard_map/attention/pallas_call | solution.py:178
  32.7 1.9 %collective-permute-start.2 = (bf16[24,2048]{1,0:T(8,128)(2,1)}, bf16[24,2048]{1,0:T(8,128)(2,1)S(1)}, u32[]{:S(2)}, u32[]{:S(2)}) collective-permute-start(bf16[24,2048]{1,0:T(8,128)(2,1)} %get-tuple-element.27.refs_0_), channel_id=1, source_target_pairs={{0,3},{1,0},{2,1},{3,2},{4,7},{5,4},{6,5},{7,6},{8,11},{9,8},{10,9... | collective-permute-start | bytes 294920 | tf_op jit(solution)/shard_map/ppermute | solution.py:26
  35.3 2.5 %collective-permute-start.16 = (bf16[384,512]{1,0:T(8,128)(2,1)}, bf16[384,512]{1,0:T(8,128)(2,1)S(1)}, u32[]{:S(2)}, u32[]{:S(2)}) collective-permute-start(bf16[384,512]{1,0:T(8,128)(2,1)} %collective-permute-done.14.refs_10_.refs_6_), channel_id=1, source_target_pairs={{0,224},{32,0},{64,32},{96,64},{128,96},{160,128},{192,160},{224,1... | collective-permute-start | bytes 1179656 | tf_op jit(solution)/shard_map/ppermute | solution.py:26
  37.9 2.0 %collective-permute-done.1.refs_2_ = bf16[24,2048]{1,0:T(8,128)(2,1)S(1)} collective-permute-done((bf16[24,2048]{1,0:T(8,128)(2,1)}, bf16[24,2048]{1,0:T(8,128)(2,1)S(1)}, u32[]{:S(2)}, u32[]{:S(2)}) %collective-permute-start.1) | collective-permute-done | bytes 98336 | tf_op jit(solution)/shard_map/ppermute | solution.py:26
  41.6 4.2 %collective-permute-start.6 = (bf16[24,2176]{1,0:T(8,128)(2,1)S(1)}, bf16[24,2176]{1,0:T(8,128)(2,1)S(1)}, u32[]{:S(2)}, u32[]{:S(2)}) collective-permute-start(bf16[24,2176]{1,0:T(8,128)(2,1)S(1)} %get-tuple-element.28.refs_0_), channel_id=1, source_target_pairs={{0,4},{4,0},{1,5},{5,1},{2,6},{6,2},{3,7},{7,3},{8,12},{12,8},{9,1... | collective-permute-start | bytes 313352 | tf_op jit(solution)/shard_map/ppermute | solution.py:26
  45.8 2.7 %collective-permute-start.5 = (bf16[24,2176]{1,0:T(8,128)(2,1)S(1)}, bf16[24,2176]{1,0:T(8,128)(2,1)S(1)}, u32[]{:S(2)}, u32[]{:S(2)}) collective-permute-start(bf16[24,2176]{1,0:T(8,128)(2,1)S(1)} %get-tuple-element.28.refs_0_), channel_id=1, source_target_pairs={{0,24},{8,0},{16,8},{24,16},{1,25},{9,1},{17,9},{25,17},{2,26},{10... | collective-permute-start | bytes 313352 | tf_op jit(solution)/shard_map/ppermute | solution.py:26
  49.6 3.1 %collective-permute-done.5.refs_3_ = bf16[24,2176]{1,0:T(8,128)(2,1)S(1)} collective-permute-done((bf16[24,2176]{1,0:T(8,128)(2,1)S(1)}, bf16[24,2176]{1,0:T(8,128)(2,1)S(1)}, u32[]{:S(2)}, u32[]{:S(2)}) %collective-permute-start.5) | collective-permute-done | bytes 104480 | tf_op jit(solution)/shard_map/ppermute | solution.py:26
  52.7 1.3 %collective-permute-start.9 = (bf16[24,2176]{1,0:T(8,128)(2,1)S(1)}, bf16[24,2176]{1,0:T(8,128)(2,1)S(1)}, u32[]{:S(2)}, u32[]{:S(2)}) collective-permute-start(bf16[24,2176]{1,0:T(8,128)(2,1)S(1)} %collective-permute-done.5.refs_3_), channel_id=1, source_target_pairs={{0,4},{4,0},{1,5},{5,1},{2,6},{6,2},{3,7},{7,3},{8,12},{12,8},{9,1... | collective-permute-start | bytes 313352 | tf_op jit(solution)/shard_map/ppermute | solution.py:26
  54.0 2.4 %collective-permute-start.8 = (bf16[24,2176]{1,0:T(8,128)(2,1)S(1)}, bf16[24,2176]{1,0:T(8,128)(2,1)S(1)}, u32[]{:S(2)}, u32[]{:S(2)}) collective-permute-start(bf16[24,2176]{1,0:T(8,128)(2,1)S(1)} %collective-permute-done.4.refs_2_), channel_id=1, source_target_pairs={{0,4},{4,0},{1,5},{5,1},{2,6},{6,2},{3,7},{7,3},{8,12},{12,8},{9,1... | collective-permute-start | bytes 313352 | tf_op jit(solution)/shard_map/ppermute | solution.py:26
  60.4 5.7 %all-to-all-start = ((bf16[8,16,512]{2,1,0:T(8,128)(2,1)}), bf16[8,16,512]{2,1,0:T(8,128)(2,1)S(1)}, u32[]{:S(2)}, u32[]{:S(2)}) async-start(bf16[8,16,512]{2,1,0:T(8,128)(2,1)} %bitcast.13), calls=%async_computation | async-start | bytes 262144 | tf_op jit(solution)/shard_map/all_to_all | solution.py:502
  66.1 2.7 %collective-permute-start.18 = (bf16[384,512]{1,0:T(8,128)(2,1)S(1)}, bf16[384,512]{1,0:T(8,128)(2,1)}, u32[]{:S(2)}, u32[]{:S(2)}) collective-permute-start(bf16[384,512]{1,0:T(8,128)(2,1)S(1)} %collective-permute-done.16.refs_12_.refs_8_), channel_id=1, source_target_pairs={{0,224},{32,0},{64,32},{96,64},{128,96},{160,128},{192,160},{224,1... | collective-permute-start | bytes 1179656 | tf_op jit(solution)/shard_map/ppermute | solution.py:26
  68.9 5.2 %all-to-all-done = bf16[8,16,512]{2,1,0:T(8,128)(2,1)S(1)} async-done(((bf16[8,16,512]{2,1,0:T(8,128)(2,1)}), bf16[8,16,512]{2,1,0:T(8,128)(2,1)S(1)}, u32[]{:S(2)}, u32[]{:S(2)}) %all-to-all-start) | async-done | bytes 131104 | tf_op jit(solution)/shard_map/all_to_all | solution.py:502
  74.5 1.8 %collective-permute-start.24 = (bf16[128,256]{1,0:T(8,128)(2,1)S(1)}, bf16[128,256]{1,0:T(8,128)(2,1)S(1)}, u32[]{:S(2)}, u32[]{:S(2)}) collective-permute-start(bf16[128,256]{1,0:T(8,128)(2,1)S(1)} %get-tuple-element.38), channel_id=1, source_target_pairs={{0,2},{1,3},{2,0},{3,1},{4,6},{5,7},{6,4},{7,5},{8,10},{9,11},{10,... | collective-permute-start | bytes 196616 | tf_op jit(solution)/shard_map/ppermute | solution.py:26
  76.2 1.3 %collective-permute-start.25 = (bf16[128,256]{1,0:T(8,128)(2,1)S(1)}, bf16[128,256]{1,0:T(8,128)(2,1)S(1)}, u32[]{:S(2)}, u32[]{:S(2)}) collective-permute-start(bf16[128,256]{1,0:T(8,128)(2,1)S(1)} %get-tuple-element.39), channel_id=1, source_target_pairs={{0,3},{1,0},{2,1},{3,2},{4,7},{5,4},{6,5},{7,6},{8,11},{9,8},{10,9... | collective-permute-start | bytes 196616 | tf_op jit(solution)/shard_map/ppermute | solution.py:26
  77.5 2.4 %collective-permute-done.23.refs_1_ = bf16[128,256]{1,0:T(8,128)(2,1)S(1)} collective-permute-done((bf16[128,256]{1,0:T(8,128)(2,1)S(1)}, bf16[128,256]{1,0:T(8,128)(2,1)S(1)}, u32[]{:S(2)}, u32[]{:S(2)}) %collective-permute-start.23) | collective-permute-done | bytes 65568 | tf_op jit(solution)/shard_map/ppermute | solution.py:26
  80.5 2.3 %collective-permute-start.28 = (bf16[128,128]{1,0:T(8,128)(2,1)S(1)}, bf16[128,128]{1,0:T(8,128)(2,1)S(1)}, u32[]{:S(2)}, u32[]{:S(2)}) collective-permute-start(bf16[128,128]{1,0:T(8,128)(2,1)S(1)} %shard_map.226.refs_0_), channel_id=1, source_target_pairs={{0,3},{1,0},{2,1},{3,2},{4,7},{5,4},{6,5},{7,6},{8,11},{9,8},{10,9... | collective-permute-start | bytes 98312 | tf_op jit(solution)/shard_map/ppermute | solution.py:26
  84.0 3.2 %collective-permute-done.27.refs_2_ = bf16[128,128]{1,0:T(8,128)(2,1)S(1)} collective-permute-done((bf16[128,128]{1,0:T(8,128)(2,1)S(1)}, bf16[128,128]{1,0:T(8,128)(2,1)S(1)}, u32[]{:S(2)}, u32[]{:S(2)}) %collective-permute-start.27) | collective-permute-done | bytes 32800 | tf_op jit(solution)/shard_map/ppermute | solution.py:26
  88.4 3.4 %all-to-all-start.1 = ((bf16[8,16,512]{2,1,0:T(8,128)(2,1)}), bf16[8,16,512]{2,1,0:T(8,128)(2,1)S(1)}, u32[]{:S(2)}, u32[]{:S(2)}) async-start(bf16[8,16,512]{2,1,0:T(8,128)(2,1)} %bitcast.18), calls=%async_computation.1 | async-start | bytes 262144 | tf_op jit(solution)/shard_map/all_to_all | solution.py:502
  91.9 3.3 %shard_map.222.refs_0_ = bf16[192,256]{1,0:T(8,128)(2,1)} custom-call(bf16[24,2176]{1,0:T(8,128)(2,1)} %copy-done, bf16[24,2176]{1,0:T(8,128)(2,1)} %copy-done.4, bf16[24,2176]{1,0:T(8,128)(2,1)} %copy-done.3, bf16[24,2176]{1,0:T(8,128)(2,1)} %copy-done.2, bf16[24,2176]{1,0:T(8,128)(2,1)} %copy-done.1, bf16[24,2176]{1,0:T(8,128)(2,1)} %copy-done.7, ...), custom_call_target="tpu_custom_call" | custom-call | flops 400000000 | bytes 3000000 | tf_op jit(solution)/shard_map/pallas_call | solution.py:57
  97.2 2.7 %shard_map.224 = (bf16[192,128]{1,0:T(8,128)(2,1)}, bf16[192,128]{1,0:T(8,128)(2,1)}, f32[192,128]{1,0:T(8,128)}) custom-call(bf16[192,128]{1,0:T(8,128)(2,1)} %copy-done.16, bf16[4,2048]{1,0:T(4,128)(2,1)} %bitcast.37, bf16[64,2048]{1,0:T(8,128)(2,1)} %bitcast.36, f32[1,2048]{1,0:T(1,128)} %bitcast.39, bf16[24,2176]{1,0:T(8,128)(2,1)} %copy-done, ...), custom_call_target="tpu_custom_call" | custom-call | flops 60000000 | bytes 1500000 | tf_op jit(solution)/shard_map/pallas_call | solution.py:57
  102.5 2.6 %shard_map.228 = (f32[96,512]{1,0:T(8,128)}, bf16[96,512]{1,0:T(8,128)(2,1)}) custom-call(bf16[192,256]{1,0:T(8,128)(2,1)} %shard_map.222.refs_0_, bf16[192,256]{1,0:T(8,128)(2,1)} %copy-done.25, bf16[192,256]{1,0:T(8,128)(2,1)} %copy-done.24, bf16[192,256]{1,0:T(8,128)(2,1)} %copy-done.23, bf16[384,512]{1,0:T(8,128)(2,1)} %copy-done.18, ...), custom_call_target="tpu_custom_call" | custom-call | flops 400000000 | bytes 2000000 | tf_op jit(solution)/shard_map/pallas_call | solution.py:57
  105.1 6.5 %collective-permute-start.29 = (bf16[96,512]{1,0:T(8,128)(2,1)}, bf16[96,512]{1,0:T(8,128)(2,1)S(1)}, u32[]{:S(2)}, u32[]{:S(2)}) collective-permute-start(bf16[96,512]{1,0:T(8,128)(2,1)} %get-tuple-element.43), channel_id=1, source_target_pairs={{0,4},{4,0},{1,5},{5,1},{2,6},{6,2},{3,7},{7,3},{8,12},{12,8},{9,1... | collective-permute-start | bytes 294920 | tf_op jit(solution)/shard_map/ppermute | solution.py:26
  111.7 1.2 collective-permute-done.29.come_ref
  115.3 1.2 %collective-permute-done.30.refs_0_ = bf16[24,512]{1,0:T(8,128)(2,1)S(1)} collective-permute-done((bf16[24,512]{1,0:T(8,128)(2,1)S(1)}, bf16[24,512]{1,0:T(8,128)(2,1)S(1)}, u32[]{:S(2)}, u32[]{:S(2)}) %collective-permute-start.30) | collective-permute-done | bytes 24608 | tf_op jit(solution)/shard_map/ppermute | solution.py:26
  116.5 1.8 %collective-permute-done.31.refs_1_ = bf16[24,512]{1,0:T(8,128)(2,1)S(1)} collective-permute-done((bf16[24,512]{1,0:T(8,128)(2,1)S(1)}, bf16[24,512]{1,0:T(8,128)(2,1)S(1)}, u32[]{:S(2)}, u32[]{:S(2)}) %collective-permute-start.31) | collective-permute-done | bytes 24608 | tf_op jit(solution)/shard_map/ppermute | solution.py:26
  (110 shorter events, 22.8 us)
Async XLA Ops:
  2.6 5.7 %collective-permute-start.10 = (bf16[64,512]{1,0:T(8,128)(2,1)S(1)}, bf16[64,512]{1,0:T(8,128)(2,1)S(1)}, u32[]{:S(2)}, u32[]{:S(2)}) collective-permute-start(bf16[64,512]{1,0:T(8,128)(2,1)S(1)} %get-tuple-element.30), channel_id=1, source_target_pairs={{0,1},{1,2},{2,3},{3,0},{4,5},{5,6},{6,7},{7,4},{8,9},{9,10},{10,1... | collective-permute-start | bytes 196616 | tf_op jit(solution)/shard_map/ppermute | solution.py:26
  4.7 5.1 %collective-permute-start.11 = (bf16[64,512]{1,0:T(8,128)(2,1)S(1)}, bf16[64,512]{1,0:T(8,128)(2,1)S(1)}, u32[]{:S(2)}, u32[]{:S(2)}) collective-permute-start(bf16[64,512]{1,0:T(8,128)(2,1)S(1)} %get-tuple-element.31), channel_id=1, source_target_pairs={{0,2},{1,3},{2,0},{3,1},{4,6},{5,7},{6,4},{7,5},{8,10},{9,11},{10,... | collective-permute-start | bytes 196616 | tf_op jit(solution)/shard_map/ppermute | solution.py:26
  11.5 13.5 %collective-permute-start.13 = (bf16[384,512]{1,0:T(8,128)(2,1)S(1)}, bf16[384,512]{1,0:T(8,128)(2,1)S(1)}, u32[]{:S(2)}, u32[]{:S(2)}) collective-permute-start(bf16[384,512]{1,0:T(8,128)(2,1)S(1)} %constant_dynamic-update-slice_fusion.refs_8_.refs_4_), channel_id=1, source_target_pairs={{0,32},{32,64},{64,96},{96,128},{128,160},{160,192},{192,224},{224... | collective-permute-start | bytes 1179656 | tf_op jit(solution)/shard_map/ppermute | solution.py:26
  13.4 21.8 %collective-permute-start.14 = (bf16[384,512]{1,0:T(8,128)(2,1)S(1)}, bf16[384,512]{1,0:T(8,128)(2,1)}, u32[]{:S(2)}, u32[]{:S(2)}) collective-permute-start(bf16[384,512]{1,0:T(8,128)(2,1)S(1)} %constant_dynamic-update-slice_fusion.refs_8_.refs_4_), channel_id=1, source_target_pairs={{0,224},{32,0},{64,32},{96,64},{128,96},{160,128},{192,160},{224,1... | collective-permute-start | bytes 1179656 | tf_op jit(solution)/shard_map/ppermute | solution.py:26
  25.0 12.8 %collective-permute-start.15 = (bf16[384,512]{1,0:T(8,128)(2,1)S(1)}, bf16[384,512]{1,0:T(8,128)(2,1)}, u32[]{:S(2)}, u32[]{:S(2)}) collective-permute-start(bf16[384,512]{1,0:T(8,128)(2,1)S(1)} %collective-permute-done.13.refs_9_.refs_5_), channel_id=1, source_target_pairs={{0,32},{32,64},{64,96},{96,128},{128,160},{160,192},{192,224},{224... | collective-permute-start | bytes 1179656 | tf_op jit(solution)/shard_map/ppermute | solution.py:26
  32.7 5.2 %collective-permute-start.2 = (bf16[24,2048]{1,0:T(8,128)(2,1)}, bf16[24,2048]{1,0:T(8,128)(2,1)S(1)}, u32[]{:S(2)}, u32[]{:S(2)}) collective-permute-start(bf16[24,2048]{1,0:T(8,128)(2,1)} %get-tuple-element.27.refs_0_), channel_id=1, source_target_pairs={{0,3},{1,0},{2,1},{3,2},{4,7},{5,4},{6,5},{7,6},{8,11},{9,8},{10,9... | collective-permute-start | bytes 294920 | tf_op jit(solution)/shard_map/ppermute | solution.py:26
  34.6 5.3 %collective-permute-start.1 = (bf16[24,2048]{1,0:T(8,128)(2,1)}, bf16[24,2048]{1,0:T(8,128)(2,1)S(1)}, u32[]{:S(2)}, u32[]{:S(2)}) collective-permute-start(bf16[24,2048]{1,0:T(8,128)(2,1)} %get-tuple-element.27.refs_0_), channel_id=1, source_target_pairs={{0,2},{1,3},{2,0},{3,1},{4,6},{5,7},{6,4},{7,5},{8,10},{9,11},{10,... | collective-permute-start | bytes 294920 | tf_op jit(solution)/shard_map/ppermute | solution.py:26
  34.6 5.9 %collective-permute-start = (bf16[24,2048]{1,0:T(8,128)(2,1)}, bf16[24,2048]{1,0:T(8,128)(2,1)S(1)}, u32[]{:S(2)}, u32[]{:S(2)}) collective-permute-start(bf16[24,2048]{1,0:T(8,128)(2,1)} %get-tuple-element.27.refs_0_), channel_id=1, source_target_pairs={{0,1},{1,2},{2,3},{3,0},{4,5},{5,6},{6,7},{7,4},{8,9},{9,10},{10,1... | collective-permute-start | bytes 294920 | tf_op jit(solution)/shard_map/ppermute | solution.py:26
  35.3 30.8 %collective-permute-start.16 = (bf16[384,512]{1,0:T(8,128)(2,1)}, bf16[384,512]{1,0:T(8,128)(2,1)S(1)}, u32[]{:S(2)}, u32[]{:S(2)}) collective-permute-start(bf16[384,512]{1,0:T(8,128)(2,1)} %collective-permute-done.14.refs_10_.refs_6_), channel_id=1, source_target_pairs={{0,224},{32,0},{64,32},{96,64},{128,96},{160,128},{192,160},{224,1... | collective-permute-start | bytes 1179656 | tf_op jit(solution)/shard_map/ppermute | solution.py:26
  37.8 31.0 %collective-permute-start.17 = (bf16[384,512]{1,0:T(8,128)(2,1)}, bf16[384,512]{1,0:T(8,128)(2,1)S(1)}, u32[]{:S(2)}, u32[]{:S(2)}) collective-permute-start(bf16[384,512]{1,0:T(8,128)(2,1)} %collective-permute-done.15.refs_11_.refs_7_), channel_id=1, source_target_pairs={{0,32},{32,64},{64,96},{96,128},{128,160},{160,192},{192,224},{224... | collective-permute-start | bytes 1179656 | tf_op jit(solution)/shard_map/ppermute | solution.py:26
  41.6 7.3 %collective-permute-start.6 = (bf16[24,2176]{1,0:T(8,128)(2,1)S(1)}, bf16[24,2176]{1,0:T(8,128)(2,1)S(1)}, u32[]{:S(2)}, u32[]{:S(2)}) collective-permute-start(bf16[24,2176]{1,0:T(8,128)(2,1)S(1)} %get-tuple-element.28.refs_0_), channel_id=1, source_target_pairs={{0,4},{4,0},{1,5},{5,1},{2,6},{6,2},{3,7},{7,3},{8,12},{12,8},{9,1... | collective-permute-start | bytes 313352 | tf_op jit(solution)/shard_map/ppermute | solution.py:26
  45.8 6.8 %collective-permute-start.5 = (bf16[24,2176]{1,0:T(8,128)(2,1)S(1)}, bf16[24,2176]{1,0:T(8,128)(2,1)S(1)}, u32[]{:S(2)}, u32[]{:S(2)}) collective-permute-start(bf16[24,2176]{1,0:T(8,128)(2,1)S(1)} %get-tuple-element.28.refs_0_), channel_id=1, source_target_pairs={{0,24},{8,0},{16,8},{24,16},{1,25},{9,1},{17,9},{25,17},{2,26},{10... | collective-permute-start | bytes 313352 | tf_op jit(solution)/shard_map/ppermute | solution.py:26
  48.6 5.4 %collective-permute-start.4 = (bf16[24,2176]{1,0:T(8,128)(2,1)S(1)}, bf16[24,2176]{1,0:T(8,128)(2,1)S(1)}, u32[]{:S(2)}, u32[]{:S(2)}) collective-permute-start(bf16[24,2176]{1,0:T(8,128)(2,1)S(1)} %get-tuple-element.28.refs_0_), channel_id=1, source_target_pairs={{0,16},{8,24},{16,0},{24,8},{1,17},{9,25},{17,1},{25,9},{2,18},{10... | collective-permute-start | bytes 313352 | tf_op jit(solution)/shard_map/ppermute | solution.py:26
  48.9 8.2 %collective-permute-start.3 = (bf16[24,2176]{1,0:T(8,128)(2,1)S(1)}, bf16[24,2176]{1,0:T(8,128)(2,1)S(1)}, u32[]{:S(2)}, u32[]{:S(2)}) collective-permute-start(bf16[24,2176]{1,0:T(8,128)(2,1)S(1)} %get-tuple-element.28.refs_0_), channel_id=1, source_target_pairs={{0,8},{8,16},{16,24},{24,0},{1,9},{9,17},{17,25},{25,1},{2,10},{10... | collective-permute-start | bytes 313352 | tf_op jit(solution)/shard_map/ppermute | solution.py:26
  52.7 5.0 %collective-permute-start.9 = (bf16[24,2176]{1,0:T(8,128)(2,1)S(1)}, bf16[24,2176]{1,0:T(8,128)(2,1)S(1)}, u32[]{:S(2)}, u32[]{:S(2)}) collective-permute-start(bf16[24,2176]{1,0:T(8,128)(2,1)S(1)} %collective-permute-done.5.refs_3_), channel_id=1, source_target_pairs={{0,4},{4,0},{1,5},{5,1},{2,6},{6,2},{3,7},{7,3},{8,12},{12,8},{9,1... | collective-permute-start | bytes 313352 | tf_op jit(solution)/shard_map/ppermute | solution.py:26
  54.0 3.7 %collective-permute-start.8 = (bf16[24,2176]{1,0:T(8,128)(2,1)S(1)}, bf16[24,2176]{1,0:T(8,128)(2,1)S(1)}, u32[]{:S(2)}, u32[]{:S(2)}) collective-permute-start(bf16[24,2176]{1,0:T(8,128)(2,1)S(1)} %collective-permute-done.4.refs_2_), channel_id=1, source_target_pairs={{0,4},{4,0},{1,5},{5,1},{2,6},{6,2},{3,7},{7,3},{8,12},{12,8},{9,1... | collective-permute-start | bytes 313352 | tf_op jit(solution)/shard_map/ppermute | solution.py:26
  60.4 13.7 %all-to-all-start = ((bf16[8,16,512]{2,1,0:T(8,128)(2,1)}), bf16[8,16,512]{2,1,0:T(8,128)(2,1)S(1)}, u32[]{:S(2)}, u32[]{:S(2)}) async-start(bf16[8,16,512]{2,1,0:T(8,128)(2,1)} %bitcast.13), calls=%async_computation | async-start | bytes 262144 | tf_op jit(solution)/shard_map/all_to_all | solution.py:502
  66.1 25.6 %collective-permute-start.18 = (bf16[384,512]{1,0:T(8,128)(2,1)S(1)}, bf16[384,512]{1,0:T(8,128)(2,1)}, u32[]{:S(2)}, u32[]{:S(2)}) collective-permute-start(bf16[384,512]{1,0:T(8,128)(2,1)S(1)} %collective-permute-done.16.refs_12_.refs_8_), channel_id=1, source_target_pairs={{0,224},{32,0},{64,32},{96,64},{128,96},{160,128},{192,160},{224,1... | collective-permute-start | bytes 1179656 | tf_op jit(solution)/shard_map/ppermute | solution.py:26
  68.8 22.9 %collective-permute-start.19 = (bf16[384,512]{1,0:T(8,128)(2,1)S(1)}, bf16[384,512]{1,0:T(8,128)(2,1)}, u32[]{:S(2)}, u32[]{:S(2)}) collective-permute-start(bf16[384,512]{1,0:T(8,128)(2,1)S(1)} %collective-permute-done.17.refs_13_.refs_9_), channel_id=1, source_target_pairs={{0,32},{32,64},{64,96},{96,128},{128,160},{160,192},{192,224},{224... | collective-permute-start | bytes 1179656 | tf_op jit(solution)/shard_map/ppermute | solution.py:26
  74.4 5.5 %collective-permute-start.23 = (bf16[128,256]{1,0:T(8,128)(2,1)S(1)}, bf16[128,256]{1,0:T(8,128)(2,1)S(1)}, u32[]{:S(2)}, u32[]{:S(2)}) collective-permute-start(bf16[128,256]{1,0:T(8,128)(2,1)S(1)} %get-tuple-element.37), channel_id=1, source_target_pairs={{0,1},{1,2},{2,3},{3,0},{4,5},{5,6},{6,7},{7,4},{8,9},{9,10},{10,1... | collective-permute-start | bytes 196616 | tf_op jit(solution)/shard_map/ppermute | solution.py:26
  74.5 5.4 %collective-permute-start.24 = (bf16[128,256]{1,0:T(8,128)(2,1)S(1)}, bf16[128,256]{1,0:T(8,128)(2,1)S(1)}, u32[]{:S(2)}, u32[]{:S(2)}) collective-permute-start(bf16[128,256]{1,0:T(8,128)(2,1)S(1)} %get-tuple-element.38), channel_id=1, source_target_pairs={{0,2},{1,3},{2,0},{3,1},{4,6},{5,7},{6,4},{7,5},{8,10},{9,11},{10,... | collective-permute-start | bytes 196616 | tf_op jit(solution)/shard_map/ppermute | solution.py:26
  76.2 4.2 %collective-permute-start.25 = (bf16[128,256]{1,0:T(8,128)(2,1)S(1)}, bf16[128,256]{1,0:T(8,128)(2,1)S(1)}, u32[]{:S(2)}, u32[]{:S(2)}) collective-permute-start(bf16[128,256]{1,0:T(8,128)(2,1)S(1)} %get-tuple-element.39), channel_id=1, source_target_pairs={{0,3},{1,0},{2,1},{3,2},{4,7},{5,4},{6,5},{7,6},{8,11},{9,8},{10,9... | collective-permute-start | bytes 196616 | tf_op jit(solution)/shard_map/ppermute | solution.py:26
  80.5 3.5 %collective-permute-start.28 = (bf16[128,128]{1,0:T(8,128)(2,1)S(1)}, bf16[128,128]{1,0:T(8,128)(2,1)S(1)}, u32[]{:S(2)}, u32[]{:S(2)}) collective-permute-start(bf16[128,128]{1,0:T(8,128)(2,1)S(1)} %shard_map.226.refs_0_), channel_id=1, source_target_pairs={{0,3},{1,0},{2,1},{3,2},{4,7},{5,4},{6,5},{7,6},{8,11},{9,8},{10,9... | collective-permute-start | bytes 98312 | tf_op jit(solution)/shard_map/ppermute | solution.py:26
  82.9 4.4 %collective-permute-start.27 = (bf16[128,128]{1,0:T(8,128)(2,1)S(1)}, bf16[128,128]{1,0:T(8,128)(2,1)S(1)}, u32[]{:S(2)}, u32[]{:S(2)}) collective-permute-start(bf16[128,128]{1,0:T(8,128)(2,1)S(1)} %shard_map.226.refs_0_), channel_id=1, source_target_pairs={{0,2},{1,3},{2,0},{3,1},{4,6},{5,7},{6,4},{7,5},{8,10},{9,11},{10,... | collective-permute-start | bytes 98312 | tf_op jit(solution)/shard_map/ppermute | solution.py:26
  83.1 4.3 %collective-permute-start.26 = (bf16[128,128]{1,0:T(8,128)(2,1)S(1)}, bf16[128,128]{1,0:T(8,128)(2,1)S(1)}, u32[]{:S(2)}, u32[]{:S(2)}) collective-permute-start(bf16[128,128]{1,0:T(8,128)(2,1)S(1)} %shard_map.226.refs_0_), channel_id=1, source_target_pairs={{0,1},{1,2},{2,3},{3,0},{4,5},{5,6},{6,7},{7,4},{8,9},{9,10},{10,1... | collective-permute-start | bytes 98312 | tf_op jit(solution)/shard_map/ppermute | solution.py:26
  88.4 11.6 %all-to-all-start.1 = ((bf16[8,16,512]{2,1,0:T(8,128)(2,1)}), bf16[8,16,512]{2,1,0:T(8,128)(2,1)S(1)}, u32[]{:S(2)}, u32[]{:S(2)}) async-start(bf16[8,16,512]{2,1,0:T(8,128)(2,1)} %bitcast.18), calls=%async_computation.1 | async-start | bytes 262144 | tf_op jit(solution)/shard_map/all_to_all | solution.py:502
  95.2 4.7 %collective-permute-start.22 = (bf16[192,256]{1,0:T(8,128)(2,1)}, bf16[192,256]{1,0:T(8,128)(2,1)S(1)}, u32[]{:S(2)}, u32[]{:S(2)}) collective-permute-start(bf16[192,256]{1,0:T(8,128)(2,1)} %shard_map.222.refs_0_), channel_id=1, source_target_pairs={{0,3},{1,0},{2,1},{3,2},{4,7},{5,4},{6,5},{7,6},{8,11},{9,8},{10,9... | collective-permute-start | bytes 294920 | tf_op jit(solution)/shard_map/ppermute | solution.py:26
  95.5 5.2 %collective-permute-start.21 = (bf16[192,256]{1,0:T(8,128)(2,1)}, bf16[192,256]{1,0:T(8,128)(2,1)S(1)}, u32[]{:S(2)}, u32[]{:S(2)}) collective-permute-start(bf16[192,256]{1,0:T(8,128)(2,1)} %shard_map.222.refs_0_), channel_id=1, source_target_pairs={{0,2},{1,3},{2,0},{3,1},{4,6},{5,7},{6,4},{7,5},{8,10},{9,11},{10,... | collective-permute-start | bytes 294920 | tf_op jit(solution)/shard_map/ppermute | solution.py:26
  96.4 5.5 %collective-permute-start.20 = (bf16[192,256]{1,0:T(8,128)(2,1)}, bf16[192,256]{1,0:T(8,128)(2,1)S(1)}, u32[]{:S(2)}, u32[]{:S(2)}) collective-permute-start(bf16[192,256]{1,0:T(8,128)(2,1)} %shard_map.222.refs_0_), channel_id=1, source_target_pairs={{0,1},{1,2},{2,3},{3,0},{4,5},{5,6},{6,7},{7,4},{8,9},{9,10},{10,1... | collective-permute-start | bytes 294920 | tf_op jit(solution)/shard_map/ppermute | solution.py:26
  105.1 7.7 %collective-permute-start.29 = (bf16[96,512]{1,0:T(8,128)(2,1)}, bf16[96,512]{1,0:T(8,128)(2,1)S(1)}, u32[]{:S(2)}, u32[]{:S(2)}) collective-permute-start(bf16[96,512]{1,0:T(8,128)(2,1)} %get-tuple-element.43), channel_id=1, source_target_pairs={{0,4},{4,0},{1,5},{5,1},{2,6},{6,2},{3,7},{7,3},{8,12},{12,8},{9,1... | collective-permute-start | bytes 294920 | tf_op jit(solution)/shard_map/ppermute | solution.py:26
  114.1 4.2 %collective-permute-start.31 = (bf16[24,512]{1,0:T(8,128)(2,1)S(1)}, bf16[24,512]{1,0:T(8,128)(2,1)S(1)}, u32[]{:S(2)}, u32[]{:S(2)}) collective-permute-start(bf16[24,512]{1,0:T(8,128)(2,1)S(1)} %get-tuple-element.47), channel_id=1, source_target_pairs={{0,16},{8,24},{16,0},{24,8},{1,17},{9,25},{17,1},{25,9},{2,18},{10... | collective-permute-start | bytes 73736 | tf_op jit(solution)/shard_map/ppermute | solution.py:26
  114.5 4.4 %collective-permute-start.32 = (bf16[24,512]{1,0:T(8,128)(2,1)S(1)}, bf16[24,512]{1,0:T(8,128)(2,1)S(1)}, u32[]{:S(2)}, u32[]{:S(2)}) collective-permute-start(bf16[24,512]{1,0:T(8,128)(2,1)S(1)} %get-tuple-element.48), channel_id=1, source_target_pairs={{0,8},{8,16},{16,24},{24,0},{1,9},{9,17},{17,25},{25,1},{2,10},{10... | collective-permute-start | bytes 73736 | tf_op jit(solution)/shard_map/ppermute | solution.py:26
  (30 other events, 597.7 us)
